TPU v7x, 512 devices: a whole 4x8x8 slice. The times are simulated.
512 devices in a mesh: ep: 128 (over z, y, core), tp: 4 (over x).
Axes of the slice: x: 4, y: 8, z: 8, core: 2. Of those that a mesh axis runs over, the one named last changes fastest.
Arguments:
- tokens: bfloat16 [16384, 2048], P('ep'), may hold values from -6 to 6
- cotangent: bfloat16 [16384, 2048], P('ep'), may hold values from -6 to 6
- route_weights: float32 [16384, 2], P('ep'), may hold values from 0.25 to 2.5
- routes: int32 [16384, 2], P('ep'), may hold values from 0 to 127, all different within a row; in each aligned block of 128 rows (0 to 127, 128 to 255, ...) at most 4 rows name the same one
- gate_proj: bfloat16 [128, 2048, 512], P('ep', None, 'tp'), may hold values from -0.125 to 0.125
- up_proj: bfloat16 [128, 2048, 512], P('ep', None, 'tp'), may hold values from -0.125 to 0.125
- down_proj: bfloat16 [128, 512, 2048], P('ep', 'tp'), may hold values from -0.25 to 0.25
- shared_down: bfloat16 [2048, 512], P(None, 'tp'), may hold values from -0.25 to 0.25
- shared_hidden: bfloat16 [16384, 512], P('ep', 'tp'), may hold values from -0.29882812 to 0.29882812
Outputs:
- tokens_grad: bfloat16 [16384, 2048], P('ep', 'tp')
- weights_grad: float32 [16384, 2], P('ep')
- gate_proj_grad: bfloat16 [128, 2048, 512], P('ep', None, 'tp')
- up_proj_grad: bfloat16 [128, 2048, 512], P('ep', None, 'tp')
- down_proj_grad: bfloat16 [128, 512, 2048], P('ep', 'tp')
- hidden_grad: bfloat16 [16384, 512], P('ep', 'tp')
- shared_grad: float32 [2048, 512], P('ep', 'tp')
Inputs may be any that keep to these rules, and one draw needn't show every extreme that they name: `routes`: in each aligned block of 128 rows no expert is named more than 4 times, a bound that some block reaches; the 2 experts of a row differ.
All inputs are finite; a program needn't handle non-finite values.
Results may differ from a plain program's by a relative error of at most 0.012.
Values may be sent and summed in bfloat16 or wider, within the bound.
No kernel may reach another device: no remote copies, remote signals or barrier semaphores. Data moves between devices by JAX's collectives and lax.ppermute only.
A program may use at most 64 MiB of HBM per device.

v0:
```python
import jax
import jax.numpy as jnp
from jax import lax
from jax.sharding import Mesh
from jax.sharding import PartitionSpec as P

EP = ("ep_0", "ep_1", "ep_2")


def in_one_piece(arrays, axis, split_dim, concat_dim, along):
    columns = [a.reshape(*a.shape[:along], -1) for a in arrays]
    both = jnp.concatenate(columns, axis=along)
    out, at, finished = (
        lax.all_to_all(both, axis, split_axis=split_dim, concat_axis=concat_dim, tiled=True),
        0,
        [],
    )
    for a, column in zip(arrays, columns):
        share = out[..., at : at + column.shape[along]]
        finished.append(share.reshape(*share.shape[:along], *a.shape[along:]))
        at += column.shape[along]
    return tuple(finished)


def side_by_side(arrays, axis, dim, along):
    widths = [a.shape[along] for a in arrays]
    both = jnp.concatenate(arrays, axis=along)
    out = lax.all_gather(both, axis, axis=dim, tiled=True)
    return tuple(jnp.split(out, [sum(widths[:k]) for k in range(1, len(widths))], axis=along))


def cut_along(array, dim, size):
    before, after = (array.shape[:dim], array.shape[dim + 1 :])
    return jnp.moveaxis(array.reshape(*before, size, -1, *after), dim, 0)


def summed_on_arrival(array, axis, dim):
    size = lax.axis_size(axis)
    tiles = lax.all_to_all(cut_along(array, dim, size), axis, 0, 0, tiled=True)
    return jnp.sum(tiles.astype(jnp.float32), axis=0)


def own_block(tiles, axes, order):
    lengths = [lax.axis_size(a) for a in axes]
    tiles = tiles.reshape(*lengths, *tiles.shape[1:])
    tiles = tiles.transpose(*order, *range(len(axes), tiles.ndim))
    tiles = tiles.reshape(-1, *tiles.shape[len(axes) :])
    for k in order:
        tiles = lax.psum_scatter(tiles, axes[k], scatter_dimension=0, tiled=True)
    return tiles[0]


def summed_rows(array, axes, order, dim):
    size = lax.axis_size(axes)
    return own_block(cut_along(array, dim, size), axes, order)


def shards(
    tokens,
    cotangent,
    route_weights,
    routes,
    gate_proj,
    up_proj,
    down_proj,
    shared_down,
    shared_hidden,
):
    tok_rows, feat_width = tokens.shape
    top_count = routes.shape[1]
    exp_local = gate_proj.shape[0]
    ep_size = lax.axis_size(EP)
    tp_size = lax.axis_size("tp")
    exp_total = exp_local * ep_size
    capacity = 2 * tok_rows * top_count // exp_total
    quarter = feat_width // tp_size
    filled = exp_total * capacity
    flat_routes = routes.reshape(-1)
    one_hot = (flat_routes[:, None] == jnp.arange(exp_total, dtype=jnp.int32)[None, :]).astype(
        jnp.int32
    )
    rank_in = jnp.sum((jnp.cumsum(one_hot, axis=0) - one_hot) * one_hot, axis=1)
    slot_ids = flat_routes * capacity + rank_in
    route_owner = jnp.arange(flat_routes.shape[0], dtype=jnp.int32) // top_count
    owner_ids = jnp.full((filled,), tok_rows, jnp.int32).at[slot_ids].set(route_owner)
    sent_weights = (
        jnp.zeros((filled,), jnp.bfloat16)
        .at[slot_ids]
        .set(route_weights.reshape(-1).astype(jnp.bfloat16))
    )
    first_col = lax.axis_index("tp") * quarter
    own_rows = lax.dynamic_slice_in_dim(tokens, first_col, quarter, 1)
    own_grads = lax.dynamic_slice_in_dim(cotangent, first_col, quarter, 1)
    sent_rows = jnp.take(own_rows, owner_ids, axis=0, mode="fill", fill_value=0)
    sent_grads = jnp.take(own_grads, owner_ids, axis=0, mode="fill", fill_value=0)
    got_rows, got_grads, got_weights = in_one_piece(
        (sent_rows, sent_grads, sent_weights), EP, 0, 0, 1
    )
    got_rows, got_grads = side_by_side((got_rows, got_grads), "tp", 1, 0)
    slot_rows = got_rows.reshape(ep_size, exp_local, capacity, feat_width)
    slot_grads = got_grads.reshape(ep_size, exp_local, capacity, feat_width)
    weight_col = got_weights.reshape(ep_size, exp_local, capacity, 1).astype(jnp.float32)
    gate = jnp.einsum("secd,edf->secf", slot_rows, gate_proj, preferred_element_type=jnp.float32)
    upper = jnp.einsum("secd,edf->secf", slot_rows, up_proj, preferred_element_type=jnp.float32)
    active = jax.nn.silu(gate)
    hidden = (active * upper).astype(jnp.bfloat16)
    backed = jnp.einsum("secd,efd->secf", slot_grads, down_proj, preferred_element_type=jnp.float32)
    gate_share = jnp.sum(hidden.astype(jnp.float32) * backed, axis=3)
    d_hidden = weight_col * backed
    sigma = jax.nn.sigmoid(gate)
    d_gate = (d_hidden * upper * sigma * (1.0 + gate * (1.0 - sigma))).astype(jnp.bfloat16)
    d_up = (d_hidden * active).astype(jnp.bfloat16)
    scaled = (weight_col * slot_grads).astype(jnp.bfloat16)
    down_proj_grad = jnp.einsum(
        "secf,secd->efd", hidden, scaled, preferred_element_type=jnp.float32
    ).astype(jnp.bfloat16)
    gate_proj_grad = jnp.einsum(
        "secd,secf->edf", slot_rows, d_gate, preferred_element_type=jnp.float32
    ).astype(jnp.bfloat16)
    up_proj_grad = jnp.einsum(
        "secd,secf->edf", slot_rows, d_up, preferred_element_type=jnp.float32
    ).astype(jnp.bfloat16)
    partial_value = jnp.einsum(
        "secf,edf->secd", d_gate, gate_proj, preferred_element_type=jnp.float32
    )
    partial_value = partial_value + jnp.einsum(
        "secf,edf->secd", d_up, up_proj, preferred_element_type=jnp.float32
    )
    gate_whole = lax.psum(gate_share, "tp")
    input_cols = summed_on_arrival(partial_value.astype(jnp.bfloat16), "tp", 3).astype(jnp.bfloat16)
    back_cols, back_gate = (
        lax.all_to_all(
            input_cols.reshape(filled, quarter), EP, split_axis=0, concat_axis=0, tiled=True
        ),
        lax.all_to_all(
            gate_whole.astype(jnp.bfloat16).reshape(filled),
            EP,
            split_axis=0,
            concat_axis=0,
            tiled=True,
        ),
    )
    picked = back_cols[slot_ids].reshape(tok_rows, top_count, quarter)
    tokens_grad = jnp.sum(picked.astype(jnp.float32), axis=1).astype(jnp.bfloat16)
    weights_grad = back_gate[slot_ids].astype(jnp.float32).reshape(tok_rows, top_count)
    hidden_grad = jnp.dot(cotangent, shared_down, preferred_element_type=jnp.float32).astype(
        jnp.bfloat16
    )
    shared_grad = summed_rows(
        jnp.einsum("td,th->dh", cotangent, shared_hidden, preferred_element_type=jnp.float32),
        EP,
        (2, 0, 1),
        0,
    )
    return (
        tokens_grad,
        weights_grad,
        gate_proj_grad,
        up_proj_grad,
        down_proj_grad,
        hidden_grad,
        shared_grad,
    )


def solution(mesh):
    split = Mesh(mesh.devices.reshape(8, 8, 2, mesh.shape["tp"]), ("ep_0", "ep_1", "ep_2", "tp"))
    placed = (
        P(EP, None),
        P(EP, None),
        P(EP, None),
        P(EP, None),
        P(EP, None, "tp"),
        P(EP, None, "tp"),
        P(EP, "tp", None),
        P(None, "tp"),
        P(EP, "tp"),
    )
    return jax.shard_map(
        shards,
        mesh=split,
        in_specs=placed,
        out_specs=(
            P(EP, "tp"),
            P(EP, None),
            P(EP, None, "tp"),
            P(EP, None, "tp"),
            P(EP, "tp", None),
            P(EP, "tp"),
            P(EP, "tp"),
        ),
        check_vma=False,
    )
```

profile of v0, /device:TPU:6, one launch (start us, length us, event | category | flops | bytes accessed | tf_op | source)
XLA Modules:
  0.0 244.1 jit_solution(5376992635086670584)
XLA Ops:
  10.7 1.4 scatter_custom_fusion
  13.2 2.2 scatter_custom_fusion.1
  16.6 2.0 gather_fusion.3
  18.6 2.0 gather_fusion.2
  21.5 50.5 %all_to_all.35 = bf16[128,4,1025]{2,1,0:T(4,128)(2,1)S(1)} all-to-all(bf16[128,4,1025]{2,1,0:T(4,128)(2,1)S(1)} %pad_maximum_fusion), channel_id=1, replica_groups=mesh['ep_0'=8,'ep_1'=8,'ep_2'=2,'tp'=4] {'ep_0','ep_1','ep_2'}, dimensions={0} | all-to-all | bytes 2099200 | tf_op jit(solution)/shard_map/all_to_all | solution.py:14
  74.4 1.1 copy.97
  75.9 44.1 %all-gather.2.cloned.1.call-done = bf16[1024,2048]{1,0:T(8,128)(2,1)} async-done(((bf16[1024,512]{1,0:T(8,128)(2,1)}), bf16[1024,2048]{1,0:T(8,128)(2,1)}) %all-gather.2.cloned.1.call-update) | async-done | bytes 4194320 | tf_op jit(solution)/shard_map/all_gather | solution.py:28
  119.9 4.0 %fusion.32 = (bf16[512,2048]{1,0:T(8,128)(2,1)}, bf16[512,2048]{1,0:T(8,128)(2,1)S(1)}) fusion(bf16[1024,2048]{1,0:T(8,128)(2,1)} %all-gather.2.cloned.1.call-done), kind=kLoop, calls=%fused_computation.73 | loop fusion | bytes 8388608 | tf_op jit(solution)/shard_map/split | solution.py:29
  123.9 4.1 %reshape.170 = bf16[128,4,2048]{2,1,0:T(4,128)(2,1)} reshape(bf16[512,2048]{1,0:T(8,128)(2,1)} %get-tuple-element.31) | data formatting | bytes 4194304 | tf_op jit(solution)/shard_map/reshape.6
  128.0 2.2 reshape.172
  130.3 3.4 %copy.92 = bf16[128,4,2048]{0,2,1:T(8,128)(2,1)S(1)} copy(bf16[128,4,2048]{2,1,0:T(4,128)(2,1)} %reshape.172) | data formatting | bytes 4194304 | tf_op jit(solution)/shard_map/reshape.9
  133.7 1.7 convolution_bitcast_fusion.3
  135.5 2.4 fusion.9
  137.9 1.2 multiply_reduce_fusion
  140.7 1.6 copy.116
  142.2 6.7 %all-to-all-start.1 = ((bf16[4,128,1,4,512]{4,1,3,2,0:T(8,128)(2,1)}), bf16[4,128,1,4,512]{4,1,3,2,0:T(8,128)(2,1)}, u32[]{:S(2)}, u32[]{:S(2)}) async-start(bf16[4,128,1,4,512]{4,1,3,2,0:T(8,128)(2,1)} %bitcast.124), calls=%async_computation.1 | async-start | bytes 4194304 | tf_op jit(solution)/shard_map/all_to_all | solution.py:39
  149.5 1.9 convolution_convert_fusion
  151.4 24.1 %psum.7 = bf16[128,1,4]{0,2,1:T(4,128)(2,1)S(1)} all-reduce(f32[128,1,4]{0,2,1:T(4,128)S(1)} %bitcast.136), channel_id=1, replica_groups=mesh['ep_0'=8,'ep_1'=8,'ep_2'=2,'tp'=4] {'tp'}, use_global_device_ids=true, to_apply=%region_8.10 | all-reduce | flops 512 | bytes 3072 | tf_op jit(solution)/shard_map/psum | solution.py:129
  176.3 14.5 %all-to-all-start.3 = ((bf16[128,4,1]{1,2,0:T(2,128)(2,1)}), bf16[128,4,1]{1,2,0:T(2,128)(2,1)S(1)}, u32[]{:S(2)}, u32[]{:S(2)}) async-start(bf16[128,4,1]{1,2,0:T(2,128)(2,1)} %copy.91), calls=%async_computation.3 | async-start | bytes 131072 | tf_op jit(solution)/shard_map/all_to_all | solution.py:135
  190.9 3.7 %reduce-scatter.6.cloned.1.call-done = f32[8,16,128]{2,1,0:T(8,128)} async-done(((f32[64,16,128]{2,1,0:T(8,128)}), f32[8,16,128]{2,1,0:T(8,128)}) %reduce-scatter.6.cloned.1.call-update) | async-done | bytes 65552 | tf_op jit(solution)/shard_map/reduce_scatter | solution.py:49
  194.7 2.0 reduce_sum.48
  196.7 1.2 copy.90
  197.9 4.1 %all-to-all-done.3 = bf16[128,4,1]{1,2,0:T(2,128)(2,1)S(1)} async-done(((bf16[128,4,1]{1,2,0:T(2,128)(2,1)}), bf16[128,4,1]{1,2,0:T(2,128)(2,1)S(1)}, u32[]{:S(2)}, u32[]{:S(2)}) %all-to-all-start.3) | async-done | bytes 1056 | tf_op jit(solution)/shard_map/all_to_all | solution.py:135
  201.9 7.5 %all-to-all-start.2 = ((bf16[128,4,512]{2,1,0:T(4,128)(2,1)}), bf16[128,4,512]{2,1,0:T(4,128)(2,1)S(1)}, u32[]{:S(2)}, u32[]{:S(2)}) async-start(bf16[128,4,512]{2,1,0:T(4,128)(2,1)} %copy.90), calls=%async_computation.2 | async-start | bytes 1048576 | tf_op jit(solution)/shard_map/all_to_all | solution.py:132
  209.5 1.5 fusion.5
  211.9 3.3 %fusion.3 = bf16[1,128,2048]{2,1,0:T(8,128)(2,1)} fusion(bf16[128,4,2048]{2,1,0:T(4,128)(2,1)S(1)} %multiply_convert_fusion, bf16[128,1,4,128]{0,3,2,1:T(8,128)(2,1)S(1)} %copy-done.7), kind=kOutput, calls=%fused_computation.14 | convolution fusion | flops 268697600 | bytes 2752512 | tf_op jit(solution)/shard_map/secf,secd->efd/dot_general | solution.py:114
  215.2 1.5 fusion.4
  217.0 1.9 gather_fusion.1
  219.7 9.1 %all-to-all-done.2 = bf16[128,4,512]{2,1,0:T(4,128)(2,1)S(1)} async-done(((bf16[128,4,512]{2,1,0:T(4,128)(2,1)}), bf16[128,4,512]{2,1,0:T(4,128)(2,1)S(1)}, u32[]{:S(2)}, u32[]{:S(2)}) %all-to-all-start.2) | async-done | bytes 524320 | tf_op jit(solution)/shard_map/all_to_all | solution.py:132
  229.0 1.2 gather_fusion
  230.3 1.3 reduce_sum.49
  231.6 4.9 %reduce-scatter.8.cloned.1.call-done = f32[1,16,128]{2,1,0:T(8,128)} async-done(((f32[8,16,128]{2,1,0:T(8,128)}), f32[1,16,128]{2,1,0:T(8,128)}) %reduce-scatter.8.cloned.1.call-update) | async-done | bytes 8208 | tf_op jit(solution)/shard_map/reduce_scatter | solution.py:49
  (73 shorter events, 13.8 us)
Async XLA Ops:
  8.0 129.9 %copy-start = (bf16[1,2048,128]{2,1,0:T(8,128)(2,1)S(1)}, bf16[1,2048,128]{2,1,0:T(8,128)(2,1)}, u32[]{:S(2)}) copy-start(bf16[1,2048,128]{2,1,0:T(8,128)(2,1)} %param.16) | copy-start | bytes 1572868
  8.0 111.9 %all-gather.2.cloned.1.call-start = ((), (), s32[]{:S(2)}) async-start(), calls=%async_computation.7 | async-start | bytes 5242880 | tf_op jit(solution)/shard_map/all_gather | solution.py:28
  72.7 1.3 copy-start.3
  72.7 1.3 copy-start.5
  73.8 75.1 %reduce-scatter.4.cloned.1.call-start = ((), (), s32[]{:S(2)}) async-start(), calls=%async_computation.8 | async-start | bytes 1572864 | tf_op jit(solution)/shard_map/reduce_scatter | solution.py:49
  133.7 1.7 copy-start.1
  133.7 1.8 copy-start.6
  137.9 1.3 copy-start.4
  142.2 34.1 %all-to-all-start.1 = ((bf16[4,128,1,4,512]{4,1,3,2,0:T(8,128)(2,1)}), bf16[4,128,1,4,512]{4,1,3,2,0:T(8,128)(2,1)}, u32[]{:S(2)}, u32[]{:S(2)}) async-start(bf16[4,128,1,4,512]{4,1,3,2,0:T(8,128)(2,1)} %bitcast.124), calls=%async_computation.1 | async-start | bytes 4194304 | tf_op jit(solution)/shard_map/all_to_all | solution.py:39
  148.9 45.7 %reduce-scatter.6.cloned.1.call-start = ((), (), s32[]{:S(2)}) async-start(), calls=%async_computation.9 | async-start | bytes 589824 | tf_op jit(solution)/shard_map/reduce_scatter | solution.py:49
  176.3 25.6 %all-to-all-start.3 = ((bf16[128,4,1]{1,2,0:T(2,128)(2,1)}), bf16[128,4,1]{1,2,0:T(2,128)(2,1)S(1)}, u32[]{:S(2)}, u32[]{:S(2)}) async-start(bf16[128,4,1]{1,2,0:T(2,128)(2,1)} %copy.91), calls=%async_computation.3 | async-start | bytes 131072 | tf_op jit(solution)/shard_map/all_to_all | solution.py:135
  190.8 45.6 %reduce-scatter.8.cloned.1.call-start = ((), (), s32[]{:S(2)}) async-start(), calls=%async_computation.10 | async-start | bytes 73728 | tf_op jit(solution)/shard_map/reduce_scatter | solution.py:49
  201.9 26.9 %all-to-all-start.2 = ((bf16[128,4,512]{2,1,0:T(4,128)(2,1)}), bf16[128,4,512]{2,1,0:T(4,128)(2,1)S(1)}, u32[]{:S(2)}, u32[]{:S(2)}) async-start(bf16[128,4,512]{2,1,0:T(4,128)(2,1)} %copy.90), calls=%async_computation.2 | async-start | bytes 1048576 | tf_op jit(solution)/shard_map/all_to_all | solution.py:132
  209.5 1.6 copy-start.2
  211.0 0.9 copy-start.7
Sparse Core Ops, SparseCore 0:
  73.9 45.9 all-gather.1
Sparse Core Ops, SparseCore 1:
  77.1 10.6 reduce-scatter.3
  152.2 42.4 reduce-scatter.5
  197.9 38.5 reduce-scatter.7
where the time goes:
time: 245 us; the launch traced here: 244 us
  blocking collectives  74.6 us (30%)
  waiting for transfers between devices  66.5 us (27%)
  local copies, waits for them, and re-layouts  34.4 us (14%)
  starting transfers between devices  29 us (12%)
  between operations  16 us (7%)
  matrix products  15.3 us (6%)
  other arithmetic  8.14 us (3%)
    all_to_all x1, blocking collectives, in_one_piece(): lax.all_to_all(both, axis, split_axis=split_dim, concat_axis=concat_dim,...  50.5 us
    all_gather x1, waiting for transfers between devices, side_by_side(): out = lax.all_gather(both, axis, axis=dim, tiled=True)  44.1 us
    psum x1, blocking collectives, shards(): gate_whole = lax.psum(gate_share, 'tp')  24.1 us
    all_to_all x1, starting transfers between devices, shards(): lax.all_to_all(gate_whole.astype(jnp.bfloat16).reshape(filled), EP, split...  14.5 us
    another operation x6, local copies, waits for them, and re-layouts  9.77 us
    all_to_all x1, waiting for transfers between devices, shards(): lax.all_to_all(input_cols.reshape(filled, quarter), EP, split_axis=0, con...  9.14 us
    reduce_scatter x3, waiting for transfers between devices, own_block(): tiles = lax.psum_scatter(tiles, axes[k], scatter_dimension=0, tiled=True)  8.6 us
    all_to_all x1, starting transfers between devices, shards(): lax.all_to_all(input_cols.reshape(filled, quarter), EP, split_axis=0, con...  7.51 us
  transfers between devices with their start and end apart: 7, of which 5 were waited for; matrix products, arithmetic and copies ran while one was open for 17% of the time, Pallas kernels for 0%

commit v1 on v0

v1 whole, which is shorter than its diff:
```python
import functools

import jax
import jax.numpy as jnp
from jax import lax
from jax.experimental import pallas as pl
from jax.experimental.pallas import tpu as pltpu
from jax.sharding import PartitionSpec as P

F32 = jnp.float32
BF16 = jnp.bfloat16
ROWS = (((0,), (0,)), ((), ()))
LAST = (((1,), (1,)), ((), ()))
VMEM = pl.BlockSpec(memory_space=pltpu.VMEM)
SMEM = pl.BlockSpec(memory_space=pltpu.SMEM)


def exchange(array, axis):
    return lax.all_to_all(array, axis, split_axis=0, concat_axis=0, tiled=True)


def mm(a, b, dims=(((1,), (0,)), ((), ()))):
    return lax.dot_general(a, b, dims, preferred_element_type=F32)


def chosen(routes_ref, slots, capacity):
    count = routes_ref.shape[1]
    row = lax.broadcasted_iota(jnp.int32, (slots, count), 0)
    expert = row // capacity
    first = expert == routes_ref[0:1, :]
    second = expert == routes_ref[1:2, :]
    named = jnp.where(first | second, 1.0, 0.0)
    earlier = lax.broadcasted_iota(jnp.int32, (count, count), 0)
    later = lax.broadcasted_iota(jnp.int32, (count, count), 1)
    before = jnp.where(earlier < later, 1.0, 0.0).astype(BF16)
    rank = mm(named.astype(BF16), before)
    place = (row - expert * capacity).astype(F32)
    hit = jnp.where(rank == place, named, 0.0)
    return hit, jnp.where(first, hit, 0.0), jnp.where(second, hit, 0.0)


def dispatch_kernel(col, routes_ref, weights_ref, tok_ref, cot_ref, x_ref, g_ref, pick_ref, *, cap):
    slots = x_ref.shape[0]
    hit, one, two = chosen(routes_ref, slots, cap)
    weights = weights_ref[...].astype(BF16).astype(F32)
    weight = jnp.sum(one * weights[0:1, :] + two * weights[1:2, :], axis=1, keepdims=True)
    pick = hit.astype(BF16)
    pick_ref[...] = pick
    x_ref[...] = mm(pick, tok_ref[...]).astype(BF16)
    g_ref[...] = (weight * mm(pick, cot_ref[...])).astype(BF16)


def dispatch(col, routes, weights, tokens, cotangent, slots, cap, quarter):
    rows = tokens.shape[0]
    whole = lambda *shape: pl.BlockSpec(shape, lambda i, col: (0,) * len(shape))
    part = pl.BlockSpec((rows, quarter), lambda i, col: (0, col[0]))
    return pl.pallas_call(
        functools.partial(dispatch_kernel, cap=cap),
        grid_spec=pltpu.PrefetchScalarGridSpec(
            num_scalar_prefetch=1,
            grid=(1,),
            in_specs=[whole(*routes.shape), whole(*weights.shape), part, part],
            out_specs=[whole(slots, quarter), whole(slots, quarter), whole(slots, rows)],
        ),
        out_shape=[
            jax.ShapeDtypeStruct((slots, quarter), BF16),
            jax.ShapeDtypeStruct((slots, quarter), BF16),
            jax.ShapeDtypeStruct((slots, rows), BF16),
        ],
        name="dispatch",
    )(col, routes, weights, tokens, cotangent)


def beside(ref):
    return jnp.concatenate([ref[k] for k in range(ref.shape[0])], axis=1)


def stacked(ref):
    return ref[...].reshape(-1, ref.shape[-1])


def local(kernel, out, name, *args, smem=0):
    return pl.pallas_call(
        kernel,
        in_specs=[SMEM] * smem + [VMEM] * (len(args) - smem),
        out_specs=jax.tree.map(lambda _: VMEM, out),
        out_shape=out,
        name=name,
    )(*args)


def partial_kernel(x_ref, g_ref, gate_ref, up_ref, down_ref, y_ref):
    hidden = y_ref.shape[1] // 3
    x = x_ref[...]
    y_ref[:, :hidden] = mm(x, beside(gate_ref)).astype(BF16)
    y_ref[:, hidden : 2 * hidden] = mm(x, beside(up_ref)).astype(BF16)
    y_ref[:, 2 * hidden :] = mm(g_ref[...], stacked(down_ref), LAST).astype(BF16)


def middle_kernel(col, y_ref, grads_ref, hidden_ref, share_ref):
    parts, rows, width = y_ref.shape
    hidden = width // 3
    total = y_ref[0].astype(F32)
    for k in range(1, parts):
        total = total + y_ref[k].astype(F32)
    gate = total[:, :hidden]
    upper = total[:, hidden : 2 * hidden]
    backed = total[:, 2 * hidden :]
    sigma = jax.nn.sigmoid(gate)
    active = gate * sigma
    hid = (active * upper).astype(BF16)
    d_gate = (backed * upper * sigma * (1.0 + gate * (1.0 - sigma))).astype(BF16)
    d_up = (backed * active).astype(BF16)
    share = jnp.sum(hid.astype(F32) * backed, axis=1, keepdims=True)
    share = jnp.broadcast_to(share, (rows, share_ref.shape[1]))
    for k in range(parts):
        grads_ref[k, :, :hidden] = d_gate
        grads_ref[k, :, hidden:] = d_up
        hidden_ref[k] = hid
        share_ref[k * rows : (k + 1) * rows, :] = jnp.where(col[0] == k, share, 0.0).astype(BF16)


def input_kernel(grads_ref, gate_ref, up_ref, out_ref):
    hidden = grads_ref.shape[2] // 2
    grads = stacked(grads_ref)
    out = mm(grads[:, :hidden], beside(gate_ref), LAST)
    out = out + mm(grads[:, hidden:], beside(up_ref), LAST)
    out_ref[...] = out.astype(BF16)


def weight_kernel(x_ref, grads_ref, gate_ref, up_ref):
    parts, _, block = gate_ref.shape
    hidden = grads_ref.shape[2] // 2
    grads = stacked(grads_ref)
    out = mm(x_ref[...], grads, ROWS).astype(BF16)
    for k in range(parts):
        gate_ref[k] = out[:, k * block : (k + 1) * block]
        up_ref[k] = out[:, hidden + k * block : hidden + (k + 1) * block]


def down_kernel(hidden_ref, g_ref, out_ref):
    out = mm(stacked(hidden_ref), g_ref[...], ROWS).astype(BF16)
    out_ref[...] = out.reshape(out_ref.shape)


def share_kernel(routes_ref, weights_ref, share_ref, out_ref, *, cap):
    _, one, two = chosen(routes_ref, share_ref.shape[0], cap)
    share = share_ref[...].astype(F32)
    weights = weights_ref[...].astype(BF16).astype(F32)
    out_ref[0:1, :] = jnp.sum(one * share, axis=0, keepdims=True) / weights[0:1, :]
    out_ref[1:2, :] = jnp.sum(two * share, axis=0, keepdims=True) / weights[1:2, :]


def combine_kernel(pick_ref, back_ref, out_ref):
    out_ref[...] = mm(pick_ref[...], back_ref[...], ROWS).astype(BF16)


def shards(
    tokens,
    cotangent,
    route_weights,
    routes,
    gate_proj,
    up_proj,
    down_proj,
    shared_down,
    shared_hidden,
):
    shape = jax.ShapeDtypeStruct
    rows, feat = tokens.shape
    top = routes.shape[1]
    ep = lax.axis_size("ep")
    tp = lax.axis_size("tp")
    experts = gate_proj.shape[0] * ep
    cap = 2 * rows * top // experts
    slots = experts * cap
    quarter = feat // tp
    block = gate_proj.shape[2]
    hidden = block * tp
    col = lax.axis_index("tp").astype(jnp.int32).reshape(1)
    routes_t = routes.T
    weights_t = route_weights.T

    w_gate = exchange(gate_proj.reshape(tp, quarter, block), "tp")
    w_up = exchange(up_proj.reshape(tp, quarter, block), "tp")
    w_down = exchange(
        down_proj.reshape(block, tp, quarter).transpose(1, 0, 2), "tp"
    )

    x, g, pick = dispatch(col, routes_t, weights_t, tokens, cotangent, slots, cap, quarter)
    x = exchange(x.reshape(ep, -1, quarter), "ep").reshape(slots, quarter)
    g = exchange(g.reshape(ep, -1, quarter), "ep").reshape(slots, quarter)

    part = local(partial_kernel, shape((slots, 3 * hidden), BF16), "partial", x, g, w_gate, w_up, w_down)
    part = exchange(part.reshape(tp, slots // tp, 3 * hidden), "tp")
    grads, hid, share = local(
        middle_kernel,
        (
            shape((tp, slots // tp, 2 * hidden), BF16),
            shape((tp, slots // tp, hidden), BF16),
            shape((slots, rows), BF16),
        ),
        "middle",
        col,
        part,
        smem=1,
    )
    grads = exchange(grads, "tp")
    hid = exchange(hid, "tp")
    share = exchange(share.reshape(ep, -1, rows), "ep").reshape(slots, rows)

    back = local(input_kernel, shape((slots, quarter), BF16), "input", grads, w_gate, w_up)
    back = exchange(back.reshape(ep, -1, quarter), "ep").reshape(slots, quarter)
    tokens_grad = local(combine_kernel, shape((rows, quarter), BF16), "combine", pick, back)

    gate_grad, up_grad = local(
        weight_kernel,
        (shape((tp, quarter, block), BF16), shape((tp, quarter, block), BF16)),
        "weight",
        x,
        grads,
    )
    gate_grad = exchange(gate_grad, "tp").reshape(gate_proj.shape)
    up_grad = exchange(up_grad, "tp").reshape(up_proj.shape)
    down_grad = local(down_kernel, shape((tp, block, quarter), BF16), "down", hid, g)
    down_grad = exchange(down_grad, "tp").transpose(1, 0, 2).reshape(down_proj.shape)

    weights_grad = local(
        functools.partial(share_kernel, cap=cap), shape((top, rows), F32), "share", routes_t, weights_t, share
    )
    weights_grad = lax.psum(weights_grad, "tp").T

    hidden_grad = jnp.dot(cotangent, shared_down, preferred_element_type=F32).astype(BF16)
    shared = lax.dot_general(cotangent, shared_hidden, ROWS, preferred_element_type=F32)
    shared = exchange(shared.astype(BF16).reshape(ep, feat // ep, -1), "ep")
    shared_grad = jnp.sum(shared.astype(F32), axis=0)
    return tokens_grad, weights_grad, gate_grad, up_grad, down_grad, hidden_grad, shared_grad


def solution(mesh):
    return jax.shard_map(
        shards,
        mesh=mesh,
        in_specs=(
            P("ep", None),
            P("ep", None),
            P("ep", None),
            P("ep", None),
            P("ep", None, "tp"),
            P("ep", None, "tp"),
            P("ep", "tp", None),
            P(None, "tp"),
            P("ep", "tp"),
        ),
        out_specs=(
            P("ep", "tp"),
            P("ep", None),
            P("ep", None, "tp"),
            P("ep", None, "tp"),
            P("ep", "tp", None),
            P("ep", "tp"),
            P("ep", "tp"),
        ),
        check_vma=False,
    )
```

time: 245 us -> 281 us (1.15); the launches traced: 244 us -> 276 us
  starting transfers between devices: 29 us -> 68.2 us
  waiting for transfers between devices: 66.5 us -> 99 us
  Pallas kernels: 0 us -> 21.4 us
  local copies, waits for them, and re-layouts: 34.4 us -> 13.7 us
  between operations: 16 us -> 0.75 us
  matrix products: 15.3 us -> 2.03 us
  other arithmetic: 8.14 us -> 0.73 us
  blocking collectives: 74.6 us -> 70.4 us
    all_to_all x3 -> x10, waiting for transfers between devices: 13.2 us -> 99 us  [exchange(): return lax.all_to_all(array, axis, split_axis=0, concat_axis=0, tiled=True)]
    all_gather x1 -> x0, waiting for transfers between devices: 44.1 us -> none  [side_by_side(): out = lax.all_gather(both, axis, axis=dim, tiled=True)]
    all_to_all x3 -> x10, starting transfers between devices: 28.7 us -> 68.2 us  [exchange(): return lax.all_to_all(array, axis, split_axis=0, concat_axis=0, tiled=True)]
    pallas_call x0 -> x8, Pallas kernels: none -> 21.4 us  [the longest x7 18.9 us: local(): pl.pallas_call(kernel, in_specs=[SMEM] * smem + [VMEM] * (len(args) - sme...]
    psum x1, blocking collectives: 24.1 us -> 9.24 us  [shards(): weights_grad = lax.psum(weights_grad, 'tp').T]
    dot_general x10 -> x2, matrix products: 15.3 us -> 2.03 us  [the longest x1 1.12 us: shards(): lax.dot_general(cotangent, shared_hidden, ROWS, preferred_element_type=F32)]
    all_to_all x1 -> x4, blocking collectives: 50.5 us -> 61.2 us  [exchange(): return lax.all_to_all(array, axis, split_axis=0, concat_axis=0, tiled=True)]
    another operation x6 -> x0, local copies, waits for them, and re-layouts: 9.77 us -> none
  transfers between devices with their start and end apart: 7 -> 10, of which waited for: 5 -> 10; matrix products, arithmetic and copies ran while one was open for 17% -> 4% of each run, Pallas kernels for 0% -> 6%
where the time goes in v1:
time: 281 us; the launch traced here: 276 us
  waiting for transfers between devices  99 us (35%)
  blocking collectives  70.4 us (25%)
  starting transfers between devices  68.2 us (24%)
  Pallas kernels  21.4 us (8%)
  local copies, waits for them, and re-layouts  13.7 us (5%)
    all_to_all x10, waiting for transfers between devices, exchange(): return lax.all_to_all(array, axis, split_axis=0, concat_axis=0, tiled=True)  99 us
    all_to_all x10, starting transfers between devices, exchange(): return lax.all_to_all(array, axis, split_axis=0, concat_axis=0, tiled=True)  68.2 us
    all_to_all x4, blocking collectives, exchange(): return lax.all_to_all(array, axis, split_axis=0, concat_axis=0, tiled=True)  61.2 us
    pallas_call x7, Pallas kernels, local(): pl.pallas_call(kernel, in_specs=[SMEM] * smem + [VMEM] * (len(args) - sme...  18.9 us
    psum x1, blocking collectives, shards(): weights_grad = lax.psum(weights_grad, 'tp').T  9.24 us
  transfers between devices with their start and end apart: 10, of which 10 were waited for; matrix products, arithmetic and copies ran while one was open for 4% of the time, Pallas kernels for 6%

profile of v1, /device:TPU:6, one launch (start us, length us, event | category | flops | bytes accessed | tf_op | source)
XLA Modules:
  0.0 276.1 jit_solution(6949792302898682806)
XLA Ops:
  0.6 16.2 %all_to_all.70.gate_ref = bf16[4,512,128]{2,1,0:T(8,128)(2,1)} all-to-all(bf16[4,512,128]{2,1,0:T(8,128)(2,1)} %bitcast.27), channel_id=1, replica_groups=mesh['ep'=128,'tp'=4] {'tp'}, dimensions={0} | all-to-all | bytes 1048576 | tf_op jit(solution)/shard_map/all_to_all | solution.py:19
  16.8 5.5 %all-to-all-start.3 = ((bf16[4,512,128]{2,1,0:T(8,128)(2,1)}), bf16[4,512,128]{2,1,0:T(8,128)(2,1)S(1)}, u32[]{:S(2)}, u32[]{:S(2)}) async-start(bf16[4,512,128]{2,1,0:T(8,128)(2,1)} %bitcast.28), calls=%async_computation.3 | async-start | bytes 1048576 | tf_op jit(solution)/shard_map/all_to_all | solution.py:19
  22.4 2.4 dispatch.1
  24.8 2.0 reshape.66
  28.4 14.6 %all-to-all-start = ((bf16[128,4,512]{2,1,0:T(4,128)(2,1)}), bf16[128,4,512]{2,1,0:T(4,128)(2,1)S(1)}, u32[]{:S(2)}, u32[]{:S(2)}) async-start(bf16[128,4,512]{2,1,0:T(4,128)(2,1)} %reshape.66), calls=%async_computation | async-start | bytes 1048576 | tf_op jit(solution)/shard_map/all_to_all | solution.py:19
  43.9 18.5 %all-to-all-done = bf16[128,4,512]{2,1,0:T(4,128)(2,1)S(1)} async-done(((bf16[128,4,512]{2,1,0:T(4,128)(2,1)}), bf16[128,4,512]{2,1,0:T(4,128)(2,1)S(1)}, u32[]{:S(2)}, u32[]{:S(2)}) %all-to-all-start) | async-done | bytes 524320 | tf_op jit(solution)/shard_map/all_to_all | solution.py:19
  62.4 6.5 %all-to-all-start.1 = ((bf16[128,4,512]{2,1,0:T(4,128)(2,1)}), bf16[128,4,512]{2,1,0:T(4,128)(2,1)S(1)}, u32[]{:S(2)}, u32[]{:S(2)}) async-start(bf16[128,4,512]{2,1,0:T(4,128)(2,1)} %reshape.68), calls=%async_computation.1 | async-start | bytes 1048576 | tf_op jit(solution)/shard_map/all_to_all | solution.py:19
  70.3 18.1 %all-to-all-done.1 = bf16[128,4,512]{2,1,0:T(4,128)(2,1)S(1)} async-done(((bf16[128,4,512]{2,1,0:T(4,128)(2,1)}), bf16[128,4,512]{2,1,0:T(4,128)(2,1)S(1)}, u32[]{:S(2)}, u32[]{:S(2)}) %all-to-all-start.1) | async-done | bytes 524320 | tf_op jit(solution)/shard_map/all_to_all | solution.py:19
  88.4 5.5 %all-to-all-start.4 = ((bf16[4,128,512]{2,1,0:T(8,128)(2,1)}), bf16[4,128,512]{2,1,0:T(8,128)(2,1)S(1)}, u32[]{:S(2)}, u32[]{:S(2)}) async-start(bf16[4,128,512]{2,1,0:T(8,128)(2,1)} %bitcast.6), calls=%async_computation.4 | async-start | bytes 1048576 | tf_op jit(solution)/shard_map/all_to_all | solution.py:19
  95.7 6.8 %all-to-all-done.4.down_ref = bf16[4,128,512]{2,1,0:T(8,128)(2,1)S(1)} async-done(((bf16[4,128,512]{2,1,0:T(8,128)(2,1)}), bf16[4,128,512]{2,1,0:T(8,128)(2,1)S(1)}, u32[]{:S(2)}, u32[]{:S(2)}) %all-to-all-start.4) | async-done | bytes 524320 | tf_op jit(solution)/shard_map/all_to_all | solution.py:19
  103.3 3.8 %partial.1 = bf16[512,1536]{1,0:T(8,128)(2,1)} custom-call(bf16[512,512]{1,0:T(8,128)(2,1)} %reshape.67.x_ref, bf16[512,512]{1,0:T(8,128)(2,1)} %reshape.69.g_ref, bf16[4,512,128]{2,1,0:T(8,128)(2,1)} %all_to_all.70.gate_ref, bf16[4,512,128]{2,1,0:T(8,128)(2,1)} %copy-done.4, bf16[4,128,512]{2,1,0:T(8,128)(2,1)} %copy-done.5), custom_call_target="tpu_custom_call" | custom-call | tf_op jit(solution)/shard_map/partial/pallas_call | solution.py:83
  107.1 5.7 %all-to-all-start.5 = ((bf16[4,128,1536]{2,1,0:T(8,128)(2,1)}), bf16[4,128,1536]{2,1,0:T(8,128)(2,1)S(1)}, u32[]{:S(2)}, u32[]{:S(2)}) async-start(bf16[4,128,1536]{2,1,0:T(8,128)(2,1)} %bitcast.20), calls=%async_computation.5 | async-start | bytes 3145728 | tf_op jit(solution)/shard_map/all_to_all | solution.py:19
  114.0 17.9 %all-to-all-done.5.y_ref = bf16[4,128,1536]{2,1,0:T(8,128)(2,1)S(1)} async-done(((bf16[4,128,1536]{2,1,0:T(8,128)(2,1)}), bf16[4,128,1536]{2,1,0:T(8,128)(2,1)S(1)}, u32[]{:S(2)}, u32[]{:S(2)}) %all-to-all-start.5) | async-done | bytes 1572896 | tf_op jit(solution)/shard_map/all_to_all | solution.py:19
  131.9 6.2 %all-to-all-start.13 = ((bf16[128,16,128]{2,1,0:T(8,128)(2,1)}), bf16[128,16,128]{2,1,0:T(8,128)(2,1)S(1)}, u32[]{:S(2)}, u32[]{:S(2)}) async-start(bf16[128,16,128]{2,1,0:T(8,128)(2,1)} %bitcast.24), calls=%async_computation.13 | async-start | bytes 1048576 | tf_op jit(solution)/shard_map/all_to_all | solution.py:19
  138.0 2.9 %middle.1 = (bf16[4,128,1024]{2,1,0:T(8,128)(2,1)}, bf16[4,128,512]{2,1,0:T(8,128)(2,1)}, bf16[512,128]{1,0:T(8,128)(2,1)}) custom-call(s32[1]{0:T(128)} %bitcast.col, bf16[4,128,1536]{2,1,0:T(8,128)(2,1)} %copy-done.2), custom_call_target="tpu_custom_call" | custom-call | tf_op jit(solution)/shard_map/middle/pallas_call | solution.py:83
  140.9 16.5 %all-to-all-done.13 = bf16[128,16,128]{2,1,0:T(8,128)(2,1)S(1)} async-done(((bf16[128,16,128]{2,1,0:T(8,128)(2,1)}), bf16[128,16,128]{2,1,0:T(8,128)(2,1)S(1)}, u32[]{:S(2)}, u32[]{:S(2)}) %all-to-all-start.13) | async-done | bytes 524320 | tf_op jit(solution)/shard_map/all_to_all | solution.py:19
  157.5 19.3 %all_to_all.71 = bf16[128,4,128]{2,1,0:T(4,128)(2,1)} all-to-all(bf16[128,4,128]{2,1,0:T(4,128)(2,1)} %bitcast.30), channel_id=1, replica_groups=mesh['ep'=128,'tp'=4] {'ep'}, dimensions={0} | all-to-all | bytes 262144 | tf_op jit(solution)/shard_map/all_to_all | solution.py:19
  176.7 14.2 %all_to_all.72.hidden_ref = bf16[4,128,512]{2,1,0:T(8,128)(2,1)} all-to-all(bf16[4,128,512]{2,1,0:T(8,128)(2,1)} %get-tuple-element.22), channel_id=1, replica_groups=mesh['ep'=128,'tp'=4] {'tp'}, dimensions={0} | all-to-all | bytes 1048576 | tf_op jit(solution)/shard_map/all_to_all | solution.py:19
  191.0 5.6 %all-to-all-start.6 = ((bf16[4,128,1024]{2,1,0:T(8,128)(2,1)}), bf16[4,128,1024]{2,1,0:T(8,128)(2,1)S(1)}, u32[]{:S(2)}, u32[]{:S(2)}) async-start(bf16[4,128,1024]{2,1,0:T(8,128)(2,1)} %get-tuple-element.18), calls=%async_computation.6 | async-start | bytes 2097152 | tf_op jit(solution)/shard_map/all_to_all | solution.py:19
  196.5 2.5 down.1
  199.0 10.2 %all-to-all-done.6.grads_ref = bf16[4,128,1024]{2,1,0:T(8,128)(2,1)S(1)} async-done(((bf16[4,128,1024]{2,1,0:T(8,128)(2,1)}), bf16[4,128,1024]{2,1,0:T(8,128)(2,1)S(1)}, u32[]{:S(2)}, u32[]{:S(2)}) %all-to-all-start.6) | async-done | bytes 1048608 | tf_op jit(solution)/shard_map/all_to_all | solution.py:19
  209.3 5.7 %all-to-all-start.12 = ((bf16[4,128,512]{2,1,0:T(8,128)(2,1)}), bf16[4,128,512]{2,1,0:T(8,128)(2,1)S(1)}, u32[]{:S(2)}, u32[]{:S(2)}) async-start(bf16[4,128,512]{2,1,0:T(8,128)(2,1)} %down.1), calls=%async_computation.12 | async-start | bytes 1048576 | tf_op jit(solution)/shard_map/all_to_all | solution.py:19
  215.0 2.9 %weight.1 = (bf16[4,512,128]{2,1,0:T(8,128)(2,1)}, bf16[4,512,128]{2,1,0:T(8,128)(2,1)}) custom-call(bf16[512,512]{1,0:T(8,128)(2,1)} %reshape.67.x_ref, bf16[4,128,1024]{2,1,0:T(8,128)(2,1)} %copy-done.1), custom_call_target="tpu_custom_call" | custom-call | tf_op jit(solution)/shard_map/weight/pallas_call | solution.py:83
  217.9 3.4 %all-to-all-done.12 = bf16[4,128,512]{2,1,0:T(8,128)(2,1)S(1)} async-done(((bf16[4,128,512]{2,1,0:T(8,128)(2,1)}), bf16[4,128,512]{2,1,0:T(8,128)(2,1)S(1)}, u32[]{:S(2)}, u32[]{:S(2)}) %all-to-all-start.12) | async-done | bytes 524320 | tf_op jit(solution)/shard_map/all_to_all | solution.py:19
  221.3 11.5 %all_to_all.73 = bf16[4,512,128]{2,1,0:T(8,128)(2,1)S(1)} all-to-all(bf16[4,512,128]{2,1,0:T(8,128)(2,1)} %get-tuple-element.20), channel_id=1, replica_groups=mesh['ep'=128,'tp'=4] {'tp'}, dimensions={0} | all-to-all | bytes 1048576 | tf_op jit(solution)/shard_map/all_to_all | solution.py:19
  232.7 5.5 %all-to-all-start.10 = ((bf16[4,512,128]{2,1,0:T(8,128)(2,1)}), bf16[4,512,128]{2,1,0:T(8,128)(2,1)S(1)}, u32[]{:S(2)}, u32[]{:S(2)}) async-start(bf16[4,512,128]{2,1,0:T(8,128)(2,1)} %get-tuple-element.21), calls=%async_computation.10 | async-start | bytes 1048576 | tf_op jit(solution)/shard_map/all_to_all | solution.py:19
  238.2 3.0 %input.1 = bf16[512,512]{1,0:T(8,128)(2,1)} custom-call(bf16[4,128,1024]{2,1,0:T(8,128)(2,1)} %copy-done.1, bf16[4,512,128]{2,1,0:T(8,128)(2,1)} %all_to_all.70.gate_ref, bf16[4,512,128]{2,1,0:T(8,128)(2,1)} %copy-done.4), custom_call_target="tpu_custom_call" | custom-call | tf_op jit(solution)/shard_map/input/pallas_call | solution.py:83
  241.3 2.0 reshape.74
  244.3 7.3 %all-to-all-start.7 = ((bf16[128,4,512]{2,1,0:T(4,128)(2,1)}), bf16[128,4,512]{2,1,0:T(4,128)(2,1)}, u32[]{:S(2)}, u32[]{:S(2)}) async-start(bf16[128,4,512]{2,1,0:T(4,128)(2,1)} %reshape.74), calls=%async_computation.7 | async-start | bytes 1048576 | tf_op jit(solution)/shard_map/all_to_all | solution.py:19
  255.0 9.2 %psum.7 = f32[128,2]{0,1:T(2,128)} all-reduce(f32[128,2]{0,1:T(2,128)} %bitcast.31), channel_id=1, replica_groups=mesh['ep'=128,'tp'=4] {'tp'}, use_global_device_ids=true, to_apply=%region_0.0 | all-reduce | flops 256 | bytes 2048 | tf_op jit(solution)/shard_map/psum | solution.py:231
  265.5 5.1 %all-to-all-done.7 = bf16[128,4,512]{2,1,0:T(4,128)(2,1)} async-done(((bf16[128,4,512]{2,1,0:T(4,128)(2,1)}), bf16[128,4,512]{2,1,0:T(4,128)(2,1)}, u32[]{:S(2)}, u32[]{:S(2)}) %all-to-all-start.7) | async-done | bytes 524320 | tf_op jit(solution)/shard_map/all_to_all | solution.py:19
  272.5 2.0 combine.1
  (34 shorter events, 16.8 us)
Async XLA Ops:
  0.6 250.9 %copy-start = (bf16[2048,128]{1,0:T(8,128)(2,1)S(1)}, bf16[2048,128]{1,0:T(8,128)(2,1)}, u32[]{:S(2)}) copy-start(bf16[2048,128]{1,0:T(8,128)(2,1)} %param.16) | copy-start | bytes 1572868
  16.8 11.5 %all-to-all-start.3 = ((bf16[4,512,128]{2,1,0:T(8,128)(2,1)}), bf16[4,512,128]{2,1,0:T(8,128)(2,1)S(1)}, u32[]{:S(2)}, u32[]{:S(2)}) async-start(bf16[4,512,128]{2,1,0:T(8,128)(2,1)} %bitcast.28), calls=%async_computation.3 | async-start | bytes 1048576 | tf_op jit(solution)/shard_map/all_to_all | solution.py:19
  24.8 18.2 %copy-start.7 = (bf16[512,512]{1,0:T(8,128)(2,1)S(1)}, bf16[512,512]{1,0:T(8,128)(2,1)}, u32[]{:S(2)}) copy-start(bf16[512,512]{1,0:T(8,128)(2,1)} %get-tuple-element.17) | copy-start | bytes 1572868
  26.8 42.2 %copy-start.6 = (bf16[1,128,2048]{2,1,0:T(8,128)(2,1)S(1)}, bf16[1,128,2048]{2,1,0:T(8,128)(2,1)}, u32[]{:S(2)}) copy-start(bf16[1,128,2048]{2,1,0:T(8,128)(2,1)} %param.15) | copy-start | bytes 1572868
  28.4 34.0 %copy-start.4 = (bf16[4,512,128]{2,1,0:T(8,128)(2,1)}, bf16[4,512,128]{2,1,0:T(8,128)(2,1)S(1)}, u32[]{:S(2)}) copy-start(bf16[4,512,128]{2,1,0:T(8,128)(2,1)S(1)} %all-to-all-done.3.up_ref) | copy-start | bytes 1572868
  28.4 34.0 %all-to-all-start = ((bf16[128,4,512]{2,1,0:T(4,128)(2,1)}), bf16[128,4,512]{2,1,0:T(4,128)(2,1)S(1)}, u32[]{:S(2)}, u32[]{:S(2)}) async-start(bf16[128,4,512]{2,1,0:T(4,128)(2,1)} %reshape.66), calls=%async_computation | async-start | bytes 1048576 | tf_op jit(solution)/shard_map/all_to_all | solution.py:19
  62.4 26.0 %all-to-all-start.1 = ((bf16[128,4,512]{2,1,0:T(4,128)(2,1)}), bf16[128,4,512]{2,1,0:T(4,128)(2,1)S(1)}, u32[]{:S(2)}, u32[]{:S(2)}) async-start(bf16[128,4,512]{2,1,0:T(4,128)(2,1)} %reshape.68), calls=%async_computation.1 | async-start | bytes 1048576 | tf_op jit(solution)/shard_map/all_to_all | solution.py:19
  88.4 14.1 %all-to-all-start.4 = ((bf16[4,128,512]{2,1,0:T(8,128)(2,1)}), bf16[4,128,512]{2,1,0:T(8,128)(2,1)S(1)}, u32[]{:S(2)}, u32[]{:S(2)}) async-start(bf16[4,128,512]{2,1,0:T(8,128)(2,1)} %bitcast.6), calls=%async_computation.4 | async-start | bytes 1048576 | tf_op jit(solution)/shard_map/all_to_all | solution.py:19
  102.5 0.8 copy-start.5
  107.1 5.7 %copy-start.3 = (bf16[128,2048]{1,0:T(8,128)(2,1)S(1)}, bf16[128,2048]{1,0:T(8,128)(2,1)}, u32[]{:S(2)}) copy-start(bf16[128,2048]{1,0:T(8,128)(2,1)} %cot_ref.1) | copy-start | bytes 1572868
  107.1 5.7 %copy-start.8 = (bf16[128,128]{1,0:T(8,128)(2,1)S(1)}, bf16[128,128]{1,0:T(8,128)(2,1)}, u32[]{:S(2)}) copy-start(bf16[128,128]{1,0:T(8,128)(2,1)} %param.17) | copy-start | bytes 98308
  107.1 24.7 %all-to-all-start.5 = ((bf16[4,128,1536]{2,1,0:T(8,128)(2,1)}), bf16[4,128,1536]{2,1,0:T(8,128)(2,1)S(1)}, u32[]{:S(2)}, u32[]{:S(2)}) async-start(bf16[4,128,1536]{2,1,0:T(8,128)(2,1)} %bitcast.20), calls=%async_computation.5 | async-start | bytes 3145728 | tf_op jit(solution)/shard_map/all_to_all | solution.py:19
  131.9 6.2 %copy-start.2 = (bf16[4,128,1536]{2,1,0:T(8,128)(2,1)}, bf16[4,128,1536]{2,1,0:T(8,128)(2,1)S(1)}, u32[]{:S(2)}) copy-start(bf16[4,128,1536]{2,1,0:T(8,128)(2,1)S(1)} %all-to-all-done.5.y_ref) | copy-start | bytes 4718596
  131.9 25.6 %all-to-all-start.13 = ((bf16[128,16,128]{2,1,0:T(8,128)(2,1)}), bf16[128,16,128]{2,1,0:T(8,128)(2,1)S(1)}, u32[]{:S(2)}, u32[]{:S(2)}) async-start(bf16[128,16,128]{2,1,0:T(8,128)(2,1)} %bitcast.24), calls=%async_computation.13 | async-start | bytes 1048576 | tf_op jit(solution)/shard_map/all_to_all | solution.py:19
  191.0 18.3 %all-to-all-start.6 = ((bf16[4,128,1024]{2,1,0:T(8,128)(2,1)}), bf16[4,128,1024]{2,1,0:T(8,128)(2,1)S(1)}, u32[]{:S(2)}, u32[]{:S(2)}) async-start(bf16[4,128,1024]{2,1,0:T(8,128)(2,1)} %get-tuple-element.18), calls=%async_computation.6 | async-start | bytes 2097152 | tf_op jit(solution)/shard_map/all_to_all | solution.py:19
  209.3 5.7 %copy-start.1 = (bf16[4,128,1024]{2,1,0:T(8,128)(2,1)}, bf16[4,128,1024]{2,1,0:T(8,128)(2,1)S(1)}, u32[]{:S(2)}) copy-start(bf16[4,128,1024]{2,1,0:T(8,128)(2,1)S(1)} %all-to-all-done.6.grads_ref) | copy-start | bytes 3145732
  209.3 12.0 %all-to-all-start.12 = ((bf16[4,128,512]{2,1,0:T(8,128)(2,1)}), bf16[4,128,512]{2,1,0:T(8,128)(2,1)S(1)}, u32[]{:S(2)}, u32[]{:S(2)}) async-start(bf16[4,128,512]{2,1,0:T(8,128)(2,1)} %down.1), calls=%async_computation.12 | async-start | bytes 1048576 | tf_op jit(solution)/shard_map/all_to_all | solution.py:19
  232.7 11.5 %all-to-all-start.10 = ((bf16[4,512,128]{2,1,0:T(8,128)(2,1)}), bf16[4,512,128]{2,1,0:T(8,128)(2,1)S(1)}, u32[]{:S(2)}, u32[]{:S(2)}) async-start(bf16[4,512,128]{2,1,0:T(8,128)(2,1)} %get-tuple-element.21), calls=%async_computation.10 | async-start | bytes 1048576 | tf_op jit(solution)/shard_map/all_to_all | solution.py:19
  244.3 26.3 %all-to-all-start.7 = ((bf16[128,4,512]{2,1,0:T(4,128)(2,1)}), bf16[128,4,512]{2,1,0:T(4,128)(2,1)}, u32[]{:S(2)}, u32[]{:S(2)}) async-start(bf16[128,4,512]{2,1,0:T(4,128)(2,1)} %reshape.74), calls=%async_computation.7 | async-start | bytes 1048576 | tf_op jit(solution)/shard_map/all_to_all | solution.py:19

commit v2 on v1

v2 whole, which is shorter than its diff:
```python
import jax
import jax.numpy as jnp
from jax import lax
from jax.experimental import pallas as pl
from jax.experimental.pallas import tpu as pltpu
from jax.sharding import PartitionSpec as P

F32 = jnp.float32
BF16 = jnp.bfloat16
COLS = (((1,), (0,)), ((), ()))
ROWS = (((0,), (0,)), ((), ()))
LAST = (((1,), (1,)), ((), ()))
VMEM = pl.BlockSpec(memory_space=pltpu.VMEM)
SMEM = pl.BlockSpec(memory_space=pltpu.SMEM)
LIMIT = pltpu.CompilerParams(vmem_limit_bytes=20 * 2**20)
CAP = 4
PAD = 16


def mm(a, b, dims=COLS):
    return lax.dot_general(a, b, dims, preferred_element_type=F32)


def around(array, axis):
    size = lax.axis_size(axis)
    arrays = array if isinstance(array, (list, tuple)) else [array] * (size - 1)
    return [
        lax.ppermute(part, axis, [(i, (i + k + 1) % size) for i in range(size)])
        for k, part in enumerate(arrays)
    ]


def at(col, step, parts):
    return lax.rem(col[0] + (step + parts), parts)


def span(index, width):
    return pl.ds(pl.multiple_of(index * width, width), width)


def local(kernel, out, *args, smem=0, scratch=()):
    return pl.pallas_call(
        kernel,
        in_specs=[SMEM] * smem + [VMEM] * (len(args) - smem),
        out_specs=jax.tree.map(lambda _: VMEM, out),
        out_shape=out,
        scratch_shapes=scratch,
        compiler_params=LIMIT,
    )(*args)


def weave():
    rows = 64 * CAP
    row = lax.broadcasted_iota(jnp.int32, (rows, rows), 0)
    col = lax.broadcasted_iota(jnp.int32, (rows, rows), 1)
    s, rest = row // (2 * CAP), row % (2 * CAP)
    h, r = rest // CAP, rest % CAP
    return jnp.where(col == h * (rows // 2) + s * CAP + r, 1.0, 0.0).astype(BF16)


def chosen(routes_ref, slots):
    count = routes_ref.shape[1]
    row = lax.broadcasted_iota(jnp.int32, (slots, count), 0)
    expert = row // CAP
    first = expert == routes_ref[0:1, :]
    second = expert == routes_ref[1:2, :]
    named = jnp.where(first | second, 1.0, 0.0)
    earlier = lax.broadcasted_iota(jnp.int32, (count, count), 0)
    later = lax.broadcasted_iota(jnp.int32, (count, count), 1)
    before = jnp.where(earlier < later, 1.0, 0.0).astype(BF16)
    rank = mm(named.astype(BF16), before)
    place = (row - expert * CAP).astype(F32)
    hit = jnp.where(rank == place, named, 0.0)
    return hit, jnp.where(first, hit, 0.0), jnp.where(second, hit, 0.0)


def dispatch_kernel(col, routes_ref, weights_ref, tok_ref, cot_ref, sent_ref, pick_ref):
    slots = pick_ref.shape[0]
    hit, one, two = chosen(routes_ref, slots)
    weights = weights_ref[...].astype(BF16).astype(F32)
    weight = jnp.sum(one * weights[0:1, :] + two * weights[1:2, :], axis=1, keepdims=True)
    pick = hit.astype(BF16)
    pick_ref[...] = pick
    x = mm(pick, tok_ref[...]).astype(BF16)
    g = (weight * mm(pick, cot_ref[...])).astype(BF16)
    order = weave()
    half = order.shape[0] // 2
    for b in range(slots // half):
        both = jnp.concatenate([x[b * half : (b + 1) * half], g[b * half : (b + 1) * half]], axis=0)
        sent_ref[2 * b * half : 2 * (b + 1) * half, :] = mm(order, both).astype(BF16)


def dispatch(col, routes, weights, tokens, cotangent, slots, quarter):
    rows = tokens.shape[0]
    whole = lambda *shape: pl.BlockSpec(shape, lambda i, col: (0,) * len(shape))
    part = pl.BlockSpec((rows, quarter), lambda i, col: (0, col[0]))
    return pl.pallas_call(
        dispatch_kernel,
        grid_spec=pltpu.PrefetchScalarGridSpec(
            num_scalar_prefetch=1,
            grid=(1,),
            in_specs=[whole(*routes.shape), whole(*weights.shape), part, part],
            out_specs=[whole(2 * slots, quarter), whole(slots, rows)],
        ),
        out_shape=[
            jax.ShapeDtypeStruct((2 * slots, quarter), BF16),
            jax.ShapeDtypeStruct((slots, rows), BF16),
        ],
        compiler_params=LIMIT,
        name="dispatch",
    )(col, routes, weights, tokens, cotangent)


def pack_kernel(col, gate_ref, up_ref, down_ref, *outs):
    parts = len(outs)
    quarter = gate_ref.shape[0] // parts
    block = gate_ref.shape[1]
    for k, out in enumerate(outs):
        to = at(col, k, parts)
        out[:quarter, :] = gate_ref[span(to, quarter), :]
        out[quarter : 2 * quarter, :] = up_ref[span(to, quarter), :]
        down = down_ref[:, span(to, quarter)]
        for c in range(quarter // block):
            row = 2 * quarter + c * block
            out[row : row + block, :] = down[:, c * block : (c + 1) * block]


def collect_kernel(col, *refs):
    *packed, both_ref, down_ref = refs
    parts = len(packed)
    quarter, width = both_ref.shape
    hidden = width // 2
    block = hidden // parts
    for k, ref in enumerate(packed):
        place = span(at(col, -k, parts), block)
        both_ref[:, place] = ref[:quarter, :]
        both_ref[:, span(at(col, -k, parts) + parts, block)] = ref[quarter : 2 * quarter, :]
        for c in range(quarter // block):
            row = 2 * quarter + c * block
            down_ref[place, c * block : (c + 1) * block] = ref[row : row + block, :]


def partial_kernel(col, got_ref, both_ref, down_ref, x_ref, g_ref, *refs):
    *outs, y_ref = refs
    parts = len(outs)
    width = both_ref.shape[1]
    order = weave()
    half = order.shape[0] // 2
    for b in range(got_ref.shape[0] // (2 * half)):
        split = mm(order, got_ref[2 * b * half : 2 * (b + 1) * half, :], ROWS).astype(BF16)
        x_ref[b * half : (b + 1) * half, :] = split[:half]
        g_ref[b * half : (b + 1) * half, :] = split[half:]
    y_ref[:, :width] = mm(x_ref[...], both_ref[...]).astype(BF16)
    y_ref[:, width:] = mm(g_ref[...], down_ref[...], LAST).astype(BF16)
    for k, out in enumerate(outs):
        out[...] = y_ref[span(at(col, k, parts), out.shape[0]), :]


def middle_kernel(col, *refs):
    *parts, grads_ref, share_ref = refs
    rows, width = grads_ref.shape
    hidden = width // 3
    total = parts[0][...].astype(F32)
    for ref in parts[1:]:
        total = total + ref[...].astype(F32)
    gate = total[:, :hidden]
    upper = total[:, hidden : 2 * hidden]
    backed = total[:, 2 * hidden :]
    sigma = jax.nn.sigmoid(gate)
    active = gate * sigma
    hid = (active * upper).astype(BF16)
    grads_ref[:, :hidden] = (backed * upper * sigma * (1.0 + gate * (1.0 - sigma))).astype(BF16)
    grads_ref[:, hidden : 2 * hidden] = (backed * active).astype(BF16)
    grads_ref[:, 2 * hidden :] = hid
    share = jnp.sum(hid.astype(F32) * backed, axis=1, keepdims=True)
    share = jnp.broadcast_to(share, (rows, share_ref.shape[1]))
    for k in range(len(parts)):
        share_ref[k * rows : (k + 1) * rows, :] = jnp.where(col[0] == k, share, 0.0).astype(BF16)


def input_kernel(col, *refs):
    *grads, both_ref, out_ref = refs
    parts = len(grads)
    rows = grads[0].shape[0]
    width = both_ref.shape[1]
    whole = jnp.concatenate([ref[:, :width] for ref in grads], axis=0)
    out = mm(whole, both_ref[...], LAST).astype(BF16)
    order = weave()
    half = out.shape[1] // 2
    for k in range(parts):
        own = out[k * rows : (k + 1) * rows]
        both = jnp.concatenate([own[:, :half], own[:, half:]], axis=0)
        out_ref[span(at(col, -k, parts), 2 * rows), :] = mm(order, both).astype(BF16)


def weight_kernel(col, x_ref, g_ref, routes_ref, weights_ref, share_ref, *refs):
    refs, all_ref, down_ref = refs[:-2], refs[-2], refs[-1]
    parts = len(refs) // 2
    grads, outs = refs[:parts], refs[parts:]
    rows = grads[0].shape[0]
    quarter, width = all_ref.shape
    block = outs[0].shape[1]
    order = [span(at(col, -k, parts), rows) for k in range(parts)]
    x = jnp.concatenate([x_ref[place, :] for place in order], axis=0)
    g = jnp.concatenate([g_ref[place, :] for place in order], axis=0)
    whole = jnp.concatenate([ref[...] for ref in grads], axis=0)
    all_ref[...] = mm(x, whole[:, :width], ROWS).astype(BF16)
    down_ref[...] = mm(whole[:, width:], g, ROWS).astype(BF16)
    _, one, two = chosen(routes_ref, share_ref.shape[0])
    share = share_ref[...].astype(F32)
    weights = weights_ref[...].astype(BF16).astype(F32)
    one = jnp.sum(one * share, axis=0, keepdims=True) / weights[0:1, :]
    two = jnp.sum(two * share, axis=0, keepdims=True) / weights[1:2, :]
    row = lax.broadcasted_iota(jnp.int32, (PAD, block), 0)
    share = jnp.where(row == 0, one, jnp.where(row == 1, two, 0.0)).astype(BF16)
    for k, out in enumerate(outs):
        to = at(col, k, parts)
        out[:quarter, :] = all_ref[:, span(to, block)]
        out[quarter : 2 * quarter, :] = all_ref[:, span(to + parts, block)]
        for c in range(quarter // block):
            row = 2 * quarter + c * block
            out[row : row + block, :] = down_ref[span(to, block), c * block : (c + 1) * block]
        out[3 * quarter :, :] = share


def finish_kernel(col, *refs):
    *got, gate_ref, up_ref, down_ref, share_ref = refs
    parts = len(got)
    block = gate_ref.shape[1]
    quarter = gate_ref.shape[0] // parts
    share = jnp.zeros(share_ref.shape, F32)
    for k, ref in enumerate(got):
        place = span(at(col, -k, parts), quarter)
        gate_ref[place, :] = ref[:quarter, :]
        up_ref[place, :] = ref[quarter : 2 * quarter, :]
        pieces = [ref[row : row + block, :] for row in range(2 * quarter, 3 * quarter, block)]
        down_ref[:, place] = jnp.concatenate(pieces, axis=1)
        share = share + ref[3 * quarter :, :].astype(F32)[: share.shape[0]]
    share_ref[...] = share


def combine_kernel(pick_ref, back_ref, out_ref):
    slots = pick_ref.shape[0]
    order = weave()
    half = order.shape[0] // 2
    left, right = [], []
    for b in range(slots // half):
        own = mm(order, back_ref[2 * b * half : 2 * (b + 1) * half, :], ROWS).astype(BF16)
        left.append(own[:half])
        right.append(own[half:])
    width = back_ref.shape[1]
    pick = pick_ref[...]
    out_ref[:, :width] = mm(pick, jnp.concatenate(left, axis=0), ROWS).astype(BF16)
    out_ref[:, width:] = mm(pick, jnp.concatenate(right, axis=0), ROWS).astype(BF16)


def experts(
    tokens,
    cotangent,
    route_weights,
    routes,
    gate_proj,
    up_proj,
    down_proj,
    shared_down,
    shared_hidden,
):
    rows, feat = tokens.shape
    top = routes.shape[1]
    ep = lax.axis_size("ep")
    tp = lax.axis_size("tp")
    slots = ep * CAP
    quarter = feat // tp
    block = gate_proj.shape[2]
    hidden = block * tp
    some = slots // tp
    half = lambda *shape: jax.ShapeDtypeStruct(shape, BF16)
    over_ep = lambda a: lax.all_to_all(
        a.reshape(ep, -1, a.shape[-1]), "ep", split_axis=0, concat_axis=0, tiled=True
    ).reshape(a.shape)
    col = lax.axis_index("tp").astype(jnp.int32).reshape(1)
    routes_t = routes.T
    weights_t = route_weights.T

    sent, pick = dispatch(col, routes_t, weights_t, tokens, cotangent, slots, quarter)
    got = over_ep(sent)

    packed = local(
        pack_kernel,
        [half(3 * quarter, block)] * tp,
        col,
        gate_proj.reshape(feat, block),
        up_proj.reshape(feat, block),
        down_proj.reshape(block, feat),
        smem=1,
    )
    packed = [packed[0], *around(packed[1:], "tp")]
    both, down = local(
        collect_kernel, [half(quarter, 2 * hidden), half(hidden, quarter)], col, *packed, smem=1
    )

    x, g, *part = local(
        partial_kernel,
        [half(slots, quarter)] * 2 + [half(some, 3 * hidden)] * tp,
        col,
        got,
        both,
        down,
        smem=1,
        scratch=[pltpu.VMEM((slots, 3 * hidden), BF16)],
    )
    part = [part[0], *around(part[1:], "tp")]
    grads, share = local(
        middle_kernel, [half(some, 3 * hidden), half(slots, rows)], col, *part, smem=1
    )
    grads = [grads, *around(grads, "tp")]
    share = over_ep(share)

    back = local(input_kernel, half(2 * slots, quarter // 2), col, *grads, both, smem=1)
    back = over_ep(back)
    tokens_grad = local(combine_kernel, half(rows, quarter), pick, back)

    outer = local(
        weight_kernel,
        [half(3 * quarter + PAD, block)] * tp,
        col,
        x,
        g,
        routes_t,
        weights_t,
        share,
        *grads,
        smem=1,
        scratch=[pltpu.VMEM((quarter, 2 * hidden), BF16), pltpu.VMEM((hidden, quarter), BF16)],
    )
    outer = [outer[0], *around(outer[1:], "tp")]
    gate_grad, up_grad, down_grad, weights_grad = local(
        finish_kernel,
        [half(feat, block)] * 2 + [half(block, feat), jax.ShapeDtypeStruct((top, rows), F32)],
        col,
        *outer,
        smem=1,
    )
    weights_grad = weights_grad.T

    hidden_grad = jnp.dot(cotangent, shared_down, preferred_element_type=F32).astype(BF16)
    shared = lax.dot_general(cotangent, shared_hidden, ROWS, preferred_element_type=F32)
    shared = shared.astype(BF16)
    shared = over_ep(shared)
    shared_grad = jnp.sum(shared.reshape(ep, feat // ep, -1).astype(F32), axis=0)
    return (
        tokens_grad,
        weights_grad,
        gate_grad.reshape(gate_proj.shape),
        up_grad.reshape(up_proj.shape),
        down_grad.reshape(down_proj.shape),
        hidden_grad,
        shared_grad,
    )


def solution(mesh):
    return jax.shard_map(
        experts,
        mesh=mesh,
        in_specs=(
            P("ep", None),
            P("ep", None),
            P("ep", None),
            P("ep", None),
            P("ep", None, "tp"),
            P("ep", None, "tp"),
            P("ep", "tp", None),
            P(None, "tp"),
            P("ep", "tp"),
        ),
        out_specs=(
            P("ep", "tp"),
            P("ep", None),
            P("ep", None, "tp"),
            P("ep", None, "tp"),
            P("ep", "tp", None),
            P("ep", "tp"),
            P("ep", "tp"),
        ),
        check_vma=False,
    )
```

time: 281 us -> 193 us (0.69); the launches traced: 276 us -> 191 us
  blocking collectives: 70.4 us -> 0 us
  starting transfers between devices: 68.2 us -> 83.7 us
  waiting for transfers between devices: 99 us -> 83.9 us
  Pallas kernels: 21.4 us -> 12.6 us
  local copies, waits for them, and re-layouts: 13.7 us -> 6.5 us
    all_to_all x10 -> x4, waiting for transfers between devices: 99 us -> 37.5 us  [experts(): lax.all_to_all(a.reshape(ep, -1, a.shape[-1]), 'ep', split_axis=0, concat...]
    all_to_all x4 -> x0, blocking collectives: 61.2 us -> none  [exchange(): return lax.all_to_all(array, axis, split_axis=0, concat_axis=0, tiled=True)]
    ppermute x0 -> x12, waiting for transfers between devices: none -> 46.5 us  [around(): lax.ppermute(part, axis, [(i, (i + k + 1) % size) for i in range(size)])]
    ppermute x0 -> x12, starting transfers between devices: none -> 37.2 us  [around(): lax.ppermute(part, axis, [(i, (i + k + 1) % size) for i in range(size)])]
    all_to_all x10 -> x4, starting transfers between devices: 68.2 us -> 46.5 us  [experts(): lax.all_to_all(a.reshape(ep, -1, a.shape[-1]), 'ep', split_axis=0, concat...]
    reshape x7 -> x0, local copies, waits for them, and re-layouts: 9.7 us -> none  [the longest x2 3.92 us: shards(): back = exchange(back.reshape(ep, -1, quarter), 'ep').reshape(slots, quarter)]
    psum x1 -> x0, blocking collectives: 9.24 us -> none  [shards(): weights_grad = lax.psum(weights_grad, 'tp').T]
    pallas_call x7 -> x8, Pallas kernels: 18.9 us -> 10.7 us  [local(): pl.pallas_call(kernel, in_specs=[SMEM] * smem + [VMEM] * (len(args) - sme...]
  transfers between devices with their start and end apart: 10 -> 16, of which waited for: 10 -> 11; matrix products, arithmetic and copies ran while one was open for 4% -> 2% of each run, Pallas kernels for 6% -> 5%
where the time goes in v2:
time: 193 us; the launch traced here: 191 us
  waiting for transfers between devices  83.9 us (43%)
  starting transfers between devices  83.7 us (43%)
  Pallas kernels  12.6 us (7%)
  local copies, waits for them, and re-layouts  6.5 us (3%)
  matrix products  2.04 us (1%)
    all_to_all x4, starting transfers between devices, experts(): lax.all_to_all(a.reshape(ep, -1, a.shape[-1]), 'ep', split_axis=0, concat...  46.5 us
    ppermute x12, waiting for transfers between devices, around(): lax.ppermute(part, axis, [(i, (i + k + 1) % size) for i in range(size)])  46.5 us
    all_to_all x4, waiting for transfers between devices, experts(): lax.all_to_all(a.reshape(ep, -1, a.shape[-1]), 'ep', split_axis=0, concat...  37.5 us
    ppermute x12, starting transfers between devices, around(): lax.ppermute(part, axis, [(i, (i + k + 1) % size) for i in range(size)])  37.2 us
    pallas_call x8, Pallas kernels, local(): pl.pallas_call(kernel, in_specs=[SMEM] * smem + [VMEM] * (len(args) - sme...  10.7 us
    unnamed x28, local copies, waits for them, and re-layouts  6.5 us
  transfers between devices with their start and end apart: 16, of which 11 were waited for; matrix products, arithmetic and copies ran while one was open for 2% of the time, Pallas kernels for 5%

profile of v2, /device:TPU:6, one launch (start us, length us, event | category | flops | bytes accessed | tf_op | source)
XLA Modules:
  0.0 191.5 jit_solution(10439465873099160852)
XLA Ops:
  3.5 1.9 dispatch.1
  5.4 17.9 %all-to-all-start = ((bf16[128,8,512]{2,1,0:T(8,128)(2,1)}), bf16[128,8,512]{2,1,0:T(8,128)(2,1)S(1)}, u32[]{:S(2)}, u32[]{:S(2)}) async-start(bf16[128,8,512]{2,1,0:T(8,128)(2,1)} %bitcast.3), calls=%async_computation | async-start | bytes 2097152 | tf_op jit(solution)/shard_map/all_to_all | solution.py:278
  24.5 29.1 %all-to-all-done = bf16[128,8,512]{2,1,0:T(8,128)(2,1)S(1)} async-done(((bf16[128,8,512]{2,1,0:T(8,128)(2,1)}), bf16[128,8,512]{2,1,0:T(8,128)(2,1)S(1)}, u32[]{:S(2)}, u32[]{:S(2)}) %all-to-all-start) | async-done | bytes 1048608 | tf_op jit(solution)/shard_map/all_to_all | solution.py:278
  53.5 7.8 %all-to-all-start.3 = ((bf16[128,16,128]{2,1,0:T(8,128)(2,1)}), bf16[128,16,128]{2,1,0:T(8,128)(2,1)}, u32[]{:S(2)}, u32[]{:S(2)}) async-start(bf16[128,16,128]{2,1,0:T(8,128)(2,1)} %bitcast.31), calls=%async_computation.3 | async-start | bytes 1048576 | tf_op jit(solution)/shard_map/all_to_all | solution.py:278
  62.6 2.4 %collective-permute-start = (bf16[1536,128]{1,0:T(8,128)(2,1)S(1)}, bf16[1536,128]{1,0:T(8,128)(2,1)S(1)}, u32[]{:S(2)}, u32[]{:S(2)}) collective-permute-start(bf16[1536,128]{1,0:T(8,128)(2,1)S(1)} %get-tuple-element.34), channel_id=1, source_target_pairs={{0,1},{1,2},{2,3},{3,0},{4,5},{5,6},{6,7},{7,4},{8,9},{9,10},{10,1... | collective-permute-start | bytes 1179656 | tf_op jit(solution)/shard_map/ppermute | solution.py:28
  65.0 4.3 %collective-permute-start.1 = (bf16[1536,128]{1,0:T(8,128)(2,1)S(1)}, bf16[1536,128]{1,0:T(8,128)(2,1)S(1)}, u32[]{:S(2)}, u32[]{:S(2)}) collective-permute-start(bf16[1536,128]{1,0:T(8,128)(2,1)S(1)} %get-tuple-element.35), channel_id=1, source_target_pairs={{0,2},{1,3},{2,0},{3,1},{4,6},{5,7},{6,4},{7,5},{8,10},{9,11},{10,... | collective-permute-start | bytes 1179656 | tf_op jit(solution)/shard_map/ppermute | solution.py:28
  69.3 1.9 %collective-permute-start.2 = (bf16[1536,128]{1,0:T(8,128)(2,1)S(1)}, bf16[1536,128]{1,0:T(8,128)(2,1)S(1)}, u32[]{:S(2)}, u32[]{:S(2)}) collective-permute-start(bf16[1536,128]{1,0:T(8,128)(2,1)S(1)} %get-tuple-element.36), channel_id=1, source_target_pairs={{0,3},{1,0},{2,1},{3,2},{4,7},{5,4},{6,5},{7,6},{8,11},{9,8},{10,9... | collective-permute-start | bytes 1179656 | tf_op jit(solution)/shard_map/ppermute | solution.py:28
  71.2 5.2 %collective-permute-done.refs_1_ = bf16[1536,128]{1,0:T(8,128)(2,1)S(1)} collective-permute-done((bf16[1536,128]{1,0:T(8,128)(2,1)S(1)}, bf16[1536,128]{1,0:T(8,128)(2,1)S(1)}, u32[]{:S(2)}, u32[]{:S(2)}) %collective-permute-start) | collective-permute-done | bytes 393248 | tf_op jit(solution)/shard_map/ppermute | solution.py:28
  76.5 3.9 %collective-permute-done.1.refs_2_ = bf16[1536,128]{1,0:T(8,128)(2,1)S(1)} collective-permute-done((bf16[1536,128]{1,0:T(8,128)(2,1)S(1)}, bf16[1536,128]{1,0:T(8,128)(2,1)S(1)}, u32[]{:S(2)}, u32[]{:S(2)}) %collective-permute-start.1) | collective-permute-done | bytes 393248 | tf_op jit(solution)/shard_map/ppermute | solution.py:28
  80.4 6.7 %collective-permute-done.2.refs_3_ = bf16[1536,128]{1,0:T(8,128)(2,1)S(1)} collective-permute-done((bf16[1536,128]{1,0:T(8,128)(2,1)S(1)}, bf16[1536,128]{1,0:T(8,128)(2,1)S(1)}, u32[]{:S(2)}, u32[]{:S(2)}) %collective-permute-start.2) | collective-permute-done | bytes 393248 | tf_op jit(solution)/shard_map/ppermute | solution.py:28
  87.5 1.4 shard_map.146
  90.5 2.5 %collective-permute-start.3 = (bf16[128,1536]{1,0:T(8,128)(2,1)S(1)}, bf16[128,1536]{1,0:T(8,128)(2,1)S(1)}, u32[]{:S(2)}, u32[]{:S(2)}) collective-permute-start(bf16[128,1536]{1,0:T(8,128)(2,1)S(1)} %get-tuple-element.40), channel_id=1, source_target_pairs={{0,1},{1,2},{2,3},{3,0},{4,5},{5,6},{6,7},{7,4},{8,9},{9,10},{10,1... | collective-permute-start | bytes 1179656 | tf_op jit(solution)/shard_map/ppermute | solution.py:28
  93.0 4.3 %collective-permute-start.4 = (bf16[128,1536]{1,0:T(8,128)(2,1)S(1)}, bf16[128,1536]{1,0:T(8,128)(2,1)S(1)}, u32[]{:S(2)}, u32[]{:S(2)}) collective-permute-start(bf16[128,1536]{1,0:T(8,128)(2,1)S(1)} %get-tuple-element.41), channel_id=1, source_target_pairs={{0,2},{1,3},{2,0},{3,1},{4,6},{5,7},{6,4},{7,5},{8,10},{9,11},{10,... | collective-permute-start | bytes 1179656 | tf_op jit(solution)/shard_map/ppermute | solution.py:28
  97.4 2.7 %collective-permute-start.5 = (bf16[128,1536]{1,0:T(8,128)(2,1)S(1)}, bf16[128,1536]{1,0:T(8,128)(2,1)S(1)}, u32[]{:S(2)}, u32[]{:S(2)}) collective-permute-start(bf16[128,1536]{1,0:T(8,128)(2,1)S(1)} %get-tuple-element.42), channel_id=1, source_target_pairs={{0,3},{1,0},{2,1},{3,2},{4,7},{5,4},{6,5},{7,6},{8,11},{9,8},{10,9... | collective-permute-start | bytes 1179656 | tf_op jit(solution)/shard_map/ppermute | solution.py:28
  100.1 4.3 %collective-permute-done.3.refs_1_ = bf16[128,1536]{1,0:T(8,128)(2,1)S(1)} collective-permute-done((bf16[128,1536]{1,0:T(8,128)(2,1)S(1)}, bf16[128,1536]{1,0:T(8,128)(2,1)S(1)}, u32[]{:S(2)}, u32[]{:S(2)}) %collective-permute-start.3) | collective-permute-done | bytes 393248 | tf_op jit(solution)/shard_map/ppermute | solution.py:28
  104.4 4.1 %collective-permute-done.4.refs_2_ = bf16[128,1536]{1,0:T(8,128)(2,1)S(1)} collective-permute-done((bf16[128,1536]{1,0:T(8,128)(2,1)S(1)}, bf16[128,1536]{1,0:T(8,128)(2,1)S(1)}, u32[]{:S(2)}, u32[]{:S(2)}) %collective-permute-start.4) | collective-permute-done | bytes 393248 | tf_op jit(solution)/shard_map/ppermute | solution.py:28
  108.4 6.8 %collective-permute-done.5.refs_3_ = bf16[128,1536]{1,0:T(8,128)(2,1)S(1)} collective-permute-done((bf16[128,1536]{1,0:T(8,128)(2,1)S(1)}, bf16[128,1536]{1,0:T(8,128)(2,1)S(1)}, u32[]{:S(2)}, u32[]{:S(2)}) %collective-permute-start.5) | collective-permute-done | bytes 393248 | tf_op jit(solution)/shard_map/ppermute | solution.py:28
  116.4 2.5 %collective-permute-start.6 = (bf16[128,1536]{1,0:T(8,128)(2,1)S(1)}, bf16[128,1536]{1,0:T(8,128)(2,1)S(1)}, u32[]{:S(2)}, u32[]{:S(2)}) collective-permute-start(bf16[128,1536]{1,0:T(8,128)(2,1)S(1)} %get-tuple-element.43.refs_0_), channel_id=1, source_target_pairs={{0,1},{1,2},{2,3},{3,0},{4,5},{5,6},{6,7},{7,4},{8,9},{9,10},{10,1... | collective-permute-start | bytes 1179656 | tf_op jit(solution)/shard_map/ppermute | solution.py:28
  118.9 4.3 %collective-permute-start.7 = (bf16[128,1536]{1,0:T(8,128)(2,1)S(1)}, bf16[128,1536]{1,0:T(8,128)(2,1)S(1)}, u32[]{:S(2)}, u32[]{:S(2)}) collective-permute-start(bf16[128,1536]{1,0:T(8,128)(2,1)S(1)} %get-tuple-element.43.refs_0_), channel_id=1, source_target_pairs={{0,2},{1,3},{2,0},{3,1},{4,6},{5,7},{6,4},{7,5},{8,10},{9,11},{10,... | collective-permute-start | bytes 1179656 | tf_op jit(solution)/shard_map/ppermute | solution.py:28
  123.2 2.7 %collective-permute-start.8 = (bf16[128,1536]{1,0:T(8,128)(2,1)S(1)}, bf16[128,1536]{1,0:T(8,128)(2,1)}, u32[]{:S(2)}, u32[]{:S(2)}) collective-permute-start(bf16[128,1536]{1,0:T(8,128)(2,1)S(1)} %get-tuple-element.43.refs_0_), channel_id=1, source_target_pairs={{0,3},{1,0},{2,1},{3,2},{4,7},{5,4},{6,5},{7,6},{8,11},{9,8},{10,9... | collective-permute-start | bytes 1179656 | tf_op jit(solution)/shard_map/ppermute | solution.py:28
  125.9 14.2 %all-to-all-start.2 = ((bf16[128,4,128]{2,1,0:T(4,128)(2,1)}), bf16[128,4,128]{2,1,0:T(4,128)(2,1)S(1)}, u32[]{:S(2)}, u32[]{:S(2)}) async-start(bf16[128,4,128]{2,1,0:T(4,128)(2,1)} %bitcast.10), calls=%async_computation.2 | async-start | bytes 262144 | tf_op jit(solution)/shard_map/all_to_all | solution.py:278
  141.2 2.8 %shard_map.148 = bf16[1024,256]{1,0:T(8,128)(2,1)} custom-call(s32[1]{0:T(128)} %bitcast.col, bf16[128,1536]{1,0:T(8,128)(2,1)S(1)} %get-tuple-element.43.refs_0_, bf16[128,1536]{1,0:T(8,128)(2,1)S(1)} %collective-permute-done.6.refs_1_, bf16[128,1536]{1,0:T(8,128)(2,1)S(1)} %collective-permute-done.7.refs_2_, ...), custom_call_target="tpu_custom_call" | custom-call | tf_op jit(solution)/shard_map/pallas_call | solution.py:42
  144.0 8.4 %all-to-all-done.2 = bf16[128,4,128]{2,1,0:T(4,128)(2,1)S(1)} async-done(((bf16[128,4,128]{2,1,0:T(4,128)(2,1)}), bf16[128,4,128]{2,1,0:T(4,128)(2,1)S(1)}, u32[]{:S(2)}, u32[]{:S(2)}) %all-to-all-start.2) | async-done | bytes 131104 | tf_op jit(solution)/shard_map/all_to_all | solution.py:278
  152.4 6.5 %all-to-all-start.1 = ((bf16[128,8,256]{2,1,0:T(8,128)(2,1)}), bf16[128,8,256]{2,1,0:T(8,128)(2,1)S(1)}, u32[]{:S(2)}, u32[]{:S(2)}) async-start(bf16[128,8,256]{2,1,0:T(8,128)(2,1)} %bitcast.8), calls=%async_computation.1 | async-start | bytes 1048576 | tf_op jit(solution)/shard_map/all_to_all | solution.py:278
  160.0 2.4 %shard_map.150 = (bf16[1552,128]{1,0:T(8,128)(2,1)S(1)}, bf16[1552,128]{1,0:T(8,128)(2,1)S(1)}, bf16[1552,128]{1,0:T(8,128)(2,1)S(1)}, bf16[1552,128]{1,0:T(8,128)(2,1)S(1)}) custom-call(s32[1]{0:T(128)} %bitcast.col, bf16[512,512]{1,0:T(8,128)(2,1)S(1)} %copy-done.8, bf16[512,512]{1,0:T(8,128)(2,1)S(1)} %copy-done.10, s32[2,128]{1,0:T(2,128)S(1)} %bitcast.28, ...), custom_call_target="tpu_custom_call" | custom-call | tf_op jit(solution)/shard_map/pallas_call | solution.py:42
  162.4 4.3 %collective-permute-start.9 = (bf16[1552,128]{1,0:T(8,128)(2,1)S(1)}, bf16[1552,128]{1,0:T(8,128)(2,1)S(1)}, u32[]{:S(2)}, u32[]{:S(2)}) collective-permute-start(bf16[1552,128]{1,0:T(8,128)(2,1)S(1)} %get-tuple-element.48), channel_id=1, source_target_pairs={{0,1},{1,2},{2,3},{3,0},{4,5},{5,6},{6,7},{7,4},{8,9},{9,10},{10,1... | collective-permute-start | bytes 1191944 | tf_op jit(solution)/shard_map/ppermute | solution.py:28
  166.7 2.0 %collective-permute-start.10 = (bf16[1552,128]{1,0:T(8,128)(2,1)S(1)}, bf16[1552,128]{1,0:T(8,128)(2,1)S(1)}, u32[]{:S(2)}, u32[]{:S(2)}) collective-permute-start(bf16[1552,128]{1,0:T(8,128)(2,1)S(1)} %get-tuple-element.49), channel_id=1, source_target_pairs={{0,2},{1,3},{2,0},{3,1},{4,6},{5,7},{6,4},{7,5},{8,10},{9,11},{10,... | collective-permute-start | bytes 1191944 | tf_op jit(solution)/shard_map/ppermute | solution.py:28
  168.7 3.2 %collective-permute-start.11 = (bf16[1552,128]{1,0:T(8,128)(2,1)S(1)}, bf16[1552,128]{1,0:T(8,128)(2,1)S(1)}, u32[]{:S(2)}, u32[]{:S(2)}) collective-permute-start(bf16[1552,128]{1,0:T(8,128)(2,1)S(1)} %get-tuple-element.50), channel_id=1, source_target_pairs={{0,3},{1,0},{2,1},{3,2},{4,7},{5,4},{6,5},{7,6},{8,11},{9,8},{10,9... | collective-permute-start | bytes 1191944 | tf_op jit(solution)/shard_map/ppermute | solution.py:28
  172.8 1.8 convert_reduce_fusion
  174.6 8.8 %collective-permute-done.9.refs_1_ = bf16[1552,128]{1,0:T(8,128)(2,1)S(1)} collective-permute-done((bf16[1552,128]{1,0:T(8,128)(2,1)S(1)}, bf16[1552,128]{1,0:T(8,128)(2,1)S(1)}, u32[]{:S(2)}, u32[]{:S(2)}) %collective-permute-start.9) | collective-permute-done | bytes 397344 | tf_op jit(solution)/shard_map/ppermute | solution.py:28
  183.4 5.6 %collective-permute-done.11.refs_3_ = bf16[1552,128]{1,0:T(8,128)(2,1)S(1)} collective-permute-done((bf16[1552,128]{1,0:T(8,128)(2,1)S(1)}, bf16[1552,128]{1,0:T(8,128)(2,1)S(1)}, u32[]{:S(2)}, u32[]{:S(2)}) %collective-permute-start.11) | collective-permute-done | bytes 397344 | tf_op jit(solution)/shard_map/ppermute | solution.py:28
  189.0 1.3 shard_map.151
  (40 shorter events, 12.4 us)
Async XLA Ops:
  0.6 171.3 %copy-start = (bf16[2048,128]{1,0:T(8,128)(2,1)S(1)}, bf16[2048,128]{1,0:T(8,128)(2,1)}, u32[]{:S(2)}) copy-start(bf16[2048,128]{1,0:T(8,128)(2,1)} %param.16) | copy-start | bytes 1572868
  0.7 0.7 copy-start.12
  0.7 0.7 copy-start.11
  1.4 1.0 copy-start.1
  2.4 1.0 copy-start.6
  5.4 18.0 %copy-start.2 = (bf16[128,2048]{1,0:T(8,128)(2,1)S(1)}, bf16[128,2048]{1,0:T(8,128)(2,1)}, u32[]{:S(2)}) copy-start(bf16[128,2048]{1,0:T(8,128)(2,1)} %cot_ref.1) | copy-start | bytes 1572868
  5.4 18.0 %copy-start.13 = (bf16[128,128]{1,0:T(8,128)(2,1)S(1)}, bf16[128,128]{1,0:T(8,128)(2,1)}, u32[]{:S(2)}) copy-start(bf16[128,128]{1,0:T(8,128)(2,1)} %param.17) | copy-start | bytes 98308
  5.4 48.2 %all-to-all-start = ((bf16[128,8,512]{2,1,0:T(8,128)(2,1)}), bf16[128,8,512]{2,1,0:T(8,128)(2,1)S(1)}, u32[]{:S(2)}, u32[]{:S(2)}) async-start(bf16[128,8,512]{2,1,0:T(8,128)(2,1)} %bitcast.3), calls=%async_computation | async-start | bytes 2097152 | tf_op jit(solution)/shard_map/all_to_all | solution.py:278
  53.5 7.8 %copy-start.3 = (bf16[1,2048,128]{2,1,0:T(8,128)(2,1)S(1)}, bf16[1,2048,128]{2,1,0:T(8,128)(2,1)}, u32[]{:S(2)}) copy-start(bf16[1,2048,128]{2,1,0:T(8,128)(2,1)} %param.13) | copy-start | bytes 1572868
  53.5 7.9 %copy-start.4 = (bf16[1,2048,128]{2,1,0:T(8,128)(2,1)S(1)}, bf16[1,2048,128]{2,1,0:T(8,128)(2,1)}, u32[]{:S(2)}) copy-start(bf16[1,2048,128]{2,1,0:T(8,128)(2,1)} %param.14) | copy-start | bytes 1572868
  53.5 72.4 %all-to-all-start.3 = ((bf16[128,16,128]{2,1,0:T(8,128)(2,1)}), bf16[128,16,128]{2,1,0:T(8,128)(2,1)}, u32[]{:S(2)}, u32[]{:S(2)}) async-start(bf16[128,16,128]{2,1,0:T(8,128)(2,1)} %bitcast.31), calls=%async_computation.3 | async-start | bytes 1048576 | tf_op jit(solution)/shard_map/all_to_all | solution.py:278
  61.4 1.0 copy-start.5
  62.6 13.9 %collective-permute-start = (bf16[1536,128]{1,0:T(8,128)(2,1)S(1)}, bf16[1536,128]{1,0:T(8,128)(2,1)S(1)}, u32[]{:S(2)}, u32[]{:S(2)}) collective-permute-start(bf16[1536,128]{1,0:T(8,128)(2,1)S(1)} %get-tuple-element.34), channel_id=1, source_target_pairs={{0,1},{1,2},{2,3},{3,0},{4,5},{5,6},{6,7},{7,4},{8,9},{9,10},{10,1... | collective-permute-start | bytes 1179656 | tf_op jit(solution)/shard_map/ppermute | solution.py:28
  65.0 15.4 %collective-permute-start.1 = (bf16[1536,128]{1,0:T(8,128)(2,1)S(1)}, bf16[1536,128]{1,0:T(8,128)(2,1)S(1)}, u32[]{:S(2)}, u32[]{:S(2)}) collective-permute-start(bf16[1536,128]{1,0:T(8,128)(2,1)S(1)} %get-tuple-element.35), channel_id=1, source_target_pairs={{0,2},{1,3},{2,0},{3,1},{4,6},{5,7},{6,4},{7,5},{8,10},{9,11},{10,... | collective-permute-start | bytes 1179656 | tf_op jit(solution)/shard_map/ppermute | solution.py:28
  69.3 17.8 %collective-permute-start.2 = (bf16[1536,128]{1,0:T(8,128)(2,1)S(1)}, bf16[1536,128]{1,0:T(8,128)(2,1)S(1)}, u32[]{:S(2)}, u32[]{:S(2)}) collective-permute-start(bf16[1536,128]{1,0:T(8,128)(2,1)S(1)} %get-tuple-element.36), channel_id=1, source_target_pairs={{0,3},{1,0},{2,1},{3,2},{4,7},{5,4},{6,5},{7,6},{8,11},{9,8},{10,9... | collective-permute-start | bytes 1179656 | tf_op jit(solution)/shard_map/ppermute | solution.py:28
  88.9 0.8 copy-start.7
  89.7 0.8 copy-start.9
  90.5 13.9 %collective-permute-start.3 = (bf16[128,1536]{1,0:T(8,128)(2,1)S(1)}, bf16[128,1536]{1,0:T(8,128)(2,1)S(1)}, u32[]{:S(2)}, u32[]{:S(2)}) collective-permute-start(bf16[128,1536]{1,0:T(8,128)(2,1)S(1)} %get-tuple-element.40), channel_id=1, source_target_pairs={{0,1},{1,2},{2,3},{3,0},{4,5},{5,6},{6,7},{7,4},{8,9},{9,10},{10,1... | collective-permute-start | bytes 1179656 | tf_op jit(solution)/shard_map/ppermute | solution.py:28
  93.0 15.4 %collective-permute-start.4 = (bf16[128,1536]{1,0:T(8,128)(2,1)S(1)}, bf16[128,1536]{1,0:T(8,128)(2,1)S(1)}, u32[]{:S(2)}, u32[]{:S(2)}) collective-permute-start(bf16[128,1536]{1,0:T(8,128)(2,1)S(1)} %get-tuple-element.41), channel_id=1, source_target_pairs={{0,2},{1,3},{2,0},{3,1},{4,6},{5,7},{6,4},{7,5},{8,10},{9,11},{10,... | collective-permute-start | bytes 1179656 | tf_op jit(solution)/shard_map/ppermute | solution.py:28
  97.4 17.9 %collective-permute-start.5 = (bf16[128,1536]{1,0:T(8,128)(2,1)S(1)}, bf16[128,1536]{1,0:T(8,128)(2,1)S(1)}, u32[]{:S(2)}, u32[]{:S(2)}) collective-permute-start(bf16[128,1536]{1,0:T(8,128)(2,1)S(1)} %get-tuple-element.42), channel_id=1, source_target_pairs={{0,3},{1,0},{2,1},{3,2},{4,7},{5,4},{6,5},{7,6},{8,11},{9,8},{10,9... | collective-permute-start | bytes 1179656 | tf_op jit(solution)/shard_map/ppermute | solution.py:28
  116.4 23.8 %collective-permute-start.6 = (bf16[128,1536]{1,0:T(8,128)(2,1)S(1)}, bf16[128,1536]{1,0:T(8,128)(2,1)S(1)}, u32[]{:S(2)}, u32[]{:S(2)}) collective-permute-start(bf16[128,1536]{1,0:T(8,128)(2,1)S(1)} %get-tuple-element.43.refs_0_), channel_id=1, source_target_pairs={{0,1},{1,2},{2,3},{3,0},{4,5},{5,6},{6,7},{7,4},{8,9},{9,10},{10,1... | collective-permute-start | bytes 1179656 | tf_op jit(solution)/shard_map/ppermute | solution.py:28
  118.9 21.3 %collective-permute-start.7 = (bf16[128,1536]{1,0:T(8,128)(2,1)S(1)}, bf16[128,1536]{1,0:T(8,128)(2,1)S(1)}, u32[]{:S(2)}, u32[]{:S(2)}) collective-permute-start(bf16[128,1536]{1,0:T(8,128)(2,1)S(1)} %get-tuple-element.43.refs_0_), channel_id=1, source_target_pairs={{0,2},{1,3},{2,0},{3,1},{4,6},{5,7},{6,4},{7,5},{8,10},{9,11},{10,... | collective-permute-start | bytes 1179656 | tf_op jit(solution)/shard_map/ppermute | solution.py:28
  123.2 18.1 %collective-permute-start.8 = (bf16[128,1536]{1,0:T(8,128)(2,1)S(1)}, bf16[128,1536]{1,0:T(8,128)(2,1)}, u32[]{:S(2)}, u32[]{:S(2)}) collective-permute-start(bf16[128,1536]{1,0:T(8,128)(2,1)S(1)} %get-tuple-element.43.refs_0_), channel_id=1, source_target_pairs={{0,3},{1,0},{2,1},{3,2},{4,7},{5,4},{6,5},{7,6},{8,11},{9,8},{10,9... | collective-permute-start | bytes 1179656 | tf_op jit(solution)/shard_map/ppermute | solution.py:28
  125.9 26.5 %all-to-all-start.2 = ((bf16[128,4,128]{2,1,0:T(4,128)(2,1)}), bf16[128,4,128]{2,1,0:T(4,128)(2,1)S(1)}, u32[]{:S(2)}, u32[]{:S(2)}) async-start(bf16[128,4,128]{2,1,0:T(4,128)(2,1)} %bitcast.10), calls=%async_computation.2 | async-start | bytes 262144 | tf_op jit(solution)/shard_map/all_to_all | solution.py:278
  152.4 6.5 %copy-start.8 = (bf16[512,512]{1,0:T(8,128)(2,1)S(1)}, bf16[512,512]{1,0:T(8,128)(2,1)}, u32[]{:S(2)}) copy-start(bf16[512,512]{1,0:T(8,128)(2,1)} %copy-done.7) | copy-start | bytes 1572868
  152.4 37.9 %all-to-all-start.1 = ((bf16[128,8,256]{2,1,0:T(8,128)(2,1)}), bf16[128,8,256]{2,1,0:T(8,128)(2,1)S(1)}, u32[]{:S(2)}, u32[]{:S(2)}) async-start(bf16[128,8,256]{2,1,0:T(8,128)(2,1)} %bitcast.8), calls=%async_computation.1 | async-start | bytes 1048576 | tf_op jit(solution)/shard_map/all_to_all | solution.py:278
  158.9 1.0 copy-start.10
  162.4 21.0 %collective-permute-start.9 = (bf16[1552,128]{1,0:T(8,128)(2,1)S(1)}, bf16[1552,128]{1,0:T(8,128)(2,1)S(1)}, u32[]{:S(2)}, u32[]{:S(2)}) collective-permute-start(bf16[1552,128]{1,0:T(8,128)(2,1)S(1)} %get-tuple-element.48), channel_id=1, source_target_pairs={{0,1},{1,2},{2,3},{3,0},{4,5},{5,6},{6,7},{7,4},{8,9},{9,10},{10,1... | collective-permute-start | bytes 1191944 | tf_op jit(solution)/shard_map/ppermute | solution.py:28
  166.7 16.7 %collective-permute-start.10 = (bf16[1552,128]{1,0:T(8,128)(2,1)S(1)}, bf16[1552,128]{1,0:T(8,128)(2,1)S(1)}, u32[]{:S(2)}, u32[]{:S(2)}) collective-permute-start(bf16[1552,128]{1,0:T(8,128)(2,1)S(1)} %get-tuple-element.49), channel_id=1, source_target_pairs={{0,2},{1,3},{2,0},{3,1},{4,6},{5,7},{6,4},{7,5},{8,10},{9,11},{10,... | collective-permute-start | bytes 1191944 | tf_op jit(solution)/shard_map/ppermute | solution.py:28
  168.7 20.2 %collective-permute-start.11 = (bf16[1552,128]{1,0:T(8,128)(2,1)S(1)}, bf16[1552,128]{1,0:T(8,128)(2,1)S(1)}, u32[]{:S(2)}, u32[]{:S(2)}) collective-permute-start(bf16[1552,128]{1,0:T(8,128)(2,1)S(1)} %get-tuple-element.50), channel_id=1, source_target_pairs={{0,3},{1,0},{2,1},{3,2},{4,7},{5,4},{6,5},{7,6},{8,11},{9,8},{10,9... | collective-permute-start | bytes 1191944 | tf_op jit(solution)/shard_map/ppermute | solution.py:28

commit v3 on v2

v3 whole, which is shorter than its diff:
```python
import functools

import jax
import jax.numpy as jnp
from jax import lax
from jax.experimental import pallas as pl
from jax.experimental.pallas import tpu as pltpu
from jax.sharding import Mesh
from jax.sharding import PartitionSpec as P

EP = ("z", "y", "core")
F32 = jnp.float32
BF16 = jnp.bfloat16
COLS = (((1,), (0,)), ((), ()))
ROWS = (((0,), (0,)), ((), ()))
LAST = (((1,), (1,)), ((), ()))
VMEM = pl.BlockSpec(memory_space=pltpu.VMEM)
SMEM = pl.BlockSpec(memory_space=pltpu.SMEM)
HBM = pl.BlockSpec(memory_space=pltpu.HBM)
LIMIT = pltpu.CompilerParams(vmem_limit_bytes=12 * 2**20)
CAP = 4
LANES = 128
FAR = 2
NEAR = (1, 3)
GROUP = 16


def mm(a, b, dims=COLS):
    return lax.dot_general(a, b, dims, preferred_element_type=F32)


def around(array):
    size = lax.axis_size("tp")
    arrays = array if isinstance(array, (list, tuple)) else [array] * (size - 1)
    got = []
    for k, part in enumerate(arrays):
        got.append(lax.ppermute(part, "tp", [(i, (i + k + 1) % size) for i in range(size)]))
    return got


def over(array, axes):
    size = lax.axis_size(axes)
    rows = array.reshape(size, -1, array.shape[-1])
    return lax.all_to_all(rows, axes, split_axis=0, concat_axis=0, tiled=True).reshape(array.shape)


def at(col, step, parts):
    return lax.rem(col[0] + (step + parts), parts)


def span(index, width):
    return pl.ds(pl.multiple_of(index * width, width), width)


def local(kernel, out, *args, spaces="", outs="", scratch=(), alias=None):
    spec = {"s": SMEM, "v": VMEM, "h": HBM}
    kept = {"h": pltpu.HBM}
    spaces = spaces + "v" * (len(args) - len(spaces))
    args = [
        pltpu.with_memory_space_constraint(a, kept[k]) if k in kept else a
        for a, k in zip(args, spaces)
    ]
    single = not isinstance(out, (list, tuple))
    out = [out] if single else list(out)
    outs = outs + "v" * (len(out) - len(outs))
    out = [kept[k](o.shape, o.dtype) if k in kept else o for o, k in zip(out, outs)]
    got = pl.pallas_call(
        kernel,
        in_specs=[spec[k] for k in spaces],
        out_specs=[spec[k] for k in outs],
        out_shape=out,
        scratch_shapes=scratch,
        input_output_aliases=alias or {},
        compiler_params=LIMIT,
    )(*args)
    return got[0] if single else got


def weave():
    rows = 64 * CAP
    row = lax.broadcasted_iota(jnp.int32, (rows, rows), 0)
    col = lax.broadcasted_iota(jnp.int32, (rows, rows), 1)
    s, rest = row // (2 * CAP), row % (2 * CAP)
    h, r = rest // CAP, rest % CAP
    return jnp.where(col == h * (rows // 2) + s * CAP + r, 1.0, 0.0).astype(BF16)


def chosen(routes_ref, slots):
    count = routes_ref.shape[1]
    row = lax.broadcasted_iota(jnp.int32, (slots, count), 0)
    expert = row // CAP
    first = expert == routes_ref[0:1, :]
    second = expert == routes_ref[1:2, :]
    named = jnp.where(first | second, 1.0, 0.0)
    earlier = lax.broadcasted_iota(jnp.int32, (count, count), 0)
    later = lax.broadcasted_iota(jnp.int32, (count, count), 1)
    before = jnp.where(earlier < later, 1.0, 0.0).astype(BF16)
    rank = mm(named.astype(BF16), before)
    place = (row - expert * CAP).astype(F32)
    hit = jnp.where(rank == place, named, 0.0)
    return hit, jnp.where(first, hit, 0.0), jnp.where(second, hit, 0.0)


def dispatch_kernel(
    col, routes_ref, weights_ref, tok_ref, cot_ref, sent_ref, routes, weights, tok, cot, sent, sems
):
    slots = sent_ref.shape[0] // 2
    place = span(col[0], tok.shape[1])
    copies = [
        pltpu.make_async_copy(src, dst, sems.at[k])
        for k, (src, dst) in enumerate(
            [
                (routes_ref, routes),
                (weights_ref, weights),
                (tok_ref.at[:, place], tok),
                (cot_ref.at[:, place], cot),
            ]
        )
    ]
    for copy in copies:
        copy.start()
    order = weave()
    copies[0].wait()
    hit, one, two = chosen(routes, slots)
    pick = hit.astype(BF16)
    copies[1].wait()
    scale = weights[...].astype(BF16).astype(F32)
    weight = jnp.sum(one * scale[0:1, :] + two * scale[1:2, :], axis=1, keepdims=True)
    copies[2].wait()
    x = mm(pick, tok[...]).astype(BF16)
    copies[3].wait()
    g = (weight * mm(pick, cot[...])).astype(BF16)
    half = order.shape[0] // 2
    leaving = []
    for b in range(slots // half):
        both = jnp.concatenate([x[b * half : (b + 1) * half], g[b * half : (b + 1) * half]], axis=0)
        rows = slice(2 * b * half, 2 * (b + 1) * half)
        sent[rows, :] = mm(order, both).astype(BF16)
        leaving.append(
            pltpu.make_async_copy(sent.at[rows, :], sent_ref.at[rows, :], sems.at[4 + b])
        )
        leaving[-1].start()
    for copy in leaving:
        copy.wait()


def pick_kernel(routes_ref, weights_ref, one_ref, two_ref, inverse_ref):
    _, one, two = chosen(routes_ref, one_ref.shape[0])
    one_ref[...] = one.astype(BF16)
    two_ref[...] = two.astype(BF16)
    inverse_ref[...] = 1.0 / weights_ref[...].astype(BF16).astype(F32)


def dots_kernel(cot_ref, hid_ref, down_ref, grad_ref, terms_ref):
    cot = cot_ref[...]
    grad_ref[...] = mm(cot, down_ref[...]).astype(BF16)
    terms = mm(cot, hid_ref[...], ROWS).astype(BF16)
    inner, outer, group, width = terms_ref.shape
    terms = terms.reshape(outer, inner, group, width)
    for k in range(outer):
        terms_ref[:, k] = terms[k]


def fold_kernel(terms_ref, out_ref):
    terms = terms_ref[...].astype(F32)
    out_ref[...] = jnp.sum(terms.reshape(-1, *out_ref.shape), axis=0).astype(BF16)


def total_kernel(terms_ref, out_ref):
    rows, width = terms_ref.shape
    terms = terms_ref[...].astype(F32).reshape(rows // GROUP, GROUP, width)
    out_ref[...] = jnp.sum(terms, axis=0)


def pack_kernel(col, gate_ref, up_ref, down_ref, own_out, *refs):
    *outs, own_ref, sem = refs
    parts = len(outs) + 1
    quarter = gate_ref.shape[0] // parts
    block = gate_ref.shape[1]
    own_copy = pltpu.make_async_copy(own_ref, own_out, sem)
    for k, out in enumerate([own_ref, *outs]):
        to = at(col, k, parts)
        out[:quarter, :] = gate_ref[span(to, quarter), :]
        out[quarter : 2 * quarter, :] = up_ref[span(to, quarter), :]
        down = down_ref[:, span(to, quarter)]
        for c in range(quarter // block):
            row = 2 * quarter + c * block
            out[row : row + block, :] = down[:, c * block : (c + 1) * block]
        if k == 0:
            own_copy.start()
    own_copy.wait()


def collect_kernel(col, own_ref, *refs):
    *packed, both_ref, down_ref, sems = refs
    parts = len(packed) + 1
    quarter, width = both_ref.shape
    block = width // (2 * parts)
    copies = []
    for k, ref in enumerate([own_ref, *packed]):
        index = at(col, -k, parts)
        place = span(index, block)
        pairs = [
            (slice(0, quarter), both_ref.at[:, place]),
            (slice(quarter, 2 * quarter), both_ref.at[:, span(index + parts, block)]),
        ]
        for c in range(quarter // block):
            row = 2 * quarter + c * block
            across = slice(c * block, (c + 1) * block)
            pairs.append((slice(row, row + block), down_ref.at[place, across]))
        for rows, out in pairs:
            if k == 0:
                copies.append(pltpu.make_async_copy(ref.at[rows, :], out, sems.at[len(copies)]))
                copies[-1].start()
            else:
                out[...] = ref[rows, :]
    for copy in copies:
        copy.wait()


def apart(order, got):
    split = mm(order, got, ROWS).astype(BF16)
    half = split.shape[0] // 2
    return split[:half], split[half:]


def far_kernel(col, got_ref, both_ref, down_ref, out_ref):
    rows = out_ref.shape[0]
    parts = got_ref.shape[0] // (2 * rows)
    width = both_ref.shape[1]
    x, g = apart(weave(), got_ref[span(at(col, FAR, parts), 2 * rows), :])
    out_ref[:, :width] = mm(x, both_ref[...]).astype(BF16)
    out_ref[:, width:] = mm(g, down_ref[...], LAST).astype(BF16)


def near_kernel(col, got_ref, both_ref, down_ref, xg_out, own_out, *refs):
    *outs, xg_ref, own_ref, sems = refs
    rows = own_ref.shape[0]
    parts = got_ref.shape[0] // (2 * rows)
    width = both_ref.shape[1]
    quarter = got_ref.shape[1]
    order = weave()
    for b in range(parts):
        x, g = apart(order, got_ref[2 * b * rows : 2 * (b + 1) * rows, :])
        xg_ref[b * rows : (b + 1) * rows, :quarter] = x
        xg_ref[b * rows : (b + 1) * rows, quarter:] = g
    xg_copy = pltpu.make_async_copy(xg_ref, xg_out, sems.at[0])
    xg_copy.start()
    blocks = [span(at(col, k, parts), rows) for k in [0, *NEAR]]
    xg = jnp.concatenate([xg_ref[place, :] for place in blocks], axis=0)
    grown = mm(xg[:, :quarter], both_ref[...]).astype(BF16)
    backed = mm(xg[:, quarter:], down_ref[...], LAST).astype(BF16)
    own_copy = pltpu.make_async_copy(own_ref, own_out, sems.at[1])
    for k, out in enumerate([own_ref, *outs]):
        out[:, :width] = grown[k * rows : (k + 1) * rows]
        out[:, width:] = backed[k * rows : (k + 1) * rows]
        if k == 0:
            own_copy.start()
    xg_copy.wait()
    own_copy.wait()


def middle_kernel(*refs):
    *parts, grads_ref = refs
    rows, width = parts[0].shape
    hidden = width // 3
    total = parts[0][...].astype(F32)
    for ref in parts[1:]:
        total = total + ref[...].astype(F32)
    gate = total[:, :hidden]
    upper = total[:, hidden : 2 * hidden]
    backed = total[:, 2 * hidden :]
    sigma = jax.nn.sigmoid(gate)
    active = gate * sigma
    hid = (active * upper).astype(BF16)
    grads_ref[:, :hidden] = (backed * upper * sigma * (1.0 + gate * (1.0 - sigma))).astype(BF16)
    grads_ref[:, hidden : 2 * hidden] = (backed * active).astype(BF16)
    grads_ref[:, 2 * hidden : width] = hid
    share = jnp.sum(hid.astype(F32) * backed, axis=1, keepdims=True)
    grads_ref[:, width:] = jnp.broadcast_to(share, (rows, LANES)).astype(BF16)


def input_kernel(col, *refs):
    *grads, both_ref, back_out, out_ref, sems = refs
    parts = len(grads)
    rows = grads[0].shape[0]
    width = both_ref.shape[1]
    whole = jnp.concatenate([ref[:, :width] for ref in grads], axis=0)
    out = mm(whole, both_ref[...], LAST).astype(BF16)
    order = weave()
    half = out.shape[1] // 2
    copies = []
    for k, ref in enumerate(grads):
        own = out[k * rows : (k + 1) * rows]
        both = jnp.concatenate([own[:, :half], own[:, half:]], axis=0)
        place = slice(2 * k * rows, 2 * (k + 1) * rows)
        out_ref[place, :half] = mm(order, both).astype(BF16)
        share = ref[:, ref.shape[1] - LANES :]
        out_ref[place, half:] = mm(order[:, :rows], share).astype(BF16)
        to = back_out.at[span(at(col, -k, parts), 2 * rows), :]
        copies.append(pltpu.make_async_copy(out_ref.at[place, :], to, sems.at[k]))
        copies[-1].start()
    for copy in copies:
        copy.wait()


def outer_terms(col, steps, xg_ref, grads):
    parts = len(grads)
    rows = grads[0].shape[0]
    block = (grads[0].shape[1] - LANES) // (3 * parts)
    quarter = xg_ref.shape[1] // 2
    order = [span(at(col, -k, parts), rows) for k in range(parts)]
    x = jnp.concatenate([xg_ref[place, :quarter] for place in order], axis=0)
    g = jnp.concatenate([xg_ref[place, quarter:] for place in order], axis=0)

    def units(kinds):
        places = [span(at(col, k, parts) + kind * parts, block) for k in steps for kind in kinds]
        return jnp.concatenate(
            [jnp.concatenate([ref[:, place] for place in places], axis=1) for ref in grads], axis=0
        )

    both = mm(x, units((0, 1)), ROWS).astype(BF16)
    down = mm(units((2,)), g, ROWS).astype(BF16)
    return [
        (
            both[:, 2 * n * block : (2 * n + 1) * block],
            both[:, (2 * n + 1) * block : (2 * n + 2) * block],
            down[n * block : (n + 1) * block],
        )
        for n in range(len(steps))
    ]


def outer_kernel(col, xg_ref, *refs, steps):
    grads, outs = refs[: -len(steps)], refs[-len(steps) :]
    for out, (gate, up, down) in zip(outs, outer_terms(col, steps, xg_ref, grads)):
        quarter, block = gate.shape
        out[:quarter, :] = gate
        out[quarter : 2 * quarter, :] = up
        for c in range(quarter // block):
            row = 2 * quarter + c * block
            out[row : row + block, :] = down[:, c * block : (c + 1) * block]


def own_kernel(col, xg_ref, *refs):
    *grads, gate_out, up_out, down_out, gate_ref, up_ref, down_ref, sems = refs
    place = span(at(col, 0, len(grads)), gate_ref.shape[0])
    [(gate, up, down)] = outer_terms(col, (0,), xg_ref, grads)
    gate_ref[...] = gate
    up_ref[...] = up
    down_ref[...] = down
    copies = [
        pltpu.make_async_copy(gate_ref, gate_out.at[place, :], sems.at[0]),
        pltpu.make_async_copy(up_ref, up_out.at[place, :], sems.at[1]),
        pltpu.make_async_copy(down_ref, down_out.at[:, place], sems.at[2]),
    ]
    for copy in copies:
        copy.start()
    for copy in copies:
        copy.wait()


def finish_kernel(col, *refs):
    *refs, sems = refs
    parts = len(refs) - 5
    got, (gate_ref, up_ref, down_ref) = refs[: parts - 1], refs[parts + 2 :]
    block = gate_ref.shape[1]
    quarter = gate_ref.shape[0] // parts
    copies = []
    for k, ref in enumerate(got):
        index = at(col, -k - 1, parts)
        place = span(index, quarter)
        pairs = [
            (ref.at[:quarter, :], gate_ref.at[place, :]),
            (ref.at[quarter : 2 * quarter, :], up_ref.at[place, :]),
        ]
        for c in range(quarter // block):
            row = 2 * quarter + c * block
            across = span(index * (quarter // block) + c, block)
            pairs.append((ref.at[row : row + block, :], down_ref.at[:, across]))
        for src, dst in pairs:
            copies.append(pltpu.make_async_copy(src, dst, sems.at[len(copies)]))
            copies[-1].start()
    for copy in copies:
        copy.wait()


def combine_kernel(inverse_ref, one_ref, two_ref, back_ref, out_ref, weights_out):
    slots = one_ref.shape[0]
    order = weave()
    half = order.shape[0] // 2
    width = out_ref.shape[1] // 2
    left, right, shares = [], [], []
    for b in range(slots // half):
        own = mm(order, back_ref[2 * b * half : 2 * (b + 1) * half, :], ROWS).astype(BF16)
        left.append(own[:half, :width])
        right.append(own[half:, :width])
        shares.append(own[:half, width:].astype(F32))
    one = one_ref[...]
    two = two_ref[...]
    pick = one + two
    out_ref[:, :width] = mm(pick, jnp.concatenate(left, axis=0), ROWS).astype(BF16)
    out_ref[:, width:] = mm(pick, jnp.concatenate(right, axis=0), ROWS).astype(BF16)
    share = jnp.concatenate(shares, axis=0)
    for k, mask in enumerate([one, two]):
        total = jnp.sum(mask.astype(F32) * share, axis=0, keepdims=True)
        weights_out[k : k + 1, :] = total * inverse_ref[k : k + 1, :]


def experts(
    tokens,
    cotangent,
    route_weights,
    routes,
    gate_proj,
    up_proj,
    down_proj,
    shared_down,
    shared_hidden,
):
    rows, feat = tokens.shape
    top = routes.shape[1]
    ep = lax.axis_size(EP)
    tp = lax.axis_size("tp")
    slots = ep * CAP
    quarter = feat // tp
    block = gate_proj.shape[2]
    hidden = block * tp
    some = slots // tp
    half = lambda *shape: jax.ShapeDtypeStruct(shape, BF16)
    col = lax.axis_index("tp").astype(jnp.int32).reshape(1)
    routes_t = routes.T
    weights_t = route_weights.T

    sent = local(
        dispatch_kernel,
        half(2 * slots, quarter),
        col,
        routes_t,
        weights_t,
        tokens,
        cotangent,
        spaces="shhhh",
        outs="h",
        scratch=[
            pltpu.VMEM(routes_t.shape, jnp.int32),
            pltpu.VMEM(weights_t.shape, F32),
            pltpu.VMEM((rows, quarter), BF16),
            pltpu.VMEM((rows, quarter), BF16),
            pltpu.VMEM((2 * slots, quarter), BF16),
            pltpu.SemaphoreType.DMA((4 + tp,)),
        ],
    )
    got = over(sent, EP)

    packed = local(
        pack_kernel,
        [half(3 * quarter, block)] * tp,
        col,
        gate_proj.reshape(feat, block),
        up_proj.reshape(feat, block),
        down_proj.reshape(block, feat),
        spaces="s",
        outs="h",
        scratch=[pltpu.VMEM((3 * quarter, block), BF16), pltpu.SemaphoreType.DMA],
    )
    packed = [packed[0], *around(packed[1:])]
    both, down = local(
        collect_kernel,
        [half(quarter, 2 * hidden), half(hidden, quarter)],
        col,
        *packed,
        spaces="sh",
        scratch=[pltpu.SemaphoreType.DMA((2 + tp,))],
    )

    far = local(far_kernel, half(some, 3 * hidden), col, got, both, down, spaces="s")
    xg, own, *near = local(
        near_kernel,
        [half(slots, 2 * quarter)] + [half(some, 3 * hidden)] * (1 + len(NEAR)),
        col,
        got,
        both,
        down,
        spaces="s",
        outs="hh",
        scratch=[
            pltpu.VMEM((slots, 2 * quarter), BF16),
            pltpu.VMEM((some, 3 * hidden), BF16),
            pltpu.SemaphoreType.DMA((2,)),
        ],
    )
    part = [own, *around([near[0], far, near[1]])]
    grads = local(middle_kernel, half(some, 3 * hidden + LANES), *part)
    grads = [grads, *around(grads)]

    back = local(
        input_kernel,
        half(2 * slots, quarter // 2 + LANES),
        col,
        *grads,
        both,
        spaces="s",
        outs="h",
        scratch=[
            pltpu.VMEM((2 * slots, quarter // 2 + LANES), BF16),
            pltpu.SemaphoreType.DMA((tp,)),
        ],
    )
    back = over(back, EP)
    one, two, inverse = local(
        pick_kernel,
        [half(slots, rows)] * 2 + [jax.ShapeDtypeStruct((top, rows), F32)],
        routes_t,
        weights_t,
    )
    tokens_grad, weights_grad = local(
        combine_kernel,
        [half(rows, quarter), jax.ShapeDtypeStruct((top, rows), F32)],
        inverse,
        one,
        two,
        back,
    )
    weights_grad = weights_grad.T

    outer = {}
    for steps in ((FAR,), NEAR):
        got = local(
            functools.partial(outer_kernel, steps=steps),
            [half(3 * quarter, block)] * len(steps),
            col,
            xg,
            *grads,
            spaces="s",
        )
        outer.update(zip(steps, got))
    outer = around([outer[k] for k in range(1, tp)])
    whole = [half(feat, block), half(feat, block), half(block, feat)]
    own = local(
        own_kernel,
        whole,
        col,
        xg,
        *grads,
        spaces="s",
        outs="hhh",
        scratch=[
            pltpu.VMEM((quarter, block), BF16),
            pltpu.VMEM((quarter, block), BF16),
            pltpu.VMEM((block, quarter), BF16),
            pltpu.SemaphoreType.DMA((3,)),
        ],
    )
    gate_grad, up_grad, down_grad = local(
        finish_kernel,
        whole,
        col,
        *outer,
        *own,
        spaces="s" + "v" * (tp - 1) + "hhh",
        outs="hhh",
        scratch=[pltpu.SemaphoreType.DMA(((tp - 1) * (2 + tp),))],
        alias={tp: 0, tp + 1: 1, tp + 2: 2},
    )

    inner = ep // lax.axis_size("z")
    group = feat // ep
    hidden_grad, shared = local(
        dots_kernel,
        [half(rows, block), half(inner, ep // inner, group, block)],
        cotangent,
        shared_hidden,
        shared_down,
    )
    shared = over(shared.reshape(feat, block), ("y", "core"))
    shared = local(fold_kernel, half(feat // inner, block), shared)
    shared = over(shared, "z")
    shared_grad = local(
        total_kernel, jax.ShapeDtypeStruct((feat // ep, block), F32), shared
    )
    return (
        tokens_grad,
        weights_grad,
        gate_grad.reshape(gate_proj.shape),
        up_grad.reshape(up_proj.shape),
        down_grad.reshape(down_proj.shape),
        hidden_grad,
        shared_grad,
    )


def solution(mesh):
    devices = mesh.devices
    split = Mesh(devices.reshape(8, -1, 2, devices.shape[-1]), (*EP, "tp"))
    return jax.shard_map(
        experts,
        mesh=split,
        in_specs=(
            P(EP, None),
            P(EP, None),
            P(EP, None),
            P(EP, None),
            P(EP, None, "tp"),
            P(EP, None, "tp"),
            P(EP, "tp", None),
            P(None, "tp"),
            P(EP, "tp"),
        ),
        out_specs=(
            P(EP, "tp"),
            P(EP, None),
            P(EP, None, "tp"),
            P(EP, None, "tp"),
            P(EP, "tp", None),
            P(EP, "tp"),
            P(EP, "tp"),
        ),
        check_vma=False,
    )
```

time: 193 us -> 156 us (0.81)
  waiting for transfers between devices: 83.9 us -> 59.6 us
  starting transfers between devices: 83.7 us -> 72.5 us
  Pallas kernels: 12.6 us -> 20.2 us
  local copies, waits for them, and re-layouts: 6.5 us -> 0.06 us
  matrix products: 2.04 us -> 0 us
    all_to_all x4, waiting for transfers between devices: 37.5 us -> 18.4 us  [over(): lax.all_to_all(rows, axes, split_axis=0, concat_axis=0, tiled=True)]
    all_to_all x4, starting transfers between devices: 46.5 us -> 36.1 us  [over(): lax.all_to_all(rows, axes, split_axis=0, concat_axis=0, tiled=True)]
    pallas_call x9 -> x16, Pallas kernels: 12.6 us -> 20.2 us  [local(): pl.pallas_call(kernel, in_specs=[spec[k] for k in spaces], out_specs=[spe...]
    unnamed x28 -> x20, local copies, waits for them, and re-layouts: 6.5 us -> 0.06 us
    ppermute x12, waiting for transfers between devices: 46.5 us -> 41.2 us  [around(): lax.ppermute(part, 'tp', [(i, (i + k + 1) % size) for i in range(size)])]
    dot_general x2 -> x0, matrix products: 2.04 us -> none  [the longest x1 1.14 us: experts(): lax.dot_general(cotangent, shared_hidden, ROWS, preferred_element_type=F32)]
  transfers between devices with their start and end apart: 16 -> 16, of which waited for: 11 -> 9; matrix products, arithmetic and copies ran while one was open for 2% -> 0% of each run, Pallas kernels for 5% -> 10%
where the time goes in v3:
time: 156 us; the launch traced here: 153 us
  starting transfers between devices  72.5 us (46%)
  waiting for transfers between devices  59.6 us (38%)
  Pallas kernels  20.2 us (13%)
    ppermute x12, waiting for transfers between devices, around(): lax.ppermute(part, 'tp', [(i, (i + k + 1) % size) for i in range(size)])  41.2 us
    ppermute x12, starting transfers between devices, around(): lax.ppermute(part, 'tp', [(i, (i + k + 1) % size) for i in range(size)])  36.4 us
    all_to_all x4, starting transfers between devices, over(): lax.all_to_all(rows, axes, split_axis=0, concat_axis=0, tiled=True)  36.1 us
    pallas_call x16, Pallas kernels, local(): pl.pallas_call(kernel, in_specs=[spec[k] for k in spaces], out_specs=[spe...  20.2 us
    all_to_all x4, waiting for transfers between devices, over(): lax.all_to_all(rows, axes, split_axis=0, concat_axis=0, tiled=True)  18.4 us
  transfers between devices with their start and end apart: 16, of which 9 were waited for; matrix products, arithmetic and copies ran while one was open for 0% of the time, Pallas kernels for 10%

profile of v3, /device:TPU:6, one launch (start us, length us, event | category | flops | bytes accessed | tf_op | source)
XLA Modules:
  0.0 153.4 jit_solution(7219881661347888721)
XLA Ops:
  0.6 2.8 %shard_map.145 = bf16[1024,512]{1,0:T(8,128)(2,1)} custom-call(s32[1]{0:T(128)} %bitcast.2.col, s32[2,128]{1,0:T(2,128)} %bitcast.24, f32[2,128]{1,0:T(2,128)} %bitcast.26, bf16[128,2048]{1,0:T(8,128)(2,1)} %tok_ref.1, bf16[128,2048]{1,0:T(8,128)(2,1)} %cot_ref.3), custom_call_target="tpu_custom_call" | custom-call | tf_op jit(solution)/shard_map/pallas_call | solution.py:67
  3.5 17.9 %all-to-all-start = ((bf16[128,8,512]{2,1,0:T(8,128)(2,1)}), bf16[128,8,512]{2,1,0:T(8,128)(2,1)S(1)}, u32[]{:S(2)}, u32[]{:S(2)}) async-start(bf16[128,8,512]{2,1,0:T(8,128)(2,1)} %bitcast.28), calls=%async_computation | async-start | bytes 2097152 | tf_op jit(solution)/shard_map/all_to_all | solution.py:44
  21.5 1.8 %shard_map.146 = (bf16[1536,128]{1,0:T(8,128)(2,1)}, bf16[1536,128]{1,0:T(8,128)(2,1)}, bf16[1536,128]{1,0:T(8,128)(2,1)}, bf16[1536,128]{1,0:T(8,128)(2,1)}) custom-call(s32[1]{0:T(128)} %bitcast.2.col, bf16[2048,128]{1,0:T(8,128)(2,1)S(1)} %bitcast.20, bf16[2048,128]{1,0:T(8,128)(2,1)S(1)} %bitcast.21, bf16[128,2048]{1,0:T(8,128)(2,1)S(1)} %bitcast.22), custom_call_target="tpu_custom_call" | custom-call | tf_op jit(solution)/shard_map/pallas_call | solution.py:67
  23.3 2.4 %collective-permute-start = (bf16[1536,128]{1,0:T(8,128)(2,1)}, bf16[1536,128]{1,0:T(8,128)(2,1)S(1)}, u32[]{:S(2)}, u32[]{:S(2)}) collective-permute-start(bf16[1536,128]{1,0:T(8,128)(2,1)} %get-tuple-element.36), channel_id=1, source_target_pairs={{0,1},{1,2},{2,3},{3,0},{4,5},{5,6},{6,7},{7,4},{8,9},{9,10},{10,1... | collective-permute-start | bytes 1179656 | tf_op jit(solution)/shard_map/ppermute | solution.py:37
  25.7 4.3 %collective-permute-start.1 = (bf16[1536,128]{1,0:T(8,128)(2,1)}, bf16[1536,128]{1,0:T(8,128)(2,1)S(1)}, u32[]{:S(2)}, u32[]{:S(2)}) collective-permute-start(bf16[1536,128]{1,0:T(8,128)(2,1)} %get-tuple-element.37), channel_id=1, source_target_pairs={{0,2},{1,3},{2,0},{3,1},{4,6},{5,7},{6,4},{7,5},{8,10},{9,11},{10,... | collective-permute-start | bytes 1179656 | tf_op jit(solution)/shard_map/ppermute | solution.py:37
  30.0 1.9 %collective-permute-start.2 = (bf16[1536,128]{1,0:T(8,128)(2,1)}, bf16[1536,128]{1,0:T(8,128)(2,1)S(1)}, u32[]{:S(2)}, u32[]{:S(2)}) collective-permute-start(bf16[1536,128]{1,0:T(8,128)(2,1)} %get-tuple-element.38), channel_id=1, source_target_pairs={{0,3},{1,0},{2,1},{3,2},{4,7},{5,4},{6,5},{7,6},{8,11},{9,8},{10,9... | collective-permute-start | bytes 1179656 | tf_op jit(solution)/shard_map/ppermute | solution.py:37
  32.0 1.2 shard_map.157
  33.2 18.4 %all-to-all-done = bf16[128,8,512]{2,1,0:T(8,128)(2,1)S(1)} async-done(((bf16[128,8,512]{2,1,0:T(8,128)(2,1)}), bf16[128,8,512]{2,1,0:T(8,128)(2,1)S(1)}, u32[]{:S(2)}, u32[]{:S(2)}) %all-to-all-start) | async-done | bytes 1048608 | tf_op jit(solution)/shard_map/all_to_all | solution.py:44
  51.6 4.3 %all-to-all-start.2 = ((bf16[16,128,128]{2,1,0:T(8,128)(2,1)}), bf16[16,128,128]{2,1,0:T(8,128)(2,1)}, u32[]{:S(2)}, u32[]{:S(2)}) async-start(bf16[16,128,128]{2,1,0:T(8,128)(2,1)} %bitcast.14), calls=%async_computation.2 | async-start | bytes 1048576 | tf_op jit(solution)/shard_map/all_to_all | solution.py:44
  57.0 2.2 %shard_map.148 = (bf16[512,1024]{1,0:T(8,128)(2,1)}, bf16[128,1536]{1,0:T(8,128)(2,1)}, bf16[128,1536]{1,0:T(8,128)(2,1)S(1)}, bf16[128,1536]{1,0:T(8,128)(2,1)S(1)}) custom-call(s32[1]{0:T(128)} %bitcast.2.col, bf16[1024,512]{1,0:T(8,128)(2,1)S(1)} %bitcast.18, bf16[512,1024]{1,0:T(8,128)(2,1)S(1)} %get-tuple-element.39.both_ref.refs_4_, ...), custom_call_target="tpu_custom_call" | custom-call | tf_op jit(solution)/shard_map/pallas_call | solution.py:67
  59.9 2.4 %collective-permute-start.3 = (bf16[128,1536]{1,0:T(8,128)(2,1)S(1)}, bf16[128,1536]{1,0:T(8,128)(2,1)S(1)}, u32[]{:S(2)}, u32[]{:S(2)}) collective-permute-start(bf16[128,1536]{1,0:T(8,128)(2,1)S(1)} %get-tuple-element.42), channel_id=1, source_target_pairs={{0,1},{1,2},{2,3},{3,0},{4,5},{5,6},{6,7},{7,4},{8,9},{9,10},{10,1... | collective-permute-start | bytes 1179656 | tf_op jit(solution)/shard_map/ppermute | solution.py:37
  62.3 4.3 %collective-permute-start.4 = (bf16[128,1536]{1,0:T(8,128)(2,1)S(1)}, bf16[128,1536]{1,0:T(8,128)(2,1)S(1)}, u32[]{:S(2)}, u32[]{:S(2)}) collective-permute-start(bf16[128,1536]{1,0:T(8,128)(2,1)S(1)} %shard_map.149), channel_id=1, source_target_pairs={{0,2},{1,3},{2,0},{3,1},{4,6},{5,7},{6,4},{7,5},{8,10},{9,11},{10,... | collective-permute-start | bytes 1179656 | tf_op jit(solution)/shard_map/ppermute | solution.py:37
  66.6 1.9 %collective-permute-start.5 = (bf16[128,1536]{1,0:T(8,128)(2,1)S(1)}, bf16[128,1536]{1,0:T(8,128)(2,1)S(1)}, u32[]{:S(2)}, u32[]{:S(2)}) collective-permute-start(bf16[128,1536]{1,0:T(8,128)(2,1)S(1)} %get-tuple-element.43), channel_id=1, source_target_pairs={{0,3},{1,0},{2,1},{3,2},{4,7},{5,4},{6,5},{7,6},{8,11},{9,8},{10,9... | collective-permute-start | bytes 1179656 | tf_op jit(solution)/shard_map/ppermute | solution.py:37
  68.5 5.2 %collective-permute-done.3.refs_1_ = bf16[128,1536]{1,0:T(8,128)(2,1)S(1)} collective-permute-done((bf16[128,1536]{1,0:T(8,128)(2,1)S(1)}, bf16[128,1536]{1,0:T(8,128)(2,1)S(1)}, u32[]{:S(2)}, u32[]{:S(2)}) %collective-permute-start.3) | collective-permute-done | bytes 393248 | tf_op jit(solution)/shard_map/ppermute | solution.py:37
  73.8 3.9 %collective-permute-done.4.refs_2_ = bf16[128,1536]{1,0:T(8,128)(2,1)S(1)} collective-permute-done((bf16[128,1536]{1,0:T(8,128)(2,1)S(1)}, bf16[128,1536]{1,0:T(8,128)(2,1)S(1)}, u32[]{:S(2)}, u32[]{:S(2)}) %collective-permute-start.4) | collective-permute-done | bytes 393248 | tf_op jit(solution)/shard_map/ppermute | solution.py:37
  77.7 7.5 %collective-permute-done.5.refs_3_ = bf16[128,1536]{1,0:T(8,128)(2,1)S(1)} collective-permute-done((bf16[128,1536]{1,0:T(8,128)(2,1)S(1)}, bf16[128,1536]{1,0:T(8,128)(2,1)S(1)}, u32[]{:S(2)}, u32[]{:S(2)}) %collective-permute-start.5) | collective-permute-done | bytes 393248 | tf_op jit(solution)/shard_map/ppermute | solution.py:37
  85.6 2.5 %collective-permute-start.6 = (bf16[128,1664]{1,0:T(8,128)(2,1)S(1)}, bf16[128,1664]{1,0:T(8,128)(2,1)S(1)}, u32[]{:S(2)}, u32[]{:S(2)}) collective-permute-start(bf16[128,1664]{1,0:T(8,128)(2,1)S(1)} %shard_map.150.refs_0_), channel_id=1, source_target_pairs={{0,1},{1,2},{2,3},{3,0},{4,5},{5,6},{6,7},{7,4},{8,9},{9,10},{10,1... | collective-permute-start | bytes 1277960 | tf_op jit(solution)/shard_map/ppermute | solution.py:37
  88.1 4.3 %collective-permute-start.7 = (bf16[128,1664]{1,0:T(8,128)(2,1)S(1)}, bf16[128,1664]{1,0:T(8,128)(2,1)S(1)}, u32[]{:S(2)}, u32[]{:S(2)}) collective-permute-start(bf16[128,1664]{1,0:T(8,128)(2,1)S(1)} %shard_map.150.refs_0_), channel_id=1, source_target_pairs={{0,2},{1,3},{2,0},{3,1},{4,6},{5,7},{6,4},{7,5},{8,10},{9,11},{10,... | collective-permute-start | bytes 1277960 | tf_op jit(solution)/shard_map/ppermute | solution.py:37
  92.4 2.7 %collective-permute-start.8 = (bf16[128,1664]{1,0:T(8,128)(2,1)S(1)}, bf16[128,1664]{1,0:T(8,128)(2,1)S(1)}, u32[]{:S(2)}, u32[]{:S(2)}) collective-permute-start(bf16[128,1664]{1,0:T(8,128)(2,1)S(1)} %shard_map.150.refs_0_), channel_id=1, source_target_pairs={{0,3},{1,0},{2,1},{3,2},{4,7},{5,4},{6,5},{7,6},{8,11},{9,8},{10,9... | collective-permute-start | bytes 1277960 | tf_op jit(solution)/shard_map/ppermute | solution.py:37
  95.2 1.7 %shard_map.158 = bf16[128,128]{1,0:T(8,128)(2,1)} custom-call(bf16[2048,128]{1,0:T(8,128)(2,1)} %bitcast.15.terms_ref), custom_call_target="tpu_custom_call" | custom-call | tf_op jit(solution)/shard_map/pallas_call | solution.py:67
  96.9 3.4 %all-to-all-start.3 = ((bf16[8,16,128]{2,1,0:T(8,128)(2,1)}), bf16[8,16,128]{2,1,0:T(8,128)(2,1)S(1)}, u32[]{:S(2)}, u32[]{:S(2)}) async-start(bf16[8,16,128]{2,1,0:T(8,128)(2,1)} %bitcast.16), calls=%async_computation.3 | async-start | bytes 65536 | tf_op jit(solution)/shard_map/all_to_all | solution.py:44
  100.3 3.9 %collective-permute-done.7.refs_2_ = bf16[128,1664]{1,0:T(8,128)(2,1)S(1)} collective-permute-done((bf16[128,1664]{1,0:T(8,128)(2,1)S(1)}, bf16[128,1664]{1,0:T(8,128)(2,1)S(1)}, u32[]{:S(2)}, u32[]{:S(2)}) %collective-permute-start.7) | collective-permute-done | bytes 426016 | tf_op jit(solution)/shard_map/ppermute | solution.py:37
  104.3 7.5 %collective-permute-done.8.refs_3_ = bf16[128,1664]{1,0:T(8,128)(2,1)S(1)} collective-permute-done((bf16[128,1664]{1,0:T(8,128)(2,1)S(1)}, bf16[128,1664]{1,0:T(8,128)(2,1)S(1)}, u32[]{:S(2)}, u32[]{:S(2)}) %collective-permute-start.8) | collective-permute-done | bytes 426016 | tf_op jit(solution)/shard_map/ppermute | solution.py:37
  111.8 1.8 %shard_map.151 = bf16[1024,384]{1,0:T(8,128)(2,1)} custom-call(s32[1]{0:T(128)} %bitcast.2.col, bf16[128,1664]{1,0:T(8,128)(2,1)S(1)} %shard_map.150.refs_0_, bf16[128,1664]{1,0:T(8,128)(2,1)S(1)} %collective-permute-done.6.refs_1_, bf16[128,1664]{1,0:T(8,128)(2,1)S(1)} %collective-permute-done.7.refs_2_, ...), custom_call_target="tpu_custom_call" | custom-call | tf_op jit(solution)/shard_map/pallas_call | solution.py:67
  113.6 10.5 %all-to-all-start.1 = ((bf16[128,8,384]{2,1,0:T(8,128)(2,1)}), bf16[128,8,384]{2,1,0:T(8,128)(2,1)}, u32[]{:S(2)}, u32[]{:S(2)}) async-start(bf16[128,8,384]{2,1,0:T(8,128)(2,1)} %bitcast.29), calls=%async_computation.1 | async-start | bytes 1572864 | tf_op jit(solution)/shard_map/all_to_all | solution.py:44
  124.7 2.5 %collective-permute-start.9 = (bf16[1536,128]{1,0:T(8,128)(2,1)S(1)}, bf16[1536,128]{1,0:T(8,128)(2,1)S(1)}, u32[]{:S(2)}, u32[]{:S(2)}) collective-permute-start(bf16[1536,128]{1,0:T(8,128)(2,1)S(1)} %get-tuple-element.47), channel_id=1, source_target_pairs={{0,1},{1,2},{2,3},{3,0},{4,5},{5,6},{6,7},{7,4},{8,9},{9,10},{10,1... | collective-permute-start | bytes 1179656 | tf_op jit(solution)/shard_map/ppermute | solution.py:37
  127.7 4.3 %collective-permute-start.10 = (bf16[1536,128]{1,0:T(8,128)(2,1)S(1)}, bf16[1536,128]{1,0:T(8,128)(2,1)S(1)}, u32[]{:S(2)}, u32[]{:S(2)}) collective-permute-start(bf16[1536,128]{1,0:T(8,128)(2,1)S(1)} %shard_map.154), channel_id=1, source_target_pairs={{0,2},{1,3},{2,0},{3,1},{4,6},{5,7},{6,4},{7,5},{8,10},{9,11},{10,... | collective-permute-start | bytes 1179656 | tf_op jit(solution)/shard_map/ppermute | solution.py:37
  132.0 2.7 %collective-permute-start.11 = (bf16[1536,128]{1,0:T(8,128)(2,1)S(1)}, bf16[1536,128]{1,0:T(8,128)(2,1)S(1)}, u32[]{:S(2)}, u32[]{:S(2)}) collective-permute-start(bf16[1536,128]{1,0:T(8,128)(2,1)S(1)} %get-tuple-element.48), channel_id=1, source_target_pairs={{0,3},{1,0},{2,1},{3,2},{4,7},{5,4},{6,5},{7,6},{8,11},{9,8},{10,9... | collective-permute-start | bytes 1179656 | tf_op jit(solution)/shard_map/ppermute | solution.py:37
  136.8 1.8 %collective-permute-done.9.refs_0_ = bf16[1536,128]{1,0:T(8,128)(2,1)S(1)} collective-permute-done((bf16[1536,128]{1,0:T(8,128)(2,1)S(1)}, bf16[1536,128]{1,0:T(8,128)(2,1)S(1)}, u32[]{:S(2)}, u32[]{:S(2)}) %collective-permute-start.9) | collective-permute-done | bytes 393248 | tf_op jit(solution)/shard_map/ppermute | solution.py:37
  138.6 4.5 %collective-permute-done.10.refs_1_ = bf16[1536,128]{1,0:T(8,128)(2,1)S(1)} collective-permute-done((bf16[1536,128]{1,0:T(8,128)(2,1)S(1)}, bf16[1536,128]{1,0:T(8,128)(2,1)S(1)}, u32[]{:S(2)}, u32[]{:S(2)}) %collective-permute-start.10) | collective-permute-done | bytes 393248 | tf_op jit(solution)/shard_map/ppermute | solution.py:37
  143.1 6.7 %collective-permute-done.11.refs_2_ = bf16[1536,128]{1,0:T(8,128)(2,1)S(1)} collective-permute-done((bf16[1536,128]{1,0:T(8,128)(2,1)S(1)}, bf16[1536,128]{1,0:T(8,128)(2,1)S(1)}, u32[]{:S(2)}, u32[]{:S(2)}) %collective-permute-start.11) | collective-permute-done | bytes 393248 | tf_op jit(solution)/shard_map/ppermute | solution.py:37
  151.0 2.5 %shard_map.152 = (bf16[128,512]{1,0:T(8,128)(2,1)}, f32[2,128]{1,0:T(2,128)}) custom-call(f32[2,128]{1,0:T(2,128)S(1)} %get-tuple-element.32.inverse_ref, bf16[512,128]{1,0:T(8,128)(2,1)S(1)} %get-tuple-element.33.one_ref, bf16[512,128]{1,0:T(8,128)(2,1)S(1)} %get-tuple-element.34.two_ref, bf16[1024,384]{1,0:T(8,128)(2,1)} %bitcast.9.back_ref), custom_call_target="tpu_custom_call" | custom-call | tf_op jit(solution)/shard_map/pallas_call | solution.py:67
  (36 shorter events, 6.4 us)
Async XLA Ops:
  3.4 18.0 %copy-start.2 = (bf16[1,2048,128]{2,1,0:T(8,128)(2,1)S(1)}, bf16[1,2048,128]{2,1,0:T(8,128)(2,1)}, u32[]{:S(2)}) copy-start(bf16[1,2048,128]{2,1,0:T(8,128)(2,1)} %param.13) | copy-start | bytes 1572868
  3.4 18.0 %copy-start.3 = (bf16[1,2048,128]{2,1,0:T(8,128)(2,1)S(1)}, bf16[1,2048,128]{2,1,0:T(8,128)(2,1)}, u32[]{:S(2)}) copy-start(bf16[1,2048,128]{2,1,0:T(8,128)(2,1)} %param.14) | copy-start | bytes 1572868
  3.4 18.0 %copy-start.4 = (bf16[1,128,2048]{2,1,0:T(8,128)(2,1)S(1)}, bf16[1,128,2048]{2,1,0:T(8,128)(2,1)}, u32[]{:S(2)}) copy-start(bf16[1,128,2048]{2,1,0:T(8,128)(2,1)} %param.15) | copy-start | bytes 1572868
  3.5 48.2 %all-to-all-start = ((bf16[128,8,512]{2,1,0:T(8,128)(2,1)}), bf16[128,8,512]{2,1,0:T(8,128)(2,1)S(1)}, u32[]{:S(2)}, u32[]{:S(2)}) async-start(bf16[128,8,512]{2,1,0:T(8,128)(2,1)} %bitcast.28), calls=%async_computation | async-start | bytes 2097152 | tf_op jit(solution)/shard_map/all_to_all | solution.py:44
  21.4 10.5 %copy-start.1 = (bf16[128,2048]{1,0:T(8,128)(2,1)S(1)}, bf16[128,2048]{1,0:T(8,128)(2,1)}, u32[]{:S(2)}) copy-start(bf16[128,2048]{1,0:T(8,128)(2,1)} %cot_ref.3) | copy-start | bytes 1572868
  21.5 10.5 %copy-start.5 = (bf16[2048,128]{1,0:T(8,128)(2,1)S(1)}, bf16[2048,128]{1,0:T(8,128)(2,1)}, u32[]{:S(2)}) copy-start(bf16[2048,128]{1,0:T(8,128)(2,1)} %down_ref.1) | copy-start | bytes 1572868
  21.5 10.5 %copy-start.7 = (bf16[128,128]{1,0:T(8,128)(2,1)S(1)}, bf16[128,128]{1,0:T(8,128)(2,1)}, u32[]{:S(2)}) copy-start(bf16[128,128]{1,0:T(8,128)(2,1)} %hid_ref.1) | copy-start | bytes 98308
  23.3 32.6 %collective-permute-start = (bf16[1536,128]{1,0:T(8,128)(2,1)}, bf16[1536,128]{1,0:T(8,128)(2,1)S(1)}, u32[]{:S(2)}, u32[]{:S(2)}) collective-permute-start(bf16[1536,128]{1,0:T(8,128)(2,1)} %get-tuple-element.36), channel_id=1, source_target_pairs={{0,1},{1,2},{2,3},{3,0},{4,5},{5,6},{6,7},{7,4},{8,9},{9,10},{10,1... | collective-permute-start | bytes 1179656 | tf_op jit(solution)/shard_map/ppermute | solution.py:37
  25.7 30.2 %collective-permute-start.1 = (bf16[1536,128]{1,0:T(8,128)(2,1)}, bf16[1536,128]{1,0:T(8,128)(2,1)S(1)}, u32[]{:S(2)}, u32[]{:S(2)}) collective-permute-start(bf16[1536,128]{1,0:T(8,128)(2,1)} %get-tuple-element.37), channel_id=1, source_target_pairs={{0,2},{1,3},{2,0},{3,1},{4,6},{5,7},{6,4},{7,5},{8,10},{9,11},{10,... | collective-permute-start | bytes 1179656 | tf_op jit(solution)/shard_map/ppermute | solution.py:37
  30.0 25.9 %collective-permute-start.2 = (bf16[1536,128]{1,0:T(8,128)(2,1)}, bf16[1536,128]{1,0:T(8,128)(2,1)S(1)}, u32[]{:S(2)}, u32[]{:S(2)}) collective-permute-start(bf16[1536,128]{1,0:T(8,128)(2,1)} %get-tuple-element.38), channel_id=1, source_target_pairs={{0,3},{1,0},{2,1},{3,2},{4,7},{5,4},{6,5},{7,6},{8,11},{9,8},{10,9... | collective-permute-start | bytes 1179656 | tf_op jit(solution)/shard_map/ppermute | solution.py:37
  51.6 43.6 %all-to-all-start.2 = ((bf16[16,128,128]{2,1,0:T(8,128)(2,1)}), bf16[16,128,128]{2,1,0:T(8,128)(2,1)}, u32[]{:S(2)}, u32[]{:S(2)}) async-start(bf16[16,128,128]{2,1,0:T(8,128)(2,1)} %bitcast.14), calls=%async_computation.2 | async-start | bytes 1048576 | tf_op jit(solution)/shard_map/all_to_all | solution.py:44
  59.2 26.0 %copy-start.6 = (bf16[128,1536]{1,0:T(8,128)(2,1)S(1)}, bf16[128,1536]{1,0:T(8,128)(2,1)}, u32[]{:S(2)}) copy-start(bf16[128,1536]{1,0:T(8,128)(2,1)} %get-tuple-element.41.refs_0_) | copy-start | bytes 1179652
  59.9 13.9 %collective-permute-start.3 = (bf16[128,1536]{1,0:T(8,128)(2,1)S(1)}, bf16[128,1536]{1,0:T(8,128)(2,1)S(1)}, u32[]{:S(2)}, u32[]{:S(2)}) collective-permute-start(bf16[128,1536]{1,0:T(8,128)(2,1)S(1)} %get-tuple-element.42), channel_id=1, source_target_pairs={{0,1},{1,2},{2,3},{3,0},{4,5},{5,6},{6,7},{7,4},{8,9},{9,10},{10,1... | collective-permute-start | bytes 1179656 | tf_op jit(solution)/shard_map/ppermute | solution.py:37
  62.3 15.4 %collective-permute-start.4 = (bf16[128,1536]{1,0:T(8,128)(2,1)S(1)}, bf16[128,1536]{1,0:T(8,128)(2,1)S(1)}, u32[]{:S(2)}, u32[]{:S(2)}) collective-permute-start(bf16[128,1536]{1,0:T(8,128)(2,1)S(1)} %shard_map.149), channel_id=1, source_target_pairs={{0,2},{1,3},{2,0},{3,1},{4,6},{5,7},{6,4},{7,5},{8,10},{9,11},{10,... | collective-permute-start | bytes 1179656 | tf_op jit(solution)/shard_map/ppermute | solution.py:37
  66.6 18.6 %collective-permute-start.5 = (bf16[128,1536]{1,0:T(8,128)(2,1)S(1)}, bf16[128,1536]{1,0:T(8,128)(2,1)S(1)}, u32[]{:S(2)}, u32[]{:S(2)}) collective-permute-start(bf16[128,1536]{1,0:T(8,128)(2,1)S(1)} %get-tuple-element.43), channel_id=1, source_target_pairs={{0,3},{1,0},{2,1},{3,2},{4,7},{5,4},{6,5},{7,6},{8,11},{9,8},{10,9... | collective-permute-start | bytes 1179656 | tf_op jit(solution)/shard_map/ppermute | solution.py:37
  85.6 14.7 %collective-permute-start.6 = (bf16[128,1664]{1,0:T(8,128)(2,1)S(1)}, bf16[128,1664]{1,0:T(8,128)(2,1)S(1)}, u32[]{:S(2)}, u32[]{:S(2)}) collective-permute-start(bf16[128,1664]{1,0:T(8,128)(2,1)S(1)} %shard_map.150.refs_0_), channel_id=1, source_target_pairs={{0,1},{1,2},{2,3},{3,0},{4,5},{5,6},{6,7},{7,4},{8,9},{9,10},{10,1... | collective-permute-start | bytes 1277960 | tf_op jit(solution)/shard_map/ppermute | solution.py:37
  88.1 16.1 %collective-permute-start.7 = (bf16[128,1664]{1,0:T(8,128)(2,1)S(1)}, bf16[128,1664]{1,0:T(8,128)(2,1)S(1)}, u32[]{:S(2)}, u32[]{:S(2)}) collective-permute-start(bf16[128,1664]{1,0:T(8,128)(2,1)S(1)} %shard_map.150.refs_0_), channel_id=1, source_target_pairs={{0,2},{1,3},{2,0},{3,1},{4,6},{5,7},{6,4},{7,5},{8,10},{9,11},{10,... | collective-permute-start | bytes 1277960 | tf_op jit(solution)/shard_map/ppermute | solution.py:37
  92.4 19.3 %collective-permute-start.8 = (bf16[128,1664]{1,0:T(8,128)(2,1)S(1)}, bf16[128,1664]{1,0:T(8,128)(2,1)S(1)}, u32[]{:S(2)}, u32[]{:S(2)}) collective-permute-start(bf16[128,1664]{1,0:T(8,128)(2,1)S(1)} %shard_map.150.refs_0_), channel_id=1, source_target_pairs={{0,3},{1,0},{2,1},{3,2},{4,7},{5,4},{6,5},{7,6},{8,11},{9,8},{10,9... | collective-permute-start | bytes 1277960 | tf_op jit(solution)/shard_map/ppermute | solution.py:37
  96.9 16.7 %all-to-all-start.3 = ((bf16[8,16,128]{2,1,0:T(8,128)(2,1)}), bf16[8,16,128]{2,1,0:T(8,128)(2,1)S(1)}, u32[]{:S(2)}, u32[]{:S(2)}) async-start(bf16[8,16,128]{2,1,0:T(8,128)(2,1)} %bitcast.16), calls=%async_computation.3 | async-start | bytes 65536 | tf_op jit(solution)/shard_map/all_to_all | solution.py:44
  113.6 10.5 %copy-start = (bf16[512,1024]{1,0:T(8,128)(2,1)S(1)}, bf16[512,1024]{1,0:T(8,128)(2,1)}, u32[]{:S(2)}) copy-start(bf16[512,1024]{1,0:T(8,128)(2,1)} %get-tuple-element.46.xg_ref) | copy-start | bytes 3145732
  113.6 37.4 %all-to-all-start.1 = ((bf16[128,8,384]{2,1,0:T(8,128)(2,1)}), bf16[128,8,384]{2,1,0:T(8,128)(2,1)}, u32[]{:S(2)}, u32[]{:S(2)}) async-start(bf16[128,8,384]{2,1,0:T(8,128)(2,1)} %bitcast.29), calls=%async_computation.1 | async-start | bytes 1572864 | tf_op jit(solution)/shard_map/all_to_all | solution.py:44
  124.7 13.9 %collective-permute-start.9 = (bf16[1536,128]{1,0:T(8,128)(2,1)S(1)}, bf16[1536,128]{1,0:T(8,128)(2,1)S(1)}, u32[]{:S(2)}, u32[]{:S(2)}) collective-permute-start(bf16[1536,128]{1,0:T(8,128)(2,1)S(1)} %get-tuple-element.47), channel_id=1, source_target_pairs={{0,1},{1,2},{2,3},{3,0},{4,5},{5,6},{6,7},{7,4},{8,9},{9,10},{10,1... | collective-permute-start | bytes 1179656 | tf_op jit(solution)/shard_map/ppermute | solution.py:37
  127.2 7.5 %copy-start.9 = (f32[128,2]{0,1:T(2,128)S(1)}, f32[128,2]{0,1:T(2,128)}, u32[]{:S(2)}) copy-start(f32[128,2]{0,1:T(2,128)} %param.11) | copy-start | bytes 3076
  127.7 7.1 %copy-start.8 = (s32[128,2]{0,1:T(2,128)S(1)}, s32[128,2]{0,1:T(2,128)}, u32[]{:S(2)}) copy-start(s32[128,2]{0,1:T(2,128)} %param.12) | copy-start | bytes 3076
  127.7 15.4 %collective-permute-start.10 = (bf16[1536,128]{1,0:T(8,128)(2,1)S(1)}, bf16[1536,128]{1,0:T(8,128)(2,1)S(1)}, u32[]{:S(2)}, u32[]{:S(2)}) collective-permute-start(bf16[1536,128]{1,0:T(8,128)(2,1)S(1)} %shard_map.154), channel_id=1, source_target_pairs={{0,2},{1,3},{2,0},{3,1},{4,6},{5,7},{6,4},{7,5},{8,10},{9,11},{10,... | collective-permute-start | bytes 1179656 | tf_op jit(solution)/shard_map/ppermute | solution.py:37
  132.0 17.8 %collective-permute-start.11 = (bf16[1536,128]{1,0:T(8,128)(2,1)S(1)}, bf16[1536,128]{1,0:T(8,128)(2,1)S(1)}, u32[]{:S(2)}, u32[]{:S(2)}) collective-permute-start(bf16[1536,128]{1,0:T(8,128)(2,1)S(1)} %get-tuple-element.48), channel_id=1, source_target_pairs={{0,3},{1,0},{2,1},{3,2},{4,7},{5,4},{6,5},{7,6},{8,11},{9,8},{10,9... | collective-permute-start | bytes 1179656 | tf_op jit(solution)/shard_map/ppermute | solution.py:37

commit v4 on v3

--- a/solution.py
+++ b/solution.py
@@ -20,6 +20,7 @@
 LIMIT = pltpu.CompilerParams(vmem_limit_bytes=12 * 2**20)
 CAP = 4
 LANES = 128
+PAD = 16
 FAR = 2
 NEAR = (1, 3)
 GROUP = 16
@@ -85,10 +86,10 @@
     return jnp.where(col == h * (rows // 2) + s * CAP + r, 1.0, 0.0).astype(BF16)
 
 
-def chosen(routes_ref, slots):
+def chosen(routes_ref, slots, turns=1, start=0):
     count = routes_ref.shape[1]
-    row = lax.broadcasted_iota(jnp.int32, (slots, count), 0)
-    expert = row // CAP
+    row = start + lax.broadcasted_iota(jnp.int32, (turns * slots, count), 0)
+    expert = row // (turns * CAP)
     first = expert == routes_ref[0:1, :]
     second = expert == routes_ref[1:2, :]
     named = jnp.where(first | second, 1.0, 0.0)
@@ -96,48 +97,52 @@
     later = lax.broadcasted_iota(jnp.int32, (count, count), 1)
     before = jnp.where(earlier < later, 1.0, 0.0).astype(BF16)
     rank = mm(named.astype(BF16), before)
-    place = (row - expert * CAP).astype(F32)
+    place = (row % CAP).astype(F32)
     hit = jnp.where(rank == place, named, 0.0)
     return hit, jnp.where(first, hit, 0.0), jnp.where(second, hit, 0.0)
 
 
 def dispatch_kernel(
-    col, routes_ref, weights_ref, tok_ref, cot_ref, sent_ref, routes, weights, tok, cot, sent, sems
+    col, routes_ref, weights_ref, tok_ref, cot_ref, sent_ref, routes, weights, both, sent, sems
 ):
     slots = sent_ref.shape[0] // 2
-    place = span(col[0], tok.shape[1])
+    rows, quarter = tok_ref.shape[0], both.shape[1]
+    place = span(col[0], quarter)
     copies = [
         pltpu.make_async_copy(src, dst, sems.at[k])
         for k, (src, dst) in enumerate(
             [
                 (routes_ref, routes),
                 (weights_ref, weights),
-                (tok_ref.at[:, place], tok),
-                (cot_ref.at[:, place], cot),
+                (tok_ref.at[:, place], both.at[:rows, :]),
+                (cot_ref.at[:, place], both.at[rows:, :]),
             ]
         )
     ]
     for copy in copies:
         copy.start()
-    order = weave()
-    copies[0].wait()
-    hit, one, two = chosen(routes, slots)
-    pick = hit.astype(BF16)
-    copies[1].wait()
-    scale = weights[...].astype(BF16).astype(F32)
-    weight = jnp.sum(one * scale[0:1, :] + two * scale[1:2, :], axis=1, keepdims=True)
-    copies[2].wait()
-    x = mm(pick, tok[...]).astype(BF16)
-    copies[3].wait()
-    g = (weight * mm(pick, cot[...])).astype(BF16)
-    half = order.shape[0] // 2
+    half = slots // 2
     leaving = []
-    for b in range(slots // half):
-        both = jnp.concatenate([x[b * half : (b + 1) * half], g[b * half : (b + 1) * half]], axis=0)
-        rows = slice(2 * b * half, 2 * (b + 1) * half)
-        sent[rows, :] = mm(order, both).astype(BF16)
+    for b in range(2 * slots // half):
+        if b == 0:
+            copies[0].wait()
+        hit, one, two = chosen(routes, half // 2, 2, b * half)
+        kind = (lax.broadcasted_iota(jnp.int32, hit.shape, 0) // CAP) % 2
+        pick = jnp.concatenate(
+            [jnp.where(kind == 0, hit, 0.0), jnp.where(kind == 1, hit, 0.0)], axis=1
+        )
+        if b == 0:
+            copies[1].wait()
+        scale = weights[...].astype(BF16).astype(F32)
+        weight = jnp.sum(one * scale[0:1, :] + two * scale[1:2, :], axis=1, keepdims=True)
+        weight = jnp.where(kind[:, 0:1] == 0, 1.0, weight)
+        if b == 0:
+            copies[2].wait()
+            copies[3].wait()
+        part = slice(b * half, (b + 1) * half)
+        sent[part, :] = (weight * mm(pick.astype(BF16), both[...])).astype(BF16)
         leaving.append(
-            pltpu.make_async_copy(sent.at[rows, :], sent_ref.at[rows, :], sems.at[4 + b])
+            pltpu.make_async_copy(sent.at[part, :], sent_ref.at[part, :], sems.at[4 + b])
         )
         leaving[-1].start()
     for copy in leaving:
@@ -161,7 +166,10 @@
         terms_ref[:, k] = terms[k]
 
 
-def fold_kernel(terms_ref, out_ref):
+def fold_kernel(terms_hbm, out_ref, terms_ref, sem):
+    copy = pltpu.make_async_copy(terms_hbm, terms_ref, sem)
+    copy.start()
+    copy.wait()
     terms = terms_ref[...].astype(F32)
     out_ref[...] = jnp.sum(terms.reshape(-1, *out_ref.shape), axis=0).astype(BF16)
 
@@ -233,8 +241,10 @@
     out_ref[:, width:] = mm(g, down_ref[...], LAST).astype(BF16)
 
 
-def near_kernel(col, got_ref, both_ref, down_ref, xg_out, own_out, *refs):
+def near_kernel(col, got_ref, both_ref, down_ref, xg_out, own_out, both_out, *refs):
     *outs, xg_ref, own_ref, sems = refs
+    both_copy = pltpu.make_async_copy(both_ref, both_out, sems.at[2])
+    both_copy.start()
     rows = own_ref.shape[0]
     parts = got_ref.shape[0] // (2 * rows)
     width = both_ref.shape[1]
@@ -258,6 +268,12 @@
             own_copy.start()
     xg_copy.wait()
     own_copy.wait()
+    both_copy.wait()
+
+
+def diagonal(size):
+    row = lax.broadcasted_iota(jnp.int32, (size, size), 0)
+    return row == lax.broadcasted_iota(jnp.int32, (size, size), 1)
 
 
 def middle_kernel(*refs):
@@ -273,19 +289,36 @@
     sigma = jax.nn.sigmoid(gate)
     active = gate * sigma
     hid = (active * upper).astype(BF16)
-    grads_ref[:, :hidden] = (backed * upper * sigma * (1.0 + gate * (1.0 - sigma))).astype(BF16)
-    grads_ref[:, hidden : 2 * hidden] = (backed * active).astype(BF16)
-    grads_ref[:, 2 * hidden : width] = hid
+    d_gate = (backed * upper * sigma * (1.0 + gate * (1.0 - sigma))).astype(BF16)
+    d_up = (backed * active).astype(BF16)
+    blocks = hidden // LANES
+    for k, value in enumerate([d_gate, d_up, hid]):
+        for c in range(blocks):
+            row = (k * blocks + c) * rows
+            grads_ref[row : row + rows, :] = value[:, c * LANES : (c + 1) * LANES]
     share = jnp.sum(hid.astype(F32) * backed, axis=1, keepdims=True)
-    grads_ref[:, width:] = jnp.broadcast_to(share, (rows, LANES)).astype(BF16)
+    share = jnp.sum(jnp.where(diagonal(rows), share, 0.0), axis=0, keepdims=True)
+    grads_ref[3 * blocks * rows :, :] = jnp.broadcast_to(share, (PAD, LANES)).astype(BF16)
+
+
+def ready_kernel(both_hbm, both_ref, sem):
+    copy = pltpu.make_async_copy(both_hbm, both_ref, sem)
+    copy.start()
+    copy.wait()
 
 
 def input_kernel(col, *refs):
     *grads, both_ref, back_out, out_ref, sems = refs
     parts = len(grads)
-    rows = grads[0].shape[0]
-    width = both_ref.shape[1]
-    whole = jnp.concatenate([ref[:, :width] for ref in grads], axis=0)
+    rows = out_ref.shape[0] // (2 * parts)
+    blocks = both_ref.shape[1] // LANES
+    whole = jnp.concatenate(
+        [
+            jnp.concatenate([ref[c * rows : (c + 1) * rows, :] for c in range(blocks)], axis=1)
+            for ref in grads
+        ],
+        axis=0,
+    )
     out = mm(whole, both_ref[...], LAST).astype(BF16)
     order = weave()
     half = out.shape[1] // 2
@@ -295,7 +328,9 @@
         both = jnp.concatenate([own[:, :half], own[:, half:]], axis=0)
         place = slice(2 * k * rows, 2 * (k + 1) * rows)
         out_ref[place, :half] = mm(order, both).astype(BF16)
-        share = ref[:, ref.shape[1] - LANES :]
+        share = ref[ref.shape[0] - PAD :, :].astype(F32)[0:1]
+        share = jnp.sum(jnp.where(diagonal(rows), share, 0.0), axis=1, keepdims=True)
+        share = jnp.broadcast_to(share, (rows, LANES)).astype(BF16)
         out_ref[place, half:] = mm(order[:, :rows], share).astype(BF16)
         to = back_out.at[span(at(col, -k, parts), 2 * rows), :]
         copies.append(pltpu.make_async_copy(out_ref.at[place, :], to, sems.at[k]))
@@ -306,17 +341,17 @@
 
 def outer_terms(col, steps, xg_ref, grads):
     parts = len(grads)
-    rows = grads[0].shape[0]
-    block = (grads[0].shape[1] - LANES) // (3 * parts)
+    rows = xg_ref.shape[0] // parts
+    block = LANES
     quarter = xg_ref.shape[1] // 2
     order = [span(at(col, -k, parts), rows) for k in range(parts)]
     x = jnp.concatenate([xg_ref[place, :quarter] for place in order], axis=0)
     g = jnp.concatenate([xg_ref[place, quarter:] for place in order], axis=0)
 
     def units(kinds):
-        places = [span(at(col, k, parts) + kind * parts, block) for k in steps for kind in kinds]
+        places = [span(at(col, k, parts) + kind * parts, rows) for k in steps for kind in kinds]
         return jnp.concatenate(
-            [jnp.concatenate([ref[:, place] for place in places], axis=1) for ref in grads], axis=0
+            [jnp.concatenate([ref[place, :] for place in places], axis=1) for ref in grads], axis=0
         )
 
     both = mm(x, units((0, 1)), ROWS).astype(BF16)
@@ -360,15 +395,15 @@
         copy.wait()
 
 
-def finish_kernel(col, *refs):
+def finish_kernel(col, *refs, steps):
     *refs, sems = refs
-    parts = len(refs) - 5
-    got, (gate_ref, up_ref, down_ref) = refs[: parts - 1], refs[parts + 2 :]
+    got, (gate_ref, up_ref, down_ref) = refs[: len(steps)], refs[-3:]
     block = gate_ref.shape[1]
-    quarter = gate_ref.shape[0] // parts
+    quarter = got[0].shape[0] // 3
+    parts = gate_ref.shape[0] // quarter
     copies = []
-    for k, ref in enumerate(got):
-        index = at(col, -k - 1, parts)
+    for k, ref in zip(steps, got):
+        index = at(col, -k, parts)
         place = span(index, quarter)
         pairs = [
             (ref.at[:quarter, :], gate_ref.at[place, :]),
@@ -445,8 +480,7 @@
         scratch=[
             pltpu.VMEM(routes_t.shape, jnp.int32),
             pltpu.VMEM(weights_t.shape, F32),
-            pltpu.VMEM((rows, quarter), BF16),
-            pltpu.VMEM((rows, quarter), BF16),
+            pltpu.VMEM((2 * rows, quarter), BF16),
             pltpu.VMEM((2 * slots, quarter), BF16),
             pltpu.SemaphoreType.DMA((4 + tp,)),
         ],
@@ -475,31 +509,39 @@
     )
 
     far = local(far_kernel, half(some, 3 * hidden), col, got, both, down, spaces="s")
-    xg, own, *near = local(
+    xg, own, later, *near = local(
         near_kernel,
-        [half(slots, 2 * quarter)] + [half(some, 3 * hidden)] * (1 + len(NEAR)),
+        [half(slots, 2 * quarter), half(some, 3 * hidden), half(quarter, 2 * hidden)]
+        + [half(some, 3 * hidden)] * len(NEAR),
         col,
         got,
         both,
         down,
         spaces="s",
-        outs="hh",
+        outs="hhh",
         scratch=[
             pltpu.VMEM((slots, 2 * quarter), BF16),
             pltpu.VMEM((some, 3 * hidden), BF16),
-            pltpu.SemaphoreType.DMA((2,)),
+            pltpu.SemaphoreType.DMA((3,)),
         ],
     )
     part = [own, *around([near[0], far, near[1]])]
-    grads = local(middle_kernel, half(some, 3 * hidden + LANES), *part)
+    grads = local(middle_kernel, half(3 * hidden // LANES * some + PAD, LANES), *part)
     grads = [grads, *around(grads)]
 
+    ready = local(
+        ready_kernel,
+        half(quarter, 2 * hidden),
+        later,
+        spaces="h",
+        scratch=[pltpu.SemaphoreType.DMA],
+    )
     back = local(
         input_kernel,
         half(2 * slots, quarter // 2 + LANES),
         col,
         *grads,
-        both,
+        ready,
         spaces="s",
         outs="h",
         scratch=[
@@ -552,17 +594,19 @@
             pltpu.SemaphoreType.DMA((3,)),
         ],
     )
-    gate_grad, up_grad, down_grad = local(
-        finish_kernel,
-        whole,
-        col,
-        *outer,
-        *own,
-        spaces="s" + "v" * (tp - 1) + "hhh",
-        outs="hhh",
-        scratch=[pltpu.SemaphoreType.DMA(((tp - 1) * (2 + tp),))],
-        alias={tp: 0, tp + 1: 1, tp + 2: 2},
-    )
+    for steps in ((FAR,), NEAR):
+        own = local(
+            functools.partial(finish_kernel, steps=steps),
+            whole,
+            col,
+            *[outer[k - 1] for k in steps],
+            *own,
+            spaces="s" + "v" * len(steps) + "hhh",
+            outs="hhh",
+            scratch=[pltpu.SemaphoreType.DMA((len(steps) * (2 + tp),))],
+            alias={len(steps) + 1 + k: k for k in range(3)},
+        )
+    gate_grad, up_grad, down_grad = own
 
     inner = ep // lax.axis_size("z")
     group = feat // ep
@@ -574,11 +618,15 @@
         shared_down,
     )
     shared = over(shared.reshape(feat, block), ("y", "core"))
-    shared = local(fold_kernel, half(feat // inner, block), shared)
+    shared = local(
+        fold_kernel,
+        half(feat // inner, block),
+        shared,
+        spaces="h",
+        scratch=[pltpu.VMEM((feat, block), BF16), pltpu.SemaphoreType.DMA],
+    )
     shared = over(shared, "z")
-    shared_grad = local(
-        total_kernel, jax.ShapeDtypeStruct((feat // ep, block), F32), shared
-    )
+    shared_grad = local(total_kernel, jax.ShapeDtypeStruct((feat // ep, block), F32), shared)
     return (
         tokens_grad,
         weights_grad,

time: 156 us -> 153 us (0.981)
  waiting for transfers between devices: 59.6 us -> 53.4 us
  local copies, waits for them, and re-layouts: 0.06 us -> 2.01 us
    ppermute x12, waiting for transfers between devices: 41.2 us -> 33.9 us  [around(): lax.ppermute(part, 'tp', [(i, (i + k + 1) % size) for i in range(size)])]
    unnamed x20 -> x32, local copies, waits for them, and re-layouts: 0.06 us -> 2.01 us
    pallas_call x16 -> x18, Pallas kernels: 20.2 us -> 20.9 us  [local(): pl.pallas_call(kernel, in_specs=[spec[k] for k in spaces], out_specs=[spe...]
  transfers between devices with their start and end apart: 16 -> 16, of which waited for: 9 -> 10; matrix products, arithmetic and copies ran while one was open for 0% -> 0% of each run, Pallas kernels for 10% -> 11%
where the time goes in v4:
time: 153 us; the launch traced here: 150 us
  starting transfers between devices  72.5 us (47%)
  waiting for transfers between devices  53.4 us (35%)
  Pallas kernels  20.9 us (14%)
  local copies, waits for them, and re-layouts  2.01 us (1%)
    ppermute x12, starting transfers between devices, around(): lax.ppermute(part, 'tp', [(i, (i + k + 1) % size) for i in range(size)])  37 us
    all_to_all x4, starting transfers between devices, over(): lax.all_to_all(rows, axes, split_axis=0, concat_axis=0, tiled=True)  35.5 us
    ppermute x12, waiting for transfers between devices, around(): lax.ppermute(part, 'tp', [(i, (i + k + 1) % size) for i in range(size)])  33.9 us
    pallas_call x18, Pallas kernels, local(): pl.pallas_call(kernel, in_specs=[spec[k] for k in spaces], out_specs=[spe...  20.9 us
    all_to_all x4, waiting for transfers between devices, over(): lax.all_to_all(rows, axes, split_axis=0, concat_axis=0, tiled=True)  19.5 us
  transfers between devices with their start and end apart: 16, of which 10 were waited for; matrix products, arithmetic and copies ran while one was open for 0% of the time, Pallas kernels for 11%

profile of v4, /device:TPU:6, one launch (start us, length us, event | category | flops | bytes accessed | tf_op | source)
XLA Modules:
  0.0 149.9 jit_solution(17215883043583890301)
XLA Ops:
  0.6 2.7 %shard_map.145 = bf16[1024,512]{1,0:T(8,128)(2,1)} custom-call(s32[1]{0:T(128)} %bitcast.2.col, s32[2,128]{1,0:T(2,128)} %bitcast.25, f32[2,128]{1,0:T(2,128)} %bitcast.27, bf16[128,2048]{1,0:T(8,128)(2,1)} %tok_ref.1, bf16[128,2048]{1,0:T(8,128)(2,1)} %cot_ref.3), custom_call_target="tpu_custom_call" | custom-call | tf_op jit(solution)/shard_map/pallas_call | solution.py:68
  3.4 18.0 %all-to-all-start = ((bf16[128,8,512]{2,1,0:T(8,128)(2,1)}), bf16[128,8,512]{2,1,0:T(8,128)(2,1)S(1)}, u32[]{:S(2)}, u32[]{:S(2)}) async-start(bf16[128,8,512]{2,1,0:T(8,128)(2,1)} %bitcast.29), calls=%async_computation | async-start | bytes 2097152 | tf_op jit(solution)/shard_map/all_to_all | solution.py:45
  21.4 1.5 %shard_map.146 = (bf16[1536,128]{1,0:T(8,128)(2,1)}, bf16[1536,128]{1,0:T(8,128)(2,1)}, bf16[1536,128]{1,0:T(8,128)(2,1)S(1)}, bf16[1536,128]{1,0:T(8,128)(2,1)S(1)}) custom-call(s32[1]{0:T(128)} %bitcast.2.col, bf16[2048,128]{1,0:T(8,128)(2,1)S(1)} %bitcast.21, bf16[2048,128]{1,0:T(8,128)(2,1)S(1)} %bitcast.22, bf16[128,2048]{1,0:T(8,128)(2,1)S(1)} %bitcast.23), custom_call_target="tpu_custom_call" | custom-call | tf_op jit(solution)/shard_map/pallas_call | solution.py:68
  22.9 2.4 %collective-permute-start = (bf16[1536,128]{1,0:T(8,128)(2,1)}, bf16[1536,128]{1,0:T(8,128)(2,1)S(1)}, u32[]{:S(2)}, u32[]{:S(2)}) collective-permute-start(bf16[1536,128]{1,0:T(8,128)(2,1)} %get-tuple-element.40), channel_id=1, source_target_pairs={{0,1},{1,2},{2,3},{3,0},{4,5},{5,6},{6,7},{7,4},{8,9},{9,10},{10,1... | collective-permute-start | bytes 1179656 | tf_op jit(solution)/shard_map/ppermute | solution.py:38
  25.3 4.3 %collective-permute-start.1 = (bf16[1536,128]{1,0:T(8,128)(2,1)S(1)}, bf16[1536,128]{1,0:T(8,128)(2,1)S(1)}, u32[]{:S(2)}, u32[]{:S(2)}) collective-permute-start(bf16[1536,128]{1,0:T(8,128)(2,1)S(1)} %get-tuple-element.41), channel_id=1, source_target_pairs={{0,2},{1,3},{2,0},{3,1},{4,6},{5,7},{6,4},{7,5},{8,10},{9,11},{10,... | collective-permute-start | bytes 1179656 | tf_op jit(solution)/shard_map/ppermute | solution.py:38
  29.7 1.9 %collective-permute-start.2 = (bf16[1536,128]{1,0:T(8,128)(2,1)S(1)}, bf16[1536,128]{1,0:T(8,128)(2,1)S(1)}, u32[]{:S(2)}, u32[]{:S(2)}) collective-permute-start(bf16[1536,128]{1,0:T(8,128)(2,1)S(1)} %get-tuple-element.42), channel_id=1, source_target_pairs={{0,3},{1,0},{2,1},{3,2},{4,7},{5,4},{6,5},{7,6},{8,11},{9,8},{10,9... | collective-permute-start | bytes 1179656 | tf_op jit(solution)/shard_map/ppermute | solution.py:38
  32.8 18.7 %all-to-all-done = bf16[128,8,512]{2,1,0:T(8,128)(2,1)S(1)} async-done(((bf16[128,8,512]{2,1,0:T(8,128)(2,1)}), bf16[128,8,512]{2,1,0:T(8,128)(2,1)S(1)}, u32[]{:S(2)}, u32[]{:S(2)}) %all-to-all-start) | async-done | bytes 1048608 | tf_op jit(solution)/shard_map/all_to_all | solution.py:45
  51.5 4.3 %all-to-all-start.2 = ((bf16[16,128,128]{2,1,0:T(8,128)(2,1)}), bf16[16,128,128]{2,1,0:T(8,128)(2,1)}, u32[]{:S(2)}, u32[]{:S(2)}) async-start(bf16[16,128,128]{2,1,0:T(8,128)(2,1)} %bitcast.14), calls=%async_computation.2 | async-start | bytes 1048576 | tf_op jit(solution)/shard_map/all_to_all | solution.py:45
  56.9 2.5 %shard_map.148 = (bf16[512,1024]{1,0:T(8,128)(2,1)}, bf16[128,1536]{1,0:T(8,128)(2,1)}, bf16[512,1024]{1,0:T(8,128)(2,1)}, bf16[128,1536]{1,0:T(8,128)(2,1)S(1)}, bf16[128,1536]{1,0:T(8,128)(2,1)S(1)}) custom-call(s32[1]{0:T(128)} %bitcast.2.col, bf16[1024,512]{1,0:T(8,128)(2,1)S(1)} %bitcast.18, bf16[512,1024]{1,0:T(8,128)(2,1)S(1)} %get-tuple-element.43.both_ref, ...), custom_call_target="tpu_custom_call" | custom-call | tf_op jit(solution)/shard_map/pallas_call | solution.py:68
  60.1 2.4 %collective-permute-start.3 = (bf16[128,1536]{1,0:T(8,128)(2,1)S(1)}, bf16[128,1536]{1,0:T(8,128)(2,1)S(1)}, u32[]{:S(2)}, u32[]{:S(2)}) collective-permute-start(bf16[128,1536]{1,0:T(8,128)(2,1)S(1)} %get-tuple-element.46), channel_id=1, source_target_pairs={{0,1},{1,2},{2,3},{3,0},{4,5},{5,6},{6,7},{7,4},{8,9},{9,10},{10,1... | collective-permute-start | bytes 1179656 | tf_op jit(solution)/shard_map/ppermute | solution.py:38
  62.5 4.3 %collective-permute-start.4 = (bf16[128,1536]{1,0:T(8,128)(2,1)S(1)}, bf16[128,1536]{1,0:T(8,128)(2,1)S(1)}, u32[]{:S(2)}, u32[]{:S(2)}) collective-permute-start(bf16[128,1536]{1,0:T(8,128)(2,1)S(1)} %shard_map.149), channel_id=1, source_target_pairs={{0,2},{1,3},{2,0},{3,1},{4,6},{5,7},{6,4},{7,5},{8,10},{9,11},{10,... | collective-permute-start | bytes 1179656 | tf_op jit(solution)/shard_map/ppermute | solution.py:38
  66.9 1.9 %collective-permute-start.5 = (bf16[128,1536]{1,0:T(8,128)(2,1)S(1)}, bf16[128,1536]{1,0:T(8,128)(2,1)S(1)}, u32[]{:S(2)}, u32[]{:S(2)}) collective-permute-start(bf16[128,1536]{1,0:T(8,128)(2,1)S(1)} %get-tuple-element.47), channel_id=1, source_target_pairs={{0,3},{1,0},{2,1},{3,2},{4,7},{5,4},{6,5},{7,6},{8,11},{9,8},{10,9... | collective-permute-start | bytes 1179656 | tf_op jit(solution)/shard_map/ppermute | solution.py:38
  68.8 5.2 %collective-permute-done.3.refs_1_ = bf16[128,1536]{1,0:T(8,128)(2,1)S(1)} collective-permute-done((bf16[128,1536]{1,0:T(8,128)(2,1)S(1)}, bf16[128,1536]{1,0:T(8,128)(2,1)S(1)}, u32[]{:S(2)}, u32[]{:S(2)}) %collective-permute-start.3) | collective-permute-done | bytes 393248 | tf_op jit(solution)/shard_map/ppermute | solution.py:38
  74.0 3.9 %collective-permute-done.4.refs_2_ = bf16[128,1536]{1,0:T(8,128)(2,1)S(1)} collective-permute-done((bf16[128,1536]{1,0:T(8,128)(2,1)S(1)}, bf16[128,1536]{1,0:T(8,128)(2,1)S(1)}, u32[]{:S(2)}, u32[]{:S(2)}) %collective-permute-start.4) | collective-permute-done | bytes 393248 | tf_op jit(solution)/shard_map/ppermute | solution.py:38
  78.0 7.5 %collective-permute-done.5.refs_3_ = bf16[128,1536]{1,0:T(8,128)(2,1)S(1)} collective-permute-done((bf16[128,1536]{1,0:T(8,128)(2,1)S(1)}, bf16[128,1536]{1,0:T(8,128)(2,1)S(1)}, u32[]{:S(2)}, u32[]{:S(2)}) %collective-permute-start.5) | collective-permute-done | bytes 393248 | tf_op jit(solution)/shard_map/ppermute | solution.py:38
  85.9 2.5 %collective-permute-start.6 = (bf16[1552,128]{1,0:T(8,128)(2,1)S(1)}, bf16[1552,128]{1,0:T(8,128)(2,1)S(1)}, u32[]{:S(2)}, u32[]{:S(2)}) collective-permute-start(bf16[1552,128]{1,0:T(8,128)(2,1)S(1)} %shard_map.150.refs_0_), channel_id=1, source_target_pairs={{0,1},{1,2},{2,3},{3,0},{4,5},{5,6},{6,7},{7,4},{8,9},{9,10},{10,1... | collective-permute-start | bytes 1191944 | tf_op jit(solution)/shard_map/ppermute | solution.py:38
  88.4 4.3 %collective-permute-start.7 = (bf16[1552,128]{1,0:T(8,128)(2,1)S(1)}, bf16[1552,128]{1,0:T(8,128)(2,1)S(1)}, u32[]{:S(2)}, u32[]{:S(2)}) collective-permute-start(bf16[1552,128]{1,0:T(8,128)(2,1)S(1)} %shard_map.150.refs_0_), channel_id=1, source_target_pairs={{0,2},{1,3},{2,0},{3,1},{4,6},{5,7},{6,4},{7,5},{8,10},{9,11},{10,... | collective-permute-start | bytes 1191944 | tf_op jit(solution)/shard_map/ppermute | solution.py:38
  92.7 2.7 %collective-permute-start.8 = (bf16[1552,128]{1,0:T(8,128)(2,1)S(1)}, bf16[1552,128]{1,0:T(8,128)(2,1)S(1)}, u32[]{:S(2)}, u32[]{:S(2)}) collective-permute-start(bf16[1552,128]{1,0:T(8,128)(2,1)S(1)} %shard_map.150.refs_0_), channel_id=1, source_target_pairs={{0,3},{1,0},{2,1},{3,2},{4,7},{5,4},{6,5},{7,6},{8,11},{9,8},{10,9... | collective-permute-start | bytes 1191944 | tf_op jit(solution)/shard_map/ppermute | solution.py:38
  95.5 1.7 %shard_map.160 = bf16[128,128]{1,0:T(8,128)(2,1)} custom-call(bf16[2048,128]{1,0:T(8,128)(2,1)} %bitcast.15.terms_hbm), custom_call_target="tpu_custom_call" | custom-call | tf_op jit(solution)/shard_map/pallas_call | solution.py:68
  97.2 3.4 %all-to-all-start.3 = ((bf16[8,16,128]{2,1,0:T(8,128)(2,1)}), bf16[8,16,128]{2,1,0:T(8,128)(2,1)S(1)}, u32[]{:S(2)}, u32[]{:S(2)}) async-start(bf16[8,16,128]{2,1,0:T(8,128)(2,1)} %bitcast.16), calls=%async_computation.3 | async-start | bytes 65536 | tf_op jit(solution)/shard_map/all_to_all | solution.py:45
  100.6 1.2 shard_map.151.refs_4_
  101.9 2.0 %collective-permute-done.7.refs_2_ = bf16[1552,128]{1,0:T(8,128)(2,1)S(1)} collective-permute-done((bf16[1552,128]{1,0:T(8,128)(2,1)S(1)}, bf16[1552,128]{1,0:T(8,128)(2,1)S(1)}, u32[]{:S(2)}, u32[]{:S(2)}) %collective-permute-start.7) | collective-permute-done | bytes 397344 | tf_op jit(solution)/shard_map/ppermute | solution.py:38
  103.9 6.9 %collective-permute-done.8.refs_3_ = bf16[1552,128]{1,0:T(8,128)(2,1)S(1)} collective-permute-done((bf16[1552,128]{1,0:T(8,128)(2,1)S(1)}, bf16[1552,128]{1,0:T(8,128)(2,1)S(1)}, u32[]{:S(2)}, u32[]{:S(2)}) %collective-permute-start.8) | collective-permute-done | bytes 397344 | tf_op jit(solution)/shard_map/ppermute | solution.py:38
  110.8 1.8 %shard_map.152 = bf16[1024,384]{1,0:T(8,128)(2,1)} custom-call(s32[1]{0:T(128)} %bitcast.2.col, bf16[1552,128]{1,0:T(8,128)(2,1)S(1)} %shard_map.150.refs_0_, bf16[1552,128]{1,0:T(8,128)(2,1)S(1)} %collective-permute-done.6.refs_1_, bf16[1552,128]{1,0:T(8,128)(2,1)S(1)} %collective-permute-done.7.refs_2_, ...), custom_call_target="tpu_custom_call" | custom-call | tf_op jit(solution)/shard_map/pallas_call | solution.py:68
  113.2 9.9 %all-to-all-start.1 = ((bf16[128,8,384]{2,1,0:T(8,128)(2,1)}), bf16[128,8,384]{2,1,0:T(8,128)(2,1)S(1)}, u32[]{:S(2)}, u32[]{:S(2)}) async-start(bf16[128,8,384]{2,1,0:T(8,128)(2,1)} %bitcast.30), calls=%async_computation.1 | async-start | bytes 1572864 | tf_op jit(solution)/shard_map/all_to_all | solution.py:45
  123.6 4.3 %collective-permute-start.11 = (bf16[1536,128]{1,0:T(8,128)(2,1)S(1)}, bf16[1536,128]{1,0:T(8,128)(2,1)S(1)}, u32[]{:S(2)}, u32[]{:S(2)}) collective-permute-start(bf16[1536,128]{1,0:T(8,128)(2,1)S(1)} %shard_map.155), channel_id=1, source_target_pairs={{0,2},{1,3},{2,0},{3,1},{4,6},{5,7},{6,4},{7,5},{8,10},{9,11},{10,... | collective-permute-start | bytes 1179656 | tf_op jit(solution)/shard_map/ppermute | solution.py:38
  128.5 3.1 %collective-permute-start.9 = (bf16[1536,128]{1,0:T(8,128)(2,1)S(1)}, bf16[1536,128]{1,0:T(8,128)(2,1)S(1)}, u32[]{:S(2)}, u32[]{:S(2)}) collective-permute-start(bf16[1536,128]{1,0:T(8,128)(2,1)S(1)} %get-tuple-element.52), channel_id=1, source_target_pairs={{0,1},{1,2},{2,3},{3,0},{4,5},{5,6},{6,7},{7,4},{8,9},{9,10},{10,1... | collective-permute-start | bytes 1179656 | tf_op jit(solution)/shard_map/ppermute | solution.py:38
  131.7 2.7 %collective-permute-start.10 = (bf16[1536,128]{1,0:T(8,128)(2,1)S(1)}, bf16[1536,128]{1,0:T(8,128)(2,1)S(1)}, u32[]{:S(2)}, u32[]{:S(2)}) collective-permute-start(bf16[1536,128]{1,0:T(8,128)(2,1)S(1)} %get-tuple-element.53), channel_id=1, source_target_pairs={{0,3},{1,0},{2,1},{3,2},{4,7},{5,4},{6,5},{7,6},{8,11},{9,8},{10,9... | collective-permute-start | bytes 1179656 | tf_op jit(solution)/shard_map/ppermute | solution.py:38
  137.1 1.9 %collective-permute-done.11.refs_0_ = bf16[1536,128]{1,0:T(8,128)(2,1)S(1)} collective-permute-done((bf16[1536,128]{1,0:T(8,128)(2,1)S(1)}, bf16[1536,128]{1,0:T(8,128)(2,1)S(1)}, u32[]{:S(2)}, u32[]{:S(2)}) %collective-permute-start.11) | collective-permute-done | bytes 393248 | tf_op jit(solution)/shard_map/ppermute | solution.py:38
  139.7 4.3 %collective-permute-done.9.refs_0_ = bf16[1536,128]{1,0:T(8,128)(2,1)S(1)} collective-permute-done((bf16[1536,128]{1,0:T(8,128)(2,1)S(1)}, bf16[1536,128]{1,0:T(8,128)(2,1)S(1)}, u32[]{:S(2)}, u32[]{:S(2)}) %collective-permute-start.9) | collective-permute-done | bytes 393248 | tf_op jit(solution)/shard_map/ppermute | solution.py:38
  144.0 2.1 %collective-permute-done.10.refs_1_ = bf16[1536,128]{1,0:T(8,128)(2,1)S(1)} collective-permute-done((bf16[1536,128]{1,0:T(8,128)(2,1)S(1)}, bf16[1536,128]{1,0:T(8,128)(2,1)S(1)}, u32[]{:S(2)}, u32[]{:S(2)}) %collective-permute-start.10) | collective-permute-done | bytes 393248 | tf_op jit(solution)/shard_map/ppermute | solution.py:38
  148.6 1.3 shard_map.153
  (50 shorter events, 11.0 us)
Async XLA Ops:
  3.3 18.0 %copy-start.2 = (bf16[1,2048,128]{2,1,0:T(8,128)(2,1)S(1)}, bf16[1,2048,128]{2,1,0:T(8,128)(2,1)}, u32[]{:S(2)}) copy-start(bf16[1,2048,128]{2,1,0:T(8,128)(2,1)} %param.13) | copy-start | bytes 1572868
  3.3 18.0 %copy-start.3 = (bf16[1,2048,128]{2,1,0:T(8,128)(2,1)S(1)}, bf16[1,2048,128]{2,1,0:T(8,128)(2,1)}, u32[]{:S(2)}) copy-start(bf16[1,2048,128]{2,1,0:T(8,128)(2,1)} %param.14) | copy-start | bytes 1572868
  3.3 18.0 %copy-start.4 = (bf16[1,128,2048]{2,1,0:T(8,128)(2,1)S(1)}, bf16[1,128,2048]{2,1,0:T(8,128)(2,1)}, u32[]{:S(2)}) copy-start(bf16[1,128,2048]{2,1,0:T(8,128)(2,1)} %param.15) | copy-start | bytes 1572868
  3.4 48.2 %all-to-all-start = ((bf16[128,8,512]{2,1,0:T(8,128)(2,1)}), bf16[128,8,512]{2,1,0:T(8,128)(2,1)S(1)}, u32[]{:S(2)}, u32[]{:S(2)}) async-start(bf16[128,8,512]{2,1,0:T(8,128)(2,1)} %bitcast.29), calls=%async_computation | async-start | bytes 2097152 | tf_op jit(solution)/shard_map/all_to_all | solution.py:45
  21.3 10.2 %copy-start.1 = (bf16[128,2048]{1,0:T(8,128)(2,1)S(1)}, bf16[128,2048]{1,0:T(8,128)(2,1)}, u32[]{:S(2)}) copy-start(bf16[128,2048]{1,0:T(8,128)(2,1)} %cot_ref.3) | copy-start | bytes 1572868
  21.4 10.2 %copy-start.5 = (bf16[2048,128]{1,0:T(8,128)(2,1)S(1)}, bf16[2048,128]{1,0:T(8,128)(2,1)}, u32[]{:S(2)}) copy-start(bf16[2048,128]{1,0:T(8,128)(2,1)} %down_ref.1) | copy-start | bytes 1572868
  21.4 10.2 %copy-start.11 = (bf16[128,128]{1,0:T(8,128)(2,1)S(1)}, bf16[128,128]{1,0:T(8,128)(2,1)}, u32[]{:S(2)}) copy-start(bf16[128,128]{1,0:T(8,128)(2,1)} %hid_ref.1) | copy-start | bytes 98308
  22.9 32.9 %collective-permute-start = (bf16[1536,128]{1,0:T(8,128)(2,1)}, bf16[1536,128]{1,0:T(8,128)(2,1)S(1)}, u32[]{:S(2)}, u32[]{:S(2)}) collective-permute-start(bf16[1536,128]{1,0:T(8,128)(2,1)} %get-tuple-element.40), channel_id=1, source_target_pairs={{0,1},{1,2},{2,3},{3,0},{4,5},{5,6},{6,7},{7,4},{8,9},{9,10},{10,1... | collective-permute-start | bytes 1179656 | tf_op jit(solution)/shard_map/ppermute | solution.py:38
  25.3 30.5 %collective-permute-start.1 = (bf16[1536,128]{1,0:T(8,128)(2,1)S(1)}, bf16[1536,128]{1,0:T(8,128)(2,1)S(1)}, u32[]{:S(2)}, u32[]{:S(2)}) collective-permute-start(bf16[1536,128]{1,0:T(8,128)(2,1)S(1)} %get-tuple-element.41), channel_id=1, source_target_pairs={{0,2},{1,3},{2,0},{3,1},{4,6},{5,7},{6,4},{7,5},{8,10},{9,11},{10,... | collective-permute-start | bytes 1179656 | tf_op jit(solution)/shard_map/ppermute | solution.py:38
  29.7 26.2 %collective-permute-start.2 = (bf16[1536,128]{1,0:T(8,128)(2,1)S(1)}, bf16[1536,128]{1,0:T(8,128)(2,1)S(1)}, u32[]{:S(2)}, u32[]{:S(2)}) collective-permute-start(bf16[1536,128]{1,0:T(8,128)(2,1)S(1)} %get-tuple-element.42), channel_id=1, source_target_pairs={{0,3},{1,0},{2,1},{3,2},{4,7},{5,4},{6,5},{7,6},{8,11},{9,8},{10,9... | collective-permute-start | bytes 1179656 | tf_op jit(solution)/shard_map/ppermute | solution.py:38
  51.5 43.9 %all-to-all-start.2 = ((bf16[16,128,128]{2,1,0:T(8,128)(2,1)}), bf16[16,128,128]{2,1,0:T(8,128)(2,1)}, u32[]{:S(2)}, u32[]{:S(2)}) async-start(bf16[16,128,128]{2,1,0:T(8,128)(2,1)} %bitcast.14), calls=%async_computation.2 | async-start | bytes 1048576 | tf_op jit(solution)/shard_map/all_to_all | solution.py:45
  59.4 26.0 %copy-start.6 = (bf16[128,1536]{1,0:T(8,128)(2,1)S(1)}, bf16[128,1536]{1,0:T(8,128)(2,1)}, u32[]{:S(2)}) copy-start(bf16[128,1536]{1,0:T(8,128)(2,1)} %get-tuple-element.45.refs_0_) | copy-start | bytes 1179652
  60.1 13.9 %collective-permute-start.3 = (bf16[128,1536]{1,0:T(8,128)(2,1)S(1)}, bf16[128,1536]{1,0:T(8,128)(2,1)S(1)}, u32[]{:S(2)}, u32[]{:S(2)}) collective-permute-start(bf16[128,1536]{1,0:T(8,128)(2,1)S(1)} %get-tuple-element.46), channel_id=1, source_target_pairs={{0,1},{1,2},{2,3},{3,0},{4,5},{5,6},{6,7},{7,4},{8,9},{9,10},{10,1... | collective-permute-start | bytes 1179656 | tf_op jit(solution)/shard_map/ppermute | solution.py:38
  62.5 15.4 %collective-permute-start.4 = (bf16[128,1536]{1,0:T(8,128)(2,1)S(1)}, bf16[128,1536]{1,0:T(8,128)(2,1)S(1)}, u32[]{:S(2)}, u32[]{:S(2)}) collective-permute-start(bf16[128,1536]{1,0:T(8,128)(2,1)S(1)} %shard_map.149), channel_id=1, source_target_pairs={{0,2},{1,3},{2,0},{3,1},{4,6},{5,7},{6,4},{7,5},{8,10},{9,11},{10,... | collective-permute-start | bytes 1179656 | tf_op jit(solution)/shard_map/ppermute | solution.py:38
  66.9 18.6 %collective-permute-start.5 = (bf16[128,1536]{1,0:T(8,128)(2,1)S(1)}, bf16[128,1536]{1,0:T(8,128)(2,1)S(1)}, u32[]{:S(2)}, u32[]{:S(2)}) collective-permute-start(bf16[128,1536]{1,0:T(8,128)(2,1)S(1)} %get-tuple-element.47), channel_id=1, source_target_pairs={{0,3},{1,0},{2,1},{3,2},{4,7},{5,4},{6,5},{7,6},{8,11},{9,8},{10,9... | collective-permute-start | bytes 1179656 | tf_op jit(solution)/shard_map/ppermute | solution.py:38
  85.9 16.0 %collective-permute-start.6 = (bf16[1552,128]{1,0:T(8,128)(2,1)S(1)}, bf16[1552,128]{1,0:T(8,128)(2,1)S(1)}, u32[]{:S(2)}, u32[]{:S(2)}) collective-permute-start(bf16[1552,128]{1,0:T(8,128)(2,1)S(1)} %shard_map.150.refs_0_), channel_id=1, source_target_pairs={{0,1},{1,2},{2,3},{3,0},{4,5},{5,6},{6,7},{7,4},{8,9},{9,10},{10,1... | collective-permute-start | bytes 1191944 | tf_op jit(solution)/shard_map/ppermute | solution.py:38
  88.4 15.5 %collective-permute-start.7 = (bf16[1552,128]{1,0:T(8,128)(2,1)S(1)}, bf16[1552,128]{1,0:T(8,128)(2,1)S(1)}, u32[]{:S(2)}, u32[]{:S(2)}) collective-permute-start(bf16[1552,128]{1,0:T(8,128)(2,1)S(1)} %shard_map.150.refs_0_), channel_id=1, source_target_pairs={{0,2},{1,3},{2,0},{3,1},{4,6},{5,7},{6,4},{7,5},{8,10},{9,11},{10,... | collective-permute-start | bytes 1191944 | tf_op jit(solution)/shard_map/ppermute | solution.py:38
  92.7 18.1 %collective-permute-start.8 = (bf16[1552,128]{1,0:T(8,128)(2,1)S(1)}, bf16[1552,128]{1,0:T(8,128)(2,1)S(1)}, u32[]{:S(2)}, u32[]{:S(2)}) collective-permute-start(bf16[1552,128]{1,0:T(8,128)(2,1)S(1)} %shard_map.150.refs_0_), channel_id=1, source_target_pairs={{0,3},{1,0},{2,1},{3,2},{4,7},{5,4},{6,5},{7,6},{8,11},{9,8},{10,9... | collective-permute-start | bytes 1191944 | tf_op jit(solution)/shard_map/ppermute | solution.py:38
  97.2 15.4 %all-to-all-start.3 = ((bf16[8,16,128]{2,1,0:T(8,128)(2,1)}), bf16[8,16,128]{2,1,0:T(8,128)(2,1)S(1)}, u32[]{:S(2)}, u32[]{:S(2)}) async-start(bf16[8,16,128]{2,1,0:T(8,128)(2,1)} %bitcast.16), calls=%async_computation.3 | async-start | bytes 65536 | tf_op jit(solution)/shard_map/all_to_all | solution.py:45
  112.6 10.5 %copy-start = (bf16[512,1024]{1,0:T(8,128)(2,1)S(1)}, bf16[512,1024]{1,0:T(8,128)(2,1)}, u32[]{:S(2)}) copy-start(bf16[512,1024]{1,0:T(8,128)(2,1)} %get-tuple-element.51.xg_ref) | copy-start | bytes 3145732
  112.6 0.6 copy-start.9
  113.2 34.7 %all-to-all-start.1 = ((bf16[128,8,384]{2,1,0:T(8,128)(2,1)}), bf16[128,8,384]{2,1,0:T(8,128)(2,1)S(1)}, u32[]{:S(2)}, u32[]{:S(2)}) async-start(bf16[128,8,384]{2,1,0:T(8,128)(2,1)} %bitcast.30), calls=%async_computation.1 | async-start | bytes 1572864 | tf_op jit(solution)/shard_map/all_to_all | solution.py:45
  123.5 11.8 %copy-start.10 = (bf16[8,16,128]{2,1,0:T(8,128)(2,1)S(1)}, bf16[8,16,128]{2,1,0:T(8,128)(2,1)}, u32[]{:S(2)}) copy-start(bf16[8,16,128]{2,1,0:T(8,128)(2,1)} %copy-done.9) | copy-start | bytes 98308
  123.6 15.4 %collective-permute-start.11 = (bf16[1536,128]{1,0:T(8,128)(2,1)S(1)}, bf16[1536,128]{1,0:T(8,128)(2,1)S(1)}, u32[]{:S(2)}, u32[]{:S(2)}) collective-permute-start(bf16[1536,128]{1,0:T(8,128)(2,1)S(1)} %shard_map.155), channel_id=1, source_target_pairs={{0,2},{1,3},{2,0},{3,1},{4,6},{5,7},{6,4},{7,5},{8,10},{9,11},{10,... | collective-permute-start | bytes 1179656 | tf_op jit(solution)/shard_map/ppermute | solution.py:38
  128.5 5.9 %copy-start.13 = (f32[128,2]{0,1:T(2,128)S(1)}, f32[128,2]{0,1:T(2,128)}, u32[]{:S(2)}) copy-start(f32[128,2]{0,1:T(2,128)} %param.11) | copy-start | bytes 3076
  128.5 5.9 %copy-start.12 = (s32[128,2]{0,1:T(2,128)S(1)}, s32[128,2]{0,1:T(2,128)}, u32[]{:S(2)}) copy-start(s32[128,2]{0,1:T(2,128)} %param.12) | copy-start | bytes 3076
  128.5 15.5 %collective-permute-start.9 = (bf16[1536,128]{1,0:T(8,128)(2,1)S(1)}, bf16[1536,128]{1,0:T(8,128)(2,1)S(1)}, u32[]{:S(2)}, u32[]{:S(2)}) collective-permute-start(bf16[1536,128]{1,0:T(8,128)(2,1)S(1)} %get-tuple-element.52), channel_id=1, source_target_pairs={{0,1},{1,2},{2,3},{3,0},{4,5},{5,6},{6,7},{7,4},{8,9},{9,10},{10,1... | collective-permute-start | bytes 1179656 | tf_op jit(solution)/shard_map/ppermute | solution.py:38
  131.7 14.4 %collective-permute-start.10 = (bf16[1536,128]{1,0:T(8,128)(2,1)S(1)}, bf16[1536,128]{1,0:T(8,128)(2,1)S(1)}, u32[]{:S(2)}, u32[]{:S(2)}) collective-permute-start(bf16[1536,128]{1,0:T(8,128)(2,1)S(1)} %get-tuple-element.53), channel_id=1, source_target_pairs={{0,3},{1,0},{2,1},{3,2},{4,7},{5,4},{6,5},{7,6},{8,11},{9,8},{10,9... | collective-permute-start | bytes 1179656 | tf_op jit(solution)/shard_map/ppermute | solution.py:38
  134.6 0.7 copy-start.7
  135.3 0.6 copy-start.14
  146.1 1.8 %copy-start.8 = (bf16[512,128]{1,0:T(8,128)(2,1)S(1)}, bf16[512,128]{1,0:T(8,128)(2,1)}, u32[]{:S(2)}) copy-start(bf16[512,128]{1,0:T(8,128)(2,1)} %copy-done.7) | copy-start | bytes 393220
  147.9 0.7 copy-start.15

commit v5 on v4

--- a/solution.py
+++ b/solution.py
@@ -19,6 +19,7 @@
 HBM = pl.BlockSpec(memory_space=pltpu.HBM)
 LIMIT = pltpu.CompilerParams(vmem_limit_bytes=12 * 2**20)
 CAP = 4
+CAP_BITS = 2
 LANES = 128
 PAD = 16
 FAR = 2
@@ -77,19 +78,19 @@
     return got[0] if single else got
 
 
-def weave():
+def weave(back=False):
     rows = 64 * CAP
-    row = lax.broadcasted_iota(jnp.int32, (rows, rows), 0)
-    col = lax.broadcasted_iota(jnp.int32, (rows, rows), 1)
-    s, rest = row // (2 * CAP), row % (2 * CAP)
-    h, r = rest // CAP, rest % CAP
-    return jnp.where(col == h * (rows // 2) + s * CAP + r, 1.0, 0.0).astype(BF16)
+    row = lax.broadcasted_iota(jnp.int32, (rows, rows), int(back))
+    col = lax.broadcasted_iota(jnp.int32, (rows, rows), 1 - int(back))
+    s, h, r = row >> (CAP_BITS + 1), (row >> CAP_BITS) & 1, row & (CAP - 1)
+    place = (h << (CAP_BITS + 5)) + (s << CAP_BITS) + r
+    return jnp.where(col == place, 1.0, 0.0).astype(BF16)
 
 
 def chosen(routes_ref, slots, turns=1, start=0):
     count = routes_ref.shape[1]
     row = start + lax.broadcasted_iota(jnp.int32, (turns * slots, count), 0)
-    expert = row // (turns * CAP)
+    expert = row >> (CAP_BITS + turns - 1)
     first = expert == routes_ref[0:1, :]
     second = expert == routes_ref[1:2, :]
     named = jnp.where(first | second, 1.0, 0.0)
@@ -97,7 +98,7 @@
     later = lax.broadcasted_iota(jnp.int32, (count, count), 1)
     before = jnp.where(earlier < later, 1.0, 0.0).astype(BF16)
     rank = mm(named.astype(BF16), before)
-    place = (row % CAP).astype(F32)
+    place = (row & (CAP - 1)).astype(F32)
     hit = jnp.where(rank == place, named, 0.0)
     return hit, jnp.where(first, hit, 0.0), jnp.where(second, hit, 0.0)
 
@@ -127,7 +128,7 @@
         if b == 0:
             copies[0].wait()
         hit, one, two = chosen(routes, half // 2, 2, b * half)
-        kind = (lax.broadcasted_iota(jnp.int32, hit.shape, 0) // CAP) % 2
+        kind = (lax.broadcasted_iota(jnp.int32, hit.shape, 0) >> CAP_BITS) & 1
         pick = jnp.concatenate(
             [jnp.where(kind == 0, hit, 0.0), jnp.where(kind == 1, hit, 0.0)], axis=1
         )
@@ -166,10 +167,7 @@
         terms_ref[:, k] = terms[k]
 
 
-def fold_kernel(terms_hbm, out_ref, terms_ref, sem):
-    copy = pltpu.make_async_copy(terms_hbm, terms_ref, sem)
-    copy.start()
-    copy.wait()
+def fold_kernel(terms_ref, out_ref):
     terms = terms_ref[...].astype(F32)
     out_ref[...] = jnp.sum(terms.reshape(-1, *out_ref.shape), axis=0).astype(BF16)
 
@@ -227,7 +225,7 @@
 
 
 def apart(order, got):
-    split = mm(order, got, ROWS).astype(BF16)
+    split = mm(order, got).astype(BF16)
     half = split.shape[0] // 2
     return split[:half], split[half:]
 
@@ -236,7 +234,7 @@
     rows = out_ref.shape[0]
     parts = got_ref.shape[0] // (2 * rows)
     width = both_ref.shape[1]
-    x, g = apart(weave(), got_ref[span(at(col, FAR, parts), 2 * rows), :])
+    x, g = apart(weave(True), got_ref[span(at(col, FAR, parts), 2 * rows), :])
     out_ref[:, :width] = mm(x, both_ref[...]).astype(BF16)
     out_ref[:, width:] = mm(g, down_ref[...], LAST).astype(BF16)
 
@@ -249,7 +247,7 @@
     parts = got_ref.shape[0] // (2 * rows)
     width = both_ref.shape[1]
     quarter = got_ref.shape[1]
-    order = weave()
+    order = weave(True)
     for b in range(parts):
         x, g = apart(order, got_ref[2 * b * rows : 2 * (b + 1) * rows, :])
         xg_ref[b * rows : (b + 1) * rows, :quarter] = x
@@ -422,12 +420,12 @@
 
 def combine_kernel(inverse_ref, one_ref, two_ref, back_ref, out_ref, weights_out):
     slots = one_ref.shape[0]
-    order = weave()
+    order = weave(True)
     half = order.shape[0] // 2
     width = out_ref.shape[1] // 2
     left, right, shares = [], [], []
     for b in range(slots // half):
-        own = mm(order, back_ref[2 * b * half : 2 * (b + 1) * half, :], ROWS).astype(BF16)
+        own = mm(order, back_ref[2 * b * half : 2 * (b + 1) * half, :]).astype(BF16)
         left.append(own[:half, :width])
         right.append(own[half:, :width])
         shares.append(own[:half, width:].astype(F32))
@@ -618,15 +616,11 @@
         shared_down,
     )
     shared = over(shared.reshape(feat, block), ("y", "core"))
-    shared = local(
-        fold_kernel,
-        half(feat // inner, block),
-        shared,
-        spaces="h",
-        scratch=[pltpu.VMEM((feat, block), BF16), pltpu.SemaphoreType.DMA],
-    )
+    shared = local(fold_kernel, half(feat // inner, block), shared)
     shared = over(shared, "z")
-    shared_grad = local(total_kernel, jax.ShapeDtypeStruct((feat // ep, block), F32), shared)
+    shared_grad = local(
+        total_kernel, jax.ShapeDtypeStruct((feat // ep, block), F32), shared
+    )
     return (
         tokens_grad,
         weights_grad,

time: 153 us -> 152 us (level)
  no operation moved by 1% of the time
where the time goes in v5:
time: 152 us; the launch traced here: 150 us
  starting transfers between devices  72.4 us (48%)
  waiting for transfers between devices  54.4 us (36%)
  Pallas kernels  19.8 us (13%)
  local copies, waits for them, and re-layouts  2.01 us (1%)
    ppermute x12, starting transfers between devices, around(): lax.ppermute(part, 'tp', [(i, (i + k + 1) % size) for i in range(size)])  37 us
    all_to_all x4, starting transfers between devices, over(): lax.all_to_all(rows, axes, split_axis=0, concat_axis=0, tiled=True)  35.4 us
    ppermute x12, waiting for transfers between devices, around(): lax.ppermute(part, 'tp', [(i, (i + k + 1) % size) for i in range(size)])  35 us
    pallas_call x18, Pallas kernels, local(): pl.pallas_call(kernel, in_specs=[spec[k] for k in spaces], out_specs=[spe...  19.8 us
    all_to_all x4, waiting for transfers between devices, over(): lax.all_to_all(rows, axes, split_axis=0, concat_axis=0, tiled=True)  19.4 us
  transfers between devices with their start and end apart: 16, of which 10 were waited for; matrix products, arithmetic and copies ran while one was open for 0% of the time, Pallas kernels for 11%

profile of v5, /device:TPU:6, one launch (start us, length us, event | category | flops | bytes accessed | tf_op | source)
XLA Modules:
  0.0 149.6 jit_solution(17957320744704899389)
XLA Ops:
  0.6 2.7 %shard_map.145 = bf16[1024,512]{1,0:T(8,128)(2,1)} custom-call(s32[1]{0:T(128)} %bitcast.2.col, s32[2,128]{1,0:T(2,128)} %bitcast.26, f32[2,128]{1,0:T(2,128)} %bitcast.28, bf16[128,2048]{1,0:T(8,128)(2,1)} %tok_ref.1, bf16[128,2048]{1,0:T(8,128)(2,1)} %cot_ref.3), custom_call_target="tpu_custom_call" | custom-call | tf_op jit(solution)/shard_map/pallas_call | solution.py:69
  3.4 18.0 %all-to-all-start = ((bf16[128,8,512]{2,1,0:T(8,128)(2,1)}), bf16[128,8,512]{2,1,0:T(8,128)(2,1)S(1)}, u32[]{:S(2)}, u32[]{:S(2)}) async-start(bf16[128,8,512]{2,1,0:T(8,128)(2,1)} %bitcast.30), calls=%async_computation | async-start | bytes 2097152 | tf_op jit(solution)/shard_map/all_to_all | solution.py:46
  21.4 1.7 %shard_map.146 = (bf16[1536,128]{1,0:T(8,128)(2,1)}, bf16[1536,128]{1,0:T(8,128)(2,1)}, bf16[1536,128]{1,0:T(8,128)(2,1)}, bf16[1536,128]{1,0:T(8,128)(2,1)S(1)}) custom-call(s32[1]{0:T(128)} %bitcast.2.col, bf16[2048,128]{1,0:T(8,128)(2,1)S(1)} %bitcast.22, bf16[2048,128]{1,0:T(8,128)(2,1)S(1)} %bitcast.23, bf16[128,2048]{1,0:T(8,128)(2,1)S(1)} %bitcast.24), custom_call_target="tpu_custom_call" | custom-call | tf_op jit(solution)/shard_map/pallas_call | solution.py:69
  23.1 2.4 %collective-permute-start = (bf16[1536,128]{1,0:T(8,128)(2,1)}, bf16[1536,128]{1,0:T(8,128)(2,1)S(1)}, u32[]{:S(2)}, u32[]{:S(2)}) collective-permute-start(bf16[1536,128]{1,0:T(8,128)(2,1)} %get-tuple-element.40), channel_id=1, source_target_pairs={{0,1},{1,2},{2,3},{3,0},{4,5},{5,6},{6,7},{7,4},{8,9},{9,10},{10,1... | collective-permute-start | bytes 1179656 | tf_op jit(solution)/shard_map/ppermute | solution.py:39
  25.5 4.3 %collective-permute-start.1 = (bf16[1536,128]{1,0:T(8,128)(2,1)}, bf16[1536,128]{1,0:T(8,128)(2,1)S(1)}, u32[]{:S(2)}, u32[]{:S(2)}) collective-permute-start(bf16[1536,128]{1,0:T(8,128)(2,1)} %get-tuple-element.41), channel_id=1, source_target_pairs={{0,2},{1,3},{2,0},{3,1},{4,6},{5,7},{6,4},{7,5},{8,10},{9,11},{10,... | collective-permute-start | bytes 1179656 | tf_op jit(solution)/shard_map/ppermute | solution.py:39
  29.8 1.9 %collective-permute-start.2 = (bf16[1536,128]{1,0:T(8,128)(2,1)S(1)}, bf16[1536,128]{1,0:T(8,128)(2,1)S(1)}, u32[]{:S(2)}, u32[]{:S(2)}) collective-permute-start(bf16[1536,128]{1,0:T(8,128)(2,1)S(1)} %get-tuple-element.42), channel_id=1, source_target_pairs={{0,3},{1,0},{2,1},{3,2},{4,7},{5,4},{6,5},{7,6},{8,11},{9,8},{10,9... | collective-permute-start | bytes 1179656 | tf_op jit(solution)/shard_map/ppermute | solution.py:39
  31.7 1.2 shard_map.159
  33.0 18.6 %all-to-all-done = bf16[128,8,512]{2,1,0:T(8,128)(2,1)S(1)} async-done(((bf16[128,8,512]{2,1,0:T(8,128)(2,1)}), bf16[128,8,512]{2,1,0:T(8,128)(2,1)S(1)}, u32[]{:S(2)}, u32[]{:S(2)}) %all-to-all-start) | async-done | bytes 1048608 | tf_op jit(solution)/shard_map/all_to_all | solution.py:46
  51.5 4.2 %all-to-all-start.2 = ((bf16[16,128,128]{2,1,0:T(8,128)(2,1)}), bf16[16,128,128]{2,1,0:T(8,128)(2,1)S(1)}, u32[]{:S(2)}, u32[]{:S(2)}) async-start(bf16[16,128,128]{2,1,0:T(8,128)(2,1)} %bitcast.14), calls=%async_computation.2 | async-start | bytes 1048576 | tf_op jit(solution)/shard_map/all_to_all | solution.py:46
  56.9 2.4 %shard_map.148 = (bf16[512,1024]{1,0:T(8,128)(2,1)}, bf16[128,1536]{1,0:T(8,128)(2,1)}, bf16[512,1024]{1,0:T(8,128)(2,1)}, bf16[128,1536]{1,0:T(8,128)(2,1)S(1)}, bf16[128,1536]{1,0:T(8,128)(2,1)S(1)}) custom-call(s32[1]{0:T(128)} %bitcast.2.col, bf16[1024,512]{1,0:T(8,128)(2,1)S(1)} %bitcast.18, bf16[512,1024]{1,0:T(8,128)(2,1)S(1)} %get-tuple-element.43.both_ref, ...), custom_call_target="tpu_custom_call" | custom-call | tf_op jit(solution)/shard_map/pallas_call | solution.py:69
  59.9 2.4 %collective-permute-start.3 = (bf16[128,1536]{1,0:T(8,128)(2,1)S(1)}, bf16[128,1536]{1,0:T(8,128)(2,1)S(1)}, u32[]{:S(2)}, u32[]{:S(2)}) collective-permute-start(bf16[128,1536]{1,0:T(8,128)(2,1)S(1)} %get-tuple-element.46), channel_id=1, source_target_pairs={{0,1},{1,2},{2,3},{3,0},{4,5},{5,6},{6,7},{7,4},{8,9},{9,10},{10,1... | collective-permute-start | bytes 1179656 | tf_op jit(solution)/shard_map/ppermute | solution.py:39
  62.3 4.3 %collective-permute-start.4 = (bf16[128,1536]{1,0:T(8,128)(2,1)S(1)}, bf16[128,1536]{1,0:T(8,128)(2,1)S(1)}, u32[]{:S(2)}, u32[]{:S(2)}) collective-permute-start(bf16[128,1536]{1,0:T(8,128)(2,1)S(1)} %shard_map.149), channel_id=1, source_target_pairs={{0,2},{1,3},{2,0},{3,1},{4,6},{5,7},{6,4},{7,5},{8,10},{9,11},{10,... | collective-permute-start | bytes 1179656 | tf_op jit(solution)/shard_map/ppermute | solution.py:39
  66.7 1.9 %collective-permute-start.5 = (bf16[128,1536]{1,0:T(8,128)(2,1)S(1)}, bf16[128,1536]{1,0:T(8,128)(2,1)S(1)}, u32[]{:S(2)}, u32[]{:S(2)}) collective-permute-start(bf16[128,1536]{1,0:T(8,128)(2,1)S(1)} %get-tuple-element.47), channel_id=1, source_target_pairs={{0,3},{1,0},{2,1},{3,2},{4,7},{5,4},{6,5},{7,6},{8,11},{9,8},{10,9... | collective-permute-start | bytes 1179656 | tf_op jit(solution)/shard_map/ppermute | solution.py:39
  68.6 5.2 %collective-permute-done.3.refs_1_ = bf16[128,1536]{1,0:T(8,128)(2,1)S(1)} collective-permute-done((bf16[128,1536]{1,0:T(8,128)(2,1)S(1)}, bf16[128,1536]{1,0:T(8,128)(2,1)S(1)}, u32[]{:S(2)}, u32[]{:S(2)}) %collective-permute-start.3) | collective-permute-done | bytes 393248 | tf_op jit(solution)/shard_map/ppermute | solution.py:39
  73.8 3.9 %collective-permute-done.4.refs_2_ = bf16[128,1536]{1,0:T(8,128)(2,1)S(1)} collective-permute-done((bf16[128,1536]{1,0:T(8,128)(2,1)S(1)}, bf16[128,1536]{1,0:T(8,128)(2,1)S(1)}, u32[]{:S(2)}, u32[]{:S(2)}) %collective-permute-start.4) | collective-permute-done | bytes 393248 | tf_op jit(solution)/shard_map/ppermute | solution.py:39
  77.7 7.5 %collective-permute-done.5.refs_3_ = bf16[128,1536]{1,0:T(8,128)(2,1)S(1)} collective-permute-done((bf16[128,1536]{1,0:T(8,128)(2,1)S(1)}, bf16[128,1536]{1,0:T(8,128)(2,1)S(1)}, u32[]{:S(2)}, u32[]{:S(2)}) %collective-permute-start.5) | collective-permute-done | bytes 393248 | tf_op jit(solution)/shard_map/ppermute | solution.py:39
  85.7 2.5 %collective-permute-start.6 = (bf16[1552,128]{1,0:T(8,128)(2,1)S(1)}, bf16[1552,128]{1,0:T(8,128)(2,1)S(1)}, u32[]{:S(2)}, u32[]{:S(2)}) collective-permute-start(bf16[1552,128]{1,0:T(8,128)(2,1)S(1)} %shard_map.150.refs_0_), channel_id=1, source_target_pairs={{0,1},{1,2},{2,3},{3,0},{4,5},{5,6},{6,7},{7,4},{8,9},{9,10},{10,1... | collective-permute-start | bytes 1191944 | tf_op jit(solution)/shard_map/ppermute | solution.py:39
  88.2 4.3 %collective-permute-start.7 = (bf16[1552,128]{1,0:T(8,128)(2,1)S(1)}, bf16[1552,128]{1,0:T(8,128)(2,1)S(1)}, u32[]{:S(2)}, u32[]{:S(2)}) collective-permute-start(bf16[1552,128]{1,0:T(8,128)(2,1)S(1)} %shard_map.150.refs_0_), channel_id=1, source_target_pairs={{0,2},{1,3},{2,0},{3,1},{4,6},{5,7},{6,4},{7,5},{8,10},{9,11},{10,... | collective-permute-start | bytes 1191944 | tf_op jit(solution)/shard_map/ppermute | solution.py:39
  92.6 2.7 %collective-permute-start.8 = (bf16[1552,128]{1,0:T(8,128)(2,1)S(1)}, bf16[1552,128]{1,0:T(8,128)(2,1)S(1)}, u32[]{:S(2)}, u32[]{:S(2)}) collective-permute-start(bf16[1552,128]{1,0:T(8,128)(2,1)S(1)} %shard_map.150.refs_0_), channel_id=1, source_target_pairs={{0,3},{1,0},{2,1},{3,2},{4,7},{5,4},{6,5},{7,6},{8,11},{9,8},{10,9... | collective-permute-start | bytes 1191944 | tf_op jit(solution)/shard_map/ppermute | solution.py:39
  96.0 3.3 %all-to-all-start.3 = ((bf16[8,16,128]{2,1,0:T(8,128)(2,1)}), bf16[8,16,128]{2,1,0:T(8,128)(2,1)S(1)}, u32[]{:S(2)}, u32[]{:S(2)}) async-start(bf16[8,16,128]{2,1,0:T(8,128)(2,1)} %bitcast.16), calls=%async_computation.3 | async-start | bytes 65536 | tf_op jit(solution)/shard_map/all_to_all | solution.py:46
  99.3 1.2 shard_map.151.refs_4_
  100.6 3.1 %collective-permute-done.7.refs_2_ = bf16[1552,128]{1,0:T(8,128)(2,1)S(1)} collective-permute-done((bf16[1552,128]{1,0:T(8,128)(2,1)S(1)}, bf16[1552,128]{1,0:T(8,128)(2,1)S(1)}, u32[]{:S(2)}, u32[]{:S(2)}) %collective-permute-start.7) | collective-permute-done | bytes 397344 | tf_op jit(solution)/shard_map/ppermute | solution.py:39
  103.7 6.9 %collective-permute-done.8.refs_3_ = bf16[1552,128]{1,0:T(8,128)(2,1)S(1)} collective-permute-done((bf16[1552,128]{1,0:T(8,128)(2,1)S(1)}, bf16[1552,128]{1,0:T(8,128)(2,1)S(1)}, u32[]{:S(2)}, u32[]{:S(2)}) %collective-permute-start.8) | collective-permute-done | bytes 397344 | tf_op jit(solution)/shard_map/ppermute | solution.py:39
  110.7 1.8 %shard_map.152 = bf16[1024,384]{1,0:T(8,128)(2,1)} custom-call(s32[1]{0:T(128)} %bitcast.2.col, bf16[1552,128]{1,0:T(8,128)(2,1)S(1)} %shard_map.150.refs_0_, bf16[1552,128]{1,0:T(8,128)(2,1)S(1)} %collective-permute-done.6.refs_1_, bf16[1552,128]{1,0:T(8,128)(2,1)S(1)} %collective-permute-done.7.refs_2_, ...), custom_call_target="tpu_custom_call" | custom-call | tf_op jit(solution)/shard_map/pallas_call | solution.py:69
  113.1 9.9 %all-to-all-start.1 = ((bf16[128,8,384]{2,1,0:T(8,128)(2,1)}), bf16[128,8,384]{2,1,0:T(8,128)(2,1)S(1)}, u32[]{:S(2)}, u32[]{:S(2)}) async-start(bf16[128,8,384]{2,1,0:T(8,128)(2,1)} %bitcast.31), calls=%async_computation.1 | async-start | bytes 1572864 | tf_op jit(solution)/shard_map/all_to_all | solution.py:46
  123.4 4.3 %collective-permute-start.11 = (bf16[1536,128]{1,0:T(8,128)(2,1)S(1)}, bf16[1536,128]{1,0:T(8,128)(2,1)S(1)}, u32[]{:S(2)}, u32[]{:S(2)}) collective-permute-start(bf16[1536,128]{1,0:T(8,128)(2,1)S(1)} %shard_map.155), channel_id=1, source_target_pairs={{0,2},{1,3},{2,0},{3,1},{4,6},{5,7},{6,4},{7,5},{8,10},{9,11},{10,... | collective-permute-start | bytes 1179656 | tf_op jit(solution)/shard_map/ppermute | solution.py:39
  128.4 3.1 %collective-permute-start.9 = (bf16[1536,128]{1,0:T(8,128)(2,1)S(1)}, bf16[1536,128]{1,0:T(8,128)(2,1)S(1)}, u32[]{:S(2)}, u32[]{:S(2)}) collective-permute-start(bf16[1536,128]{1,0:T(8,128)(2,1)S(1)} %get-tuple-element.52), channel_id=1, source_target_pairs={{0,1},{1,2},{2,3},{3,0},{4,5},{5,6},{6,7},{7,4},{8,9},{9,10},{10,1... | collective-permute-start | bytes 1179656 | tf_op jit(solution)/shard_map/ppermute | solution.py:39
  131.5 2.7 %collective-permute-start.10 = (bf16[1536,128]{1,0:T(8,128)(2,1)S(1)}, bf16[1536,128]{1,0:T(8,128)(2,1)S(1)}, u32[]{:S(2)}, u32[]{:S(2)}) collective-permute-start(bf16[1536,128]{1,0:T(8,128)(2,1)S(1)} %get-tuple-element.53), channel_id=1, source_target_pairs={{0,3},{1,0},{2,1},{3,2},{4,7},{5,4},{6,5},{7,6},{8,11},{9,8},{10,9... | collective-permute-start | bytes 1179656 | tf_op jit(solution)/shard_map/ppermute | solution.py:39
  136.9 1.9 %collective-permute-done.11.refs_0_ = bf16[1536,128]{1,0:T(8,128)(2,1)S(1)} collective-permute-done((bf16[1536,128]{1,0:T(8,128)(2,1)S(1)}, bf16[1536,128]{1,0:T(8,128)(2,1)S(1)}, u32[]{:S(2)}, u32[]{:S(2)}) %collective-permute-start.11) | collective-permute-done | bytes 393248 | tf_op jit(solution)/shard_map/ppermute | solution.py:39
  139.6 4.3 %collective-permute-done.9.refs_0_ = bf16[1536,128]{1,0:T(8,128)(2,1)S(1)} collective-permute-done((bf16[1536,128]{1,0:T(8,128)(2,1)S(1)}, bf16[1536,128]{1,0:T(8,128)(2,1)S(1)}, u32[]{:S(2)}, u32[]{:S(2)}) %collective-permute-start.9) | collective-permute-done | bytes 393248 | tf_op jit(solution)/shard_map/ppermute | solution.py:39
  143.8 2.1 %collective-permute-done.10.refs_1_ = bf16[1536,128]{1,0:T(8,128)(2,1)S(1)} collective-permute-done((bf16[1536,128]{1,0:T(8,128)(2,1)S(1)}, bf16[1536,128]{1,0:T(8,128)(2,1)S(1)}, u32[]{:S(2)}, u32[]{:S(2)}) %collective-permute-start.10) | collective-permute-done | bytes 393248 | tf_op jit(solution)/shard_map/ppermute | solution.py:39
  148.4 1.2 shard_map.153
  (50 shorter events, 10.4 us)
Async XLA Ops:
  3.3 18.0 %copy-start.2 = (bf16[1,2048,128]{2,1,0:T(8,128)(2,1)S(1)}, bf16[1,2048,128]{2,1,0:T(8,128)(2,1)}, u32[]{:S(2)}) copy-start(bf16[1,2048,128]{2,1,0:T(8,128)(2,1)} %param.13) | copy-start | bytes 1572868
  3.3 18.0 %copy-start.3 = (bf16[1,2048,128]{2,1,0:T(8,128)(2,1)S(1)}, bf16[1,2048,128]{2,1,0:T(8,128)(2,1)}, u32[]{:S(2)}) copy-start(bf16[1,2048,128]{2,1,0:T(8,128)(2,1)} %param.14) | copy-start | bytes 1572868
  3.3 18.0 %copy-start.4 = (bf16[1,128,2048]{2,1,0:T(8,128)(2,1)S(1)}, bf16[1,128,2048]{2,1,0:T(8,128)(2,1)}, u32[]{:S(2)}) copy-start(bf16[1,128,2048]{2,1,0:T(8,128)(2,1)} %param.15) | copy-start | bytes 1572868
  3.4 48.2 %all-to-all-start = ((bf16[128,8,512]{2,1,0:T(8,128)(2,1)}), bf16[128,8,512]{2,1,0:T(8,128)(2,1)S(1)}, u32[]{:S(2)}, u32[]{:S(2)}) async-start(bf16[128,8,512]{2,1,0:T(8,128)(2,1)} %bitcast.30), calls=%async_computation | async-start | bytes 2097152 | tf_op jit(solution)/shard_map/all_to_all | solution.py:46
  21.3 10.4 %copy-start.1 = (bf16[128,2048]{1,0:T(8,128)(2,1)S(1)}, bf16[128,2048]{1,0:T(8,128)(2,1)}, u32[]{:S(2)}) copy-start(bf16[128,2048]{1,0:T(8,128)(2,1)} %cot_ref.3) | copy-start | bytes 1572868
  21.4 10.4 %copy-start.5 = (bf16[2048,128]{1,0:T(8,128)(2,1)S(1)}, bf16[2048,128]{1,0:T(8,128)(2,1)}, u32[]{:S(2)}) copy-start(bf16[2048,128]{1,0:T(8,128)(2,1)} %down_ref.1) | copy-start | bytes 1572868
  21.4 10.4 %copy-start.11 = (bf16[128,128]{1,0:T(8,128)(2,1)S(1)}, bf16[128,128]{1,0:T(8,128)(2,1)}, u32[]{:S(2)}) copy-start(bf16[128,128]{1,0:T(8,128)(2,1)} %hid_ref.1) | copy-start | bytes 98308
  23.1 32.7 %collective-permute-start = (bf16[1536,128]{1,0:T(8,128)(2,1)}, bf16[1536,128]{1,0:T(8,128)(2,1)S(1)}, u32[]{:S(2)}, u32[]{:S(2)}) collective-permute-start(bf16[1536,128]{1,0:T(8,128)(2,1)} %get-tuple-element.40), channel_id=1, source_target_pairs={{0,1},{1,2},{2,3},{3,0},{4,5},{5,6},{6,7},{7,4},{8,9},{9,10},{10,1... | collective-permute-start | bytes 1179656 | tf_op jit(solution)/shard_map/ppermute | solution.py:39
  25.5 30.3 %collective-permute-start.1 = (bf16[1536,128]{1,0:T(8,128)(2,1)}, bf16[1536,128]{1,0:T(8,128)(2,1)S(1)}, u32[]{:S(2)}, u32[]{:S(2)}) collective-permute-start(bf16[1536,128]{1,0:T(8,128)(2,1)} %get-tuple-element.41), channel_id=1, source_target_pairs={{0,2},{1,3},{2,0},{3,1},{4,6},{5,7},{6,4},{7,5},{8,10},{9,11},{10,... | collective-permute-start | bytes 1179656 | tf_op jit(solution)/shard_map/ppermute | solution.py:39
  29.8 26.0 %collective-permute-start.2 = (bf16[1536,128]{1,0:T(8,128)(2,1)S(1)}, bf16[1536,128]{1,0:T(8,128)(2,1)S(1)}, u32[]{:S(2)}, u32[]{:S(2)}) collective-permute-start(bf16[1536,128]{1,0:T(8,128)(2,1)S(1)} %get-tuple-element.42), channel_id=1, source_target_pairs={{0,3},{1,0},{2,1},{3,2},{4,7},{5,4},{6,5},{7,6},{8,11},{9,8},{10,9... | collective-permute-start | bytes 1179656 | tf_op jit(solution)/shard_map/ppermute | solution.py:39
  51.5 43.8 %all-to-all-start.2 = ((bf16[16,128,128]{2,1,0:T(8,128)(2,1)}), bf16[16,128,128]{2,1,0:T(8,128)(2,1)S(1)}, u32[]{:S(2)}, u32[]{:S(2)}) async-start(bf16[16,128,128]{2,1,0:T(8,128)(2,1)} %bitcast.14), calls=%async_computation.2 | async-start | bytes 1048576 | tf_op jit(solution)/shard_map/all_to_all | solution.py:46
  59.3 26.0 %copy-start.6 = (bf16[128,1536]{1,0:T(8,128)(2,1)S(1)}, bf16[128,1536]{1,0:T(8,128)(2,1)}, u32[]{:S(2)}) copy-start(bf16[128,1536]{1,0:T(8,128)(2,1)} %get-tuple-element.45.refs_0_) | copy-start | bytes 1179652
  59.9 13.9 %collective-permute-start.3 = (bf16[128,1536]{1,0:T(8,128)(2,1)S(1)}, bf16[128,1536]{1,0:T(8,128)(2,1)S(1)}, u32[]{:S(2)}, u32[]{:S(2)}) collective-permute-start(bf16[128,1536]{1,0:T(8,128)(2,1)S(1)} %get-tuple-element.46), channel_id=1, source_target_pairs={{0,1},{1,2},{2,3},{3,0},{4,5},{5,6},{6,7},{7,4},{8,9},{9,10},{10,1... | collective-permute-start | bytes 1179656 | tf_op jit(solution)/shard_map/ppermute | solution.py:39
  62.3 15.4 %collective-permute-start.4 = (bf16[128,1536]{1,0:T(8,128)(2,1)S(1)}, bf16[128,1536]{1,0:T(8,128)(2,1)S(1)}, u32[]{:S(2)}, u32[]{:S(2)}) collective-permute-start(bf16[128,1536]{1,0:T(8,128)(2,1)S(1)} %shard_map.149), channel_id=1, source_target_pairs={{0,2},{1,3},{2,0},{3,1},{4,6},{5,7},{6,4},{7,5},{8,10},{9,11},{10,... | collective-permute-start | bytes 1179656 | tf_op jit(solution)/shard_map/ppermute | solution.py:39
  66.7 18.6 %collective-permute-start.5 = (bf16[128,1536]{1,0:T(8,128)(2,1)S(1)}, bf16[128,1536]{1,0:T(8,128)(2,1)S(1)}, u32[]{:S(2)}, u32[]{:S(2)}) collective-permute-start(bf16[128,1536]{1,0:T(8,128)(2,1)S(1)} %get-tuple-element.47), channel_id=1, source_target_pairs={{0,3},{1,0},{2,1},{3,2},{4,7},{5,4},{6,5},{7,6},{8,11},{9,8},{10,9... | collective-permute-start | bytes 1179656 | tf_op jit(solution)/shard_map/ppermute | solution.py:39
  85.7 14.9 %collective-permute-start.6 = (bf16[1552,128]{1,0:T(8,128)(2,1)S(1)}, bf16[1552,128]{1,0:T(8,128)(2,1)S(1)}, u32[]{:S(2)}, u32[]{:S(2)}) collective-permute-start(bf16[1552,128]{1,0:T(8,128)(2,1)S(1)} %shard_map.150.refs_0_), channel_id=1, source_target_pairs={{0,1},{1,2},{2,3},{3,0},{4,5},{5,6},{6,7},{7,4},{8,9},{9,10},{10,1... | collective-permute-start | bytes 1191944 | tf_op jit(solution)/shard_map/ppermute | solution.py:39
  88.2 15.5 %collective-permute-start.7 = (bf16[1552,128]{1,0:T(8,128)(2,1)S(1)}, bf16[1552,128]{1,0:T(8,128)(2,1)S(1)}, u32[]{:S(2)}, u32[]{:S(2)}) collective-permute-start(bf16[1552,128]{1,0:T(8,128)(2,1)S(1)} %shard_map.150.refs_0_), channel_id=1, source_target_pairs={{0,2},{1,3},{2,0},{3,1},{4,6},{5,7},{6,4},{7,5},{8,10},{9,11},{10,... | collective-permute-start | bytes 1191944 | tf_op jit(solution)/shard_map/ppermute | solution.py:39
  92.6 18.1 %collective-permute-start.8 = (bf16[1552,128]{1,0:T(8,128)(2,1)S(1)}, bf16[1552,128]{1,0:T(8,128)(2,1)S(1)}, u32[]{:S(2)}, u32[]{:S(2)}) collective-permute-start(bf16[1552,128]{1,0:T(8,128)(2,1)S(1)} %shard_map.150.refs_0_), channel_id=1, source_target_pairs={{0,3},{1,0},{2,1},{3,2},{4,7},{5,4},{6,5},{7,6},{8,11},{9,8},{10,9... | collective-permute-start | bytes 1191944 | tf_op jit(solution)/shard_map/ppermute | solution.py:39
  96.0 16.5 %all-to-all-start.3 = ((bf16[8,16,128]{2,1,0:T(8,128)(2,1)}), bf16[8,16,128]{2,1,0:T(8,128)(2,1)S(1)}, u32[]{:S(2)}, u32[]{:S(2)}) async-start(bf16[8,16,128]{2,1,0:T(8,128)(2,1)} %bitcast.16), calls=%async_computation.3 | async-start | bytes 65536 | tf_op jit(solution)/shard_map/all_to_all | solution.py:46
  112.4 10.5 %copy-start = (bf16[512,1024]{1,0:T(8,128)(2,1)S(1)}, bf16[512,1024]{1,0:T(8,128)(2,1)}, u32[]{:S(2)}) copy-start(bf16[512,1024]{1,0:T(8,128)(2,1)} %get-tuple-element.51.xg_ref) | copy-start | bytes 3145732
  112.5 0.6 copy-start.9
  113.1 34.7 %all-to-all-start.1 = ((bf16[128,8,384]{2,1,0:T(8,128)(2,1)}), bf16[128,8,384]{2,1,0:T(8,128)(2,1)S(1)}, u32[]{:S(2)}, u32[]{:S(2)}) async-start(bf16[128,8,384]{2,1,0:T(8,128)(2,1)} %bitcast.31), calls=%async_computation.1 | async-start | bytes 1572864 | tf_op jit(solution)/shard_map/all_to_all | solution.py:46
  123.4 11.8 %copy-start.10 = (bf16[8,16,128]{2,1,0:T(8,128)(2,1)S(1)}, bf16[8,16,128]{2,1,0:T(8,128)(2,1)}, u32[]{:S(2)}) copy-start(bf16[8,16,128]{2,1,0:T(8,128)(2,1)} %copy-done.9) | copy-start | bytes 98308
  123.4 15.4 %collective-permute-start.11 = (bf16[1536,128]{1,0:T(8,128)(2,1)S(1)}, bf16[1536,128]{1,0:T(8,128)(2,1)S(1)}, u32[]{:S(2)}, u32[]{:S(2)}) collective-permute-start(bf16[1536,128]{1,0:T(8,128)(2,1)S(1)} %shard_map.155), channel_id=1, source_target_pairs={{0,2},{1,3},{2,0},{3,1},{4,6},{5,7},{6,4},{7,5},{8,10},{9,11},{10,... | collective-permute-start | bytes 1179656 | tf_op jit(solution)/shard_map/ppermute | solution.py:39
  128.4 5.9 %copy-start.13 = (f32[128,2]{0,1:T(2,128)S(1)}, f32[128,2]{0,1:T(2,128)}, u32[]{:S(2)}) copy-start(f32[128,2]{0,1:T(2,128)} %param.11) | copy-start | bytes 3076
  128.4 5.9 %copy-start.12 = (s32[128,2]{0,1:T(2,128)S(1)}, s32[128,2]{0,1:T(2,128)}, u32[]{:S(2)}) copy-start(s32[128,2]{0,1:T(2,128)} %param.12) | copy-start | bytes 3076
  128.4 15.5 %collective-permute-start.9 = (bf16[1536,128]{1,0:T(8,128)(2,1)S(1)}, bf16[1536,128]{1,0:T(8,128)(2,1)S(1)}, u32[]{:S(2)}, u32[]{:S(2)}) collective-permute-start(bf16[1536,128]{1,0:T(8,128)(2,1)S(1)} %get-tuple-element.52), channel_id=1, source_target_pairs={{0,1},{1,2},{2,3},{3,0},{4,5},{5,6},{6,7},{7,4},{8,9},{9,10},{10,1... | collective-permute-start | bytes 1179656 | tf_op jit(solution)/shard_map/ppermute | solution.py:39
  131.5 14.4 %collective-permute-start.10 = (bf16[1536,128]{1,0:T(8,128)(2,1)S(1)}, bf16[1536,128]{1,0:T(8,128)(2,1)S(1)}, u32[]{:S(2)}, u32[]{:S(2)}) collective-permute-start(bf16[1536,128]{1,0:T(8,128)(2,1)S(1)} %get-tuple-element.53), channel_id=1, source_target_pairs={{0,3},{1,0},{2,1},{3,2},{4,7},{5,4},{6,5},{7,6},{8,11},{9,8},{10,9... | collective-permute-start | bytes 1179656 | tf_op jit(solution)/shard_map/ppermute | solution.py:39
  134.5 0.7 copy-start.7
  135.1 0.6 copy-start.14
  146.0 1.8 %copy-start.8 = (bf16[512,128]{1,0:T(8,128)(2,1)S(1)}, bf16[512,128]{1,0:T(8,128)(2,1)}, u32[]{:S(2)}) copy-start(bf16[512,128]{1,0:T(8,128)(2,1)} %copy-done.7) | copy-start | bytes 393220
  147.7 0.7 copy-start.15

commit v6 on v5

--- a/solution.py
+++ b/solution.py
@@ -310,29 +310,32 @@
     parts = len(grads)
     rows = out_ref.shape[0] // (2 * parts)
     blocks = both_ref.shape[1] // LANES
-    whole = jnp.concatenate(
-        [
-            jnp.concatenate([ref[c * rows : (c + 1) * rows, :] for c in range(blocks)], axis=1)
-            for ref in grads
-        ],
-        axis=0,
-    )
-    out = mm(whole, both_ref[...], LAST).astype(BF16)
     order = weave()
-    half = out.shape[1] // 2
+    half = both_ref.shape[0] // 2
     copies = []
-    for k, ref in enumerate(grads):
-        own = out[k * rows : (k + 1) * rows]
-        both = jnp.concatenate([own[:, :half], own[:, half:]], axis=0)
-        place = slice(2 * k * rows, 2 * (k + 1) * rows)
-        out_ref[place, :half] = mm(order, both).astype(BF16)
-        share = ref[ref.shape[0] - PAD :, :].astype(F32)[0:1]
-        share = jnp.sum(jnp.where(diagonal(rows), share, 0.0), axis=1, keepdims=True)
-        share = jnp.broadcast_to(share, (rows, LANES)).astype(BF16)
-        out_ref[place, half:] = mm(order[:, :rows], share).astype(BF16)
-        to = back_out.at[span(at(col, -k, parts), 2 * rows), :]
-        copies.append(pltpu.make_async_copy(out_ref.at[place, :], to, sems.at[k]))
-        copies[-1].start()
+    for first in range(0, parts, 2):
+        pair = grads[first : first + 2]
+        whole = jnp.concatenate(
+            [
+                jnp.concatenate([ref[c * rows : (c + 1) * rows, :] for c in range(blocks)], axis=1)
+                for ref in pair
+            ],
+            axis=0,
+        )
+        out = mm(whole, both_ref[...], LAST).astype(BF16)
+        for n, ref in enumerate(pair):
+            k = first + n
+            own = out[n * rows : (n + 1) * rows]
+            both = jnp.concatenate([own[:, :half], own[:, half:]], axis=0)
+            place = slice(2 * k * rows, 2 * (k + 1) * rows)
+            out_ref[place, :half] = mm(order, both).astype(BF16)
+            share = ref[ref.shape[0] - PAD :, :].astype(F32)[0:1]
+            share = jnp.sum(jnp.where(diagonal(rows), share, 0.0), axis=1, keepdims=True)
+            share = jnp.broadcast_to(share, (rows, LANES)).astype(BF16)
+            out_ref[place, half:] = mm(order[:, :rows], share).astype(BF16)
+            to = back_out.at[span(at(col, -k, parts), 2 * rows), :]
+            copies.append(pltpu.make_async_copy(out_ref.at[place, :], to, sems.at[k]))
+            copies[-1].start()
     for copy in copies:
         copy.wait()
 
@@ -618,9 +621,7 @@
     shared = over(shared.reshape(feat, block), ("y", "core"))
     shared = local(fold_kernel, half(feat // inner, block), shared)
     shared = over(shared, "z")
-    shared_grad = local(
-        total_kernel, jax.ShapeDtypeStruct((feat // ep, block), F32), shared
-    )
+    shared_grad = local(total_kernel, jax.ShapeDtypeStruct((feat // ep, block), F32), shared)
     return (
         tokens_grad,
         weights_grad,

time: 152 us -> 153 us (level)
  no operation moved by 1% of the time
where the time goes in v6:
time: 153 us; the launch traced here: 150 us
  starting transfers between devices  72.4 us (47%)
  waiting for transfers between devices  54.4 us (36%)
  Pallas kernels  20 us (13%)
  local copies, waits for them, and re-layouts  2.01 us (1%)
    ppermute x12, starting transfers between devices, around(): lax.ppermute(part, 'tp', [(i, (i + k + 1) % size) for i in range(size)])  37 us
    all_to_all x4, starting transfers between devices, over(): lax.all_to_all(rows, axes, split_axis=0, concat_axis=0, tiled=True)  35.4 us
    ppermute x12, waiting for transfers between devices, around(): lax.ppermute(part, 'tp', [(i, (i + k + 1) % size) for i in range(size)])  35 us
    pallas_call x18, Pallas kernels, local(): pl.pallas_call(kernel, in_specs=[spec[k] for k in spaces], out_specs=[spe...  20 us
    all_to_all x4, waiting for transfers between devices, over(): lax.all_to_all(rows, axes, split_axis=0, concat_axis=0, tiled=True)  19.4 us
  transfers between devices with their start and end apart: 16, of which 10 were waited for; matrix products, arithmetic and copies ran while one was open for 0% of the time, Pallas kernels for 11%

profile of v6, /device:TPU:6, one launch (start us, length us, event | category | flops | bytes accessed | tf_op | source)
XLA Modules:
  0.0 149.8 jit_solution(9419108744140765432)
XLA Ops:
  0.6 2.7 %shard_map.145 = bf16[1024,512]{1,0:T(8,128)(2,1)} custom-call(s32[1]{0:T(128)} %bitcast.2.col, s32[2,128]{1,0:T(2,128)} %bitcast.26, f32[2,128]{1,0:T(2,128)} %bitcast.28, bf16[128,2048]{1,0:T(8,128)(2,1)} %tok_ref.1, bf16[128,2048]{1,0:T(8,128)(2,1)} %cot_ref.3), custom_call_target="tpu_custom_call" | custom-call | tf_op jit(solution)/shard_map/pallas_call | solution.py:69
  3.4 18.0 %all-to-all-start = ((bf16[128,8,512]{2,1,0:T(8,128)(2,1)}), bf16[128,8,512]{2,1,0:T(8,128)(2,1)S(1)}, u32[]{:S(2)}, u32[]{:S(2)}) async-start(bf16[128,8,512]{2,1,0:T(8,128)(2,1)} %bitcast.30), calls=%async_computation | async-start | bytes 2097152 | tf_op jit(solution)/shard_map/all_to_all | solution.py:46
  21.4 1.7 %shard_map.146 = (bf16[1536,128]{1,0:T(8,128)(2,1)}, bf16[1536,128]{1,0:T(8,128)(2,1)}, bf16[1536,128]{1,0:T(8,128)(2,1)}, bf16[1536,128]{1,0:T(8,128)(2,1)S(1)}) custom-call(s32[1]{0:T(128)} %bitcast.2.col, bf16[2048,128]{1,0:T(8,128)(2,1)S(1)} %bitcast.22, bf16[2048,128]{1,0:T(8,128)(2,1)S(1)} %bitcast.23, bf16[128,2048]{1,0:T(8,128)(2,1)S(1)} %bitcast.24), custom_call_target="tpu_custom_call" | custom-call | tf_op jit(solution)/shard_map/pallas_call | solution.py:69
  23.1 2.4 %collective-permute-start = (bf16[1536,128]{1,0:T(8,128)(2,1)}, bf16[1536,128]{1,0:T(8,128)(2,1)S(1)}, u32[]{:S(2)}, u32[]{:S(2)}) collective-permute-start(bf16[1536,128]{1,0:T(8,128)(2,1)} %get-tuple-element.40), channel_id=1, source_target_pairs={{0,1},{1,2},{2,3},{3,0},{4,5},{5,6},{6,7},{7,4},{8,9},{9,10},{10,1... | collective-permute-start | bytes 1179656 | tf_op jit(solution)/shard_map/ppermute | solution.py:39
  25.5 4.3 %collective-permute-start.1 = (bf16[1536,128]{1,0:T(8,128)(2,1)}, bf16[1536,128]{1,0:T(8,128)(2,1)S(1)}, u32[]{:S(2)}, u32[]{:S(2)}) collective-permute-start(bf16[1536,128]{1,0:T(8,128)(2,1)} %get-tuple-element.41), channel_id=1, source_target_pairs={{0,2},{1,3},{2,0},{3,1},{4,6},{5,7},{6,4},{7,5},{8,10},{9,11},{10,... | collective-permute-start | bytes 1179656 | tf_op jit(solution)/shard_map/ppermute | solution.py:39
  29.8 1.9 %collective-permute-start.2 = (bf16[1536,128]{1,0:T(8,128)(2,1)S(1)}, bf16[1536,128]{1,0:T(8,128)(2,1)S(1)}, u32[]{:S(2)}, u32[]{:S(2)}) collective-permute-start(bf16[1536,128]{1,0:T(8,128)(2,1)S(1)} %get-tuple-element.42), channel_id=1, source_target_pairs={{0,3},{1,0},{2,1},{3,2},{4,7},{5,4},{6,5},{7,6},{8,11},{9,8},{10,9... | collective-permute-start | bytes 1179656 | tf_op jit(solution)/shard_map/ppermute | solution.py:39
  31.7 1.2 shard_map.159
  33.0 18.6 %all-to-all-done = bf16[128,8,512]{2,1,0:T(8,128)(2,1)S(1)} async-done(((bf16[128,8,512]{2,1,0:T(8,128)(2,1)}), bf16[128,8,512]{2,1,0:T(8,128)(2,1)S(1)}, u32[]{:S(2)}, u32[]{:S(2)}) %all-to-all-start) | async-done | bytes 1048608 | tf_op jit(solution)/shard_map/all_to_all | solution.py:46
  51.5 4.2 %all-to-all-start.2 = ((bf16[16,128,128]{2,1,0:T(8,128)(2,1)}), bf16[16,128,128]{2,1,0:T(8,128)(2,1)S(1)}, u32[]{:S(2)}, u32[]{:S(2)}) async-start(bf16[16,128,128]{2,1,0:T(8,128)(2,1)} %bitcast.14), calls=%async_computation.2 | async-start | bytes 1048576 | tf_op jit(solution)/shard_map/all_to_all | solution.py:46
  56.9 2.4 %shard_map.148 = (bf16[512,1024]{1,0:T(8,128)(2,1)}, bf16[128,1536]{1,0:T(8,128)(2,1)}, bf16[512,1024]{1,0:T(8,128)(2,1)}, bf16[128,1536]{1,0:T(8,128)(2,1)S(1)}, bf16[128,1536]{1,0:T(8,128)(2,1)S(1)}) custom-call(s32[1]{0:T(128)} %bitcast.2.col, bf16[1024,512]{1,0:T(8,128)(2,1)S(1)} %bitcast.18, bf16[512,1024]{1,0:T(8,128)(2,1)S(1)} %get-tuple-element.43.both_ref, ...), custom_call_target="tpu_custom_call" | custom-call | tf_op jit(solution)/shard_map/pallas_call | solution.py:69
  59.9 2.4 %collective-permute-start.3 = (bf16[128,1536]{1,0:T(8,128)(2,1)S(1)}, bf16[128,1536]{1,0:T(8,128)(2,1)S(1)}, u32[]{:S(2)}, u32[]{:S(2)}) collective-permute-start(bf16[128,1536]{1,0:T(8,128)(2,1)S(1)} %get-tuple-element.46), channel_id=1, source_target_pairs={{0,1},{1,2},{2,3},{3,0},{4,5},{5,6},{6,7},{7,4},{8,9},{9,10},{10,1... | collective-permute-start | bytes 1179656 | tf_op jit(solution)/shard_map/ppermute | solution.py:39
  62.3 4.3 %collective-permute-start.4 = (bf16[128,1536]{1,0:T(8,128)(2,1)S(1)}, bf16[128,1536]{1,0:T(8,128)(2,1)S(1)}, u32[]{:S(2)}, u32[]{:S(2)}) collective-permute-start(bf16[128,1536]{1,0:T(8,128)(2,1)S(1)} %shard_map.149), channel_id=1, source_target_pairs={{0,2},{1,3},{2,0},{3,1},{4,6},{5,7},{6,4},{7,5},{8,10},{9,11},{10,... | collective-permute-start | bytes 1179656 | tf_op jit(solution)/shard_map/ppermute | solution.py:39
  66.7 1.9 %collective-permute-start.5 = (bf16[128,1536]{1,0:T(8,128)(2,1)S(1)}, bf16[128,1536]{1,0:T(8,128)(2,1)S(1)}, u32[]{:S(2)}, u32[]{:S(2)}) collective-permute-start(bf16[128,1536]{1,0:T(8,128)(2,1)S(1)} %get-tuple-element.47), channel_id=1, source_target_pairs={{0,3},{1,0},{2,1},{3,2},{4,7},{5,4},{6,5},{7,6},{8,11},{9,8},{10,9... | collective-permute-start | bytes 1179656 | tf_op jit(solution)/shard_map/ppermute | solution.py:39
  68.6 5.2 %collective-permute-done.3.refs_1_ = bf16[128,1536]{1,0:T(8,128)(2,1)S(1)} collective-permute-done((bf16[128,1536]{1,0:T(8,128)(2,1)S(1)}, bf16[128,1536]{1,0:T(8,128)(2,1)S(1)}, u32[]{:S(2)}, u32[]{:S(2)}) %collective-permute-start.3) | collective-permute-done | bytes 393248 | tf_op jit(solution)/shard_map/ppermute | solution.py:39
  73.8 3.9 %collective-permute-done.4.refs_2_ = bf16[128,1536]{1,0:T(8,128)(2,1)S(1)} collective-permute-done((bf16[128,1536]{1,0:T(8,128)(2,1)S(1)}, bf16[128,1536]{1,0:T(8,128)(2,1)S(1)}, u32[]{:S(2)}, u32[]{:S(2)}) %collective-permute-start.4) | collective-permute-done | bytes 393248 | tf_op jit(solution)/shard_map/ppermute | solution.py:39
  77.7 7.5 %collective-permute-done.5.refs_3_ = bf16[128,1536]{1,0:T(8,128)(2,1)S(1)} collective-permute-done((bf16[128,1536]{1,0:T(8,128)(2,1)S(1)}, bf16[128,1536]{1,0:T(8,128)(2,1)S(1)}, u32[]{:S(2)}, u32[]{:S(2)}) %collective-permute-start.5) | collective-permute-done | bytes 393248 | tf_op jit(solution)/shard_map/ppermute | solution.py:39
  85.7 2.5 %collective-permute-start.6 = (bf16[1552,128]{1,0:T(8,128)(2,1)S(1)}, bf16[1552,128]{1,0:T(8,128)(2,1)S(1)}, u32[]{:S(2)}, u32[]{:S(2)}) collective-permute-start(bf16[1552,128]{1,0:T(8,128)(2,1)S(1)} %shard_map.150.refs_0_), channel_id=1, source_target_pairs={{0,1},{1,2},{2,3},{3,0},{4,5},{5,6},{6,7},{7,4},{8,9},{9,10},{10,1... | collective-permute-start | bytes 1191944 | tf_op jit(solution)/shard_map/ppermute | solution.py:39
  88.2 4.3 %collective-permute-start.7 = (bf16[1552,128]{1,0:T(8,128)(2,1)S(1)}, bf16[1552,128]{1,0:T(8,128)(2,1)S(1)}, u32[]{:S(2)}, u32[]{:S(2)}) collective-permute-start(bf16[1552,128]{1,0:T(8,128)(2,1)S(1)} %shard_map.150.refs_0_), channel_id=1, source_target_pairs={{0,2},{1,3},{2,0},{3,1},{4,6},{5,7},{6,4},{7,5},{8,10},{9,11},{10,... | collective-permute-start | bytes 1191944 | tf_op jit(solution)/shard_map/ppermute | solution.py:39
  92.6 2.7 %collective-permute-start.8 = (bf16[1552,128]{1,0:T(8,128)(2,1)S(1)}, bf16[1552,128]{1,0:T(8,128)(2,1)S(1)}, u32[]{:S(2)}, u32[]{:S(2)}) collective-permute-start(bf16[1552,128]{1,0:T(8,128)(2,1)S(1)} %shard_map.150.refs_0_), channel_id=1, source_target_pairs={{0,3},{1,0},{2,1},{3,2},{4,7},{5,4},{6,5},{7,6},{8,11},{9,8},{10,9... | collective-permute-start | bytes 1191944 | tf_op jit(solution)/shard_map/ppermute | solution.py:39
  96.0 3.3 %all-to-all-start.3 = ((bf16[8,16,128]{2,1,0:T(8,128)(2,1)}), bf16[8,16,128]{2,1,0:T(8,128)(2,1)S(1)}, u32[]{:S(2)}, u32[]{:S(2)}) async-start(bf16[8,16,128]{2,1,0:T(8,128)(2,1)} %bitcast.16), calls=%async_computation.3 | async-start | bytes 65536 | tf_op jit(solution)/shard_map/all_to_all | solution.py:46
  99.3 1.2 shard_map.151.refs_4_
  100.6 3.1 %collective-permute-done.7.refs_2_ = bf16[1552,128]{1,0:T(8,128)(2,1)S(1)} collective-permute-done((bf16[1552,128]{1,0:T(8,128)(2,1)S(1)}, bf16[1552,128]{1,0:T(8,128)(2,1)S(1)}, u32[]{:S(2)}, u32[]{:S(2)}) %collective-permute-start.7) | collective-permute-done | bytes 397344 | tf_op jit(solution)/shard_map/ppermute | solution.py:39
  103.7 6.9 %collective-permute-done.8.refs_3_ = bf16[1552,128]{1,0:T(8,128)(2,1)S(1)} collective-permute-done((bf16[1552,128]{1,0:T(8,128)(2,1)S(1)}, bf16[1552,128]{1,0:T(8,128)(2,1)S(1)}, u32[]{:S(2)}, u32[]{:S(2)}) %collective-permute-start.8) | collective-permute-done | bytes 397344 | tf_op jit(solution)/shard_map/ppermute | solution.py:39
  110.7 1.9 %shard_map.152 = bf16[1024,384]{1,0:T(8,128)(2,1)} custom-call(s32[1]{0:T(128)} %bitcast.2.col, bf16[1552,128]{1,0:T(8,128)(2,1)S(1)} %shard_map.150.refs_0_, bf16[1552,128]{1,0:T(8,128)(2,1)S(1)} %collective-permute-done.6.refs_1_, bf16[1552,128]{1,0:T(8,128)(2,1)S(1)} %collective-permute-done.7.refs_2_, ...), custom_call_target="tpu_custom_call" | custom-call | tf_op jit(solution)/shard_map/pallas_call | solution.py:69
  113.3 9.9 %all-to-all-start.1 = ((bf16[128,8,384]{2,1,0:T(8,128)(2,1)}), bf16[128,8,384]{2,1,0:T(8,128)(2,1)S(1)}, u32[]{:S(2)}, u32[]{:S(2)}) async-start(bf16[128,8,384]{2,1,0:T(8,128)(2,1)} %bitcast.31), calls=%async_computation.1 | async-start | bytes 1572864 | tf_op jit(solution)/shard_map/all_to_all | solution.py:46
  123.6 4.3 %collective-permute-start.11 = (bf16[1536,128]{1,0:T(8,128)(2,1)S(1)}, bf16[1536,128]{1,0:T(8,128)(2,1)S(1)}, u32[]{:S(2)}, u32[]{:S(2)}) collective-permute-start(bf16[1536,128]{1,0:T(8,128)(2,1)S(1)} %shard_map.155), channel_id=1, source_target_pairs={{0,2},{1,3},{2,0},{3,1},{4,6},{5,7},{6,4},{7,5},{8,10},{9,11},{10,... | collective-permute-start | bytes 1179656 | tf_op jit(solution)/shard_map/ppermute | solution.py:39
  128.6 3.1 %collective-permute-start.9 = (bf16[1536,128]{1,0:T(8,128)(2,1)S(1)}, bf16[1536,128]{1,0:T(8,128)(2,1)S(1)}, u32[]{:S(2)}, u32[]{:S(2)}) collective-permute-start(bf16[1536,128]{1,0:T(8,128)(2,1)S(1)} %get-tuple-element.52), channel_id=1, source_target_pairs={{0,1},{1,2},{2,3},{3,0},{4,5},{5,6},{6,7},{7,4},{8,9},{9,10},{10,1... | collective-permute-start | bytes 1179656 | tf_op jit(solution)/shard_map/ppermute | solution.py:39
  131.7 2.7 %collective-permute-start.10 = (bf16[1536,128]{1,0:T(8,128)(2,1)S(1)}, bf16[1536,128]{1,0:T(8,128)(2,1)S(1)}, u32[]{:S(2)}, u32[]{:S(2)}) collective-permute-start(bf16[1536,128]{1,0:T(8,128)(2,1)S(1)} %get-tuple-element.53), channel_id=1, source_target_pairs={{0,3},{1,0},{2,1},{3,2},{4,7},{5,4},{6,5},{7,6},{8,11},{9,8},{10,9... | collective-permute-start | bytes 1179656 | tf_op jit(solution)/shard_map/ppermute | solution.py:39
  137.1 1.8 %collective-permute-done.11.refs_0_ = bf16[1536,128]{1,0:T(8,128)(2,1)S(1)} collective-permute-done((bf16[1536,128]{1,0:T(8,128)(2,1)S(1)}, bf16[1536,128]{1,0:T(8,128)(2,1)S(1)}, u32[]{:S(2)}, u32[]{:S(2)}) %collective-permute-start.11) | collective-permute-done | bytes 393248 | tf_op jit(solution)/shard_map/ppermute | solution.py:39
  139.8 4.3 %collective-permute-done.9.refs_0_ = bf16[1536,128]{1,0:T(8,128)(2,1)S(1)} collective-permute-done((bf16[1536,128]{1,0:T(8,128)(2,1)S(1)}, bf16[1536,128]{1,0:T(8,128)(2,1)S(1)}, u32[]{:S(2)}, u32[]{:S(2)}) %collective-permute-start.9) | collective-permute-done | bytes 393248 | tf_op jit(solution)/shard_map/ppermute | solution.py:39
  144.0 2.1 %collective-permute-done.10.refs_1_ = bf16[1536,128]{1,0:T(8,128)(2,1)S(1)} collective-permute-done((bf16[1536,128]{1,0:T(8,128)(2,1)S(1)}, bf16[1536,128]{1,0:T(8,128)(2,1)S(1)}, u32[]{:S(2)}, u32[]{:S(2)}) %collective-permute-start.10) | collective-permute-done | bytes 393248 | tf_op jit(solution)/shard_map/ppermute | solution.py:39
  148.6 1.2 shard_map.153
  (50 shorter events, 10.4 us)
Async XLA Ops:
  3.3 18.0 %copy-start.2 = (bf16[1,2048,128]{2,1,0:T(8,128)(2,1)S(1)}, bf16[1,2048,128]{2,1,0:T(8,128)(2,1)}, u32[]{:S(2)}) copy-start(bf16[1,2048,128]{2,1,0:T(8,128)(2,1)} %param.13) | copy-start | bytes 1572868
  3.3 18.0 %copy-start.3 = (bf16[1,2048,128]{2,1,0:T(8,128)(2,1)S(1)}, bf16[1,2048,128]{2,1,0:T(8,128)(2,1)}, u32[]{:S(2)}) copy-start(bf16[1,2048,128]{2,1,0:T(8,128)(2,1)} %param.14) | copy-start | bytes 1572868
  3.3 18.0 %copy-start.4 = (bf16[1,128,2048]{2,1,0:T(8,128)(2,1)S(1)}, bf16[1,128,2048]{2,1,0:T(8,128)(2,1)}, u32[]{:S(2)}) copy-start(bf16[1,128,2048]{2,1,0:T(8,128)(2,1)} %param.15) | copy-start | bytes 1572868
  3.4 48.2 %all-to-all-start = ((bf16[128,8,512]{2,1,0:T(8,128)(2,1)}), bf16[128,8,512]{2,1,0:T(8,128)(2,1)S(1)}, u32[]{:S(2)}, u32[]{:S(2)}) async-start(bf16[128,8,512]{2,1,0:T(8,128)(2,1)} %bitcast.30), calls=%async_computation | async-start | bytes 2097152 | tf_op jit(solution)/shard_map/all_to_all | solution.py:46
  21.3 10.4 %copy-start.1 = (bf16[128,2048]{1,0:T(8,128)(2,1)S(1)}, bf16[128,2048]{1,0:T(8,128)(2,1)}, u32[]{:S(2)}) copy-start(bf16[128,2048]{1,0:T(8,128)(2,1)} %cot_ref.3) | copy-start | bytes 1572868
  21.4 10.4 %copy-start.5 = (bf16[2048,128]{1,0:T(8,128)(2,1)S(1)}, bf16[2048,128]{1,0:T(8,128)(2,1)}, u32[]{:S(2)}) copy-start(bf16[2048,128]{1,0:T(8,128)(2,1)} %down_ref.1) | copy-start | bytes 1572868
  21.4 10.4 %copy-start.11 = (bf16[128,128]{1,0:T(8,128)(2,1)S(1)}, bf16[128,128]{1,0:T(8,128)(2,1)}, u32[]{:S(2)}) copy-start(bf16[128,128]{1,0:T(8,128)(2,1)} %hid_ref.1) | copy-start | bytes 98308
  23.1 32.7 %collective-permute-start = (bf16[1536,128]{1,0:T(8,128)(2,1)}, bf16[1536,128]{1,0:T(8,128)(2,1)S(1)}, u32[]{:S(2)}, u32[]{:S(2)}) collective-permute-start(bf16[1536,128]{1,0:T(8,128)(2,1)} %get-tuple-element.40), channel_id=1, source_target_pairs={{0,1},{1,2},{2,3},{3,0},{4,5},{5,6},{6,7},{7,4},{8,9},{9,10},{10,1... | collective-permute-start | bytes 1179656 | tf_op jit(solution)/shard_map/ppermute | solution.py:39
  25.5 30.3 %collective-permute-start.1 = (bf16[1536,128]{1,0:T(8,128)(2,1)}, bf16[1536,128]{1,0:T(8,128)(2,1)S(1)}, u32[]{:S(2)}, u32[]{:S(2)}) collective-permute-start(bf16[1536,128]{1,0:T(8,128)(2,1)} %get-tuple-element.41), channel_id=1, source_target_pairs={{0,2},{1,3},{2,0},{3,1},{4,6},{5,7},{6,4},{7,5},{8,10},{9,11},{10,... | collective-permute-start | bytes 1179656 | tf_op jit(solution)/shard_map/ppermute | solution.py:39
  29.8 26.0 %collective-permute-start.2 = (bf16[1536,128]{1,0:T(8,128)(2,1)S(1)}, bf16[1536,128]{1,0:T(8,128)(2,1)S(1)}, u32[]{:S(2)}, u32[]{:S(2)}) collective-permute-start(bf16[1536,128]{1,0:T(8,128)(2,1)S(1)} %get-tuple-element.42), channel_id=1, source_target_pairs={{0,3},{1,0},{2,1},{3,2},{4,7},{5,4},{6,5},{7,6},{8,11},{9,8},{10,9... | collective-permute-start | bytes 1179656 | tf_op jit(solution)/shard_map/ppermute | solution.py:39
  51.5 43.8 %all-to-all-start.2 = ((bf16[16,128,128]{2,1,0:T(8,128)(2,1)}), bf16[16,128,128]{2,1,0:T(8,128)(2,1)S(1)}, u32[]{:S(2)}, u32[]{:S(2)}) async-start(bf16[16,128,128]{2,1,0:T(8,128)(2,1)} %bitcast.14), calls=%async_computation.2 | async-start | bytes 1048576 | tf_op jit(solution)/shard_map/all_to_all | solution.py:46
  59.3 26.0 %copy-start.6 = (bf16[128,1536]{1,0:T(8,128)(2,1)S(1)}, bf16[128,1536]{1,0:T(8,128)(2,1)}, u32[]{:S(2)}) copy-start(bf16[128,1536]{1,0:T(8,128)(2,1)} %get-tuple-element.45.refs_0_) | copy-start | bytes 1179652
  59.9 13.9 %collective-permute-start.3 = (bf16[128,1536]{1,0:T(8,128)(2,1)S(1)}, bf16[128,1536]{1,0:T(8,128)(2,1)S(1)}, u32[]{:S(2)}, u32[]{:S(2)}) collective-permute-start(bf16[128,1536]{1,0:T(8,128)(2,1)S(1)} %get-tuple-element.46), channel_id=1, source_target_pairs={{0,1},{1,2},{2,3},{3,0},{4,5},{5,6},{6,7},{7,4},{8,9},{9,10},{10,1... | collective-permute-start | bytes 1179656 | tf_op jit(solution)/shard_map/ppermute | solution.py:39
  62.3 15.4 %collective-permute-start.4 = (bf16[128,1536]{1,0:T(8,128)(2,1)S(1)}, bf16[128,1536]{1,0:T(8,128)(2,1)S(1)}, u32[]{:S(2)}, u32[]{:S(2)}) collective-permute-start(bf16[128,1536]{1,0:T(8,128)(2,1)S(1)} %shard_map.149), channel_id=1, source_target_pairs={{0,2},{1,3},{2,0},{3,1},{4,6},{5,7},{6,4},{7,5},{8,10},{9,11},{10,... | collective-permute-start | bytes 1179656 | tf_op jit(solution)/shard_map/ppermute | solution.py:39
  66.7 18.6 %collective-permute-start.5 = (bf16[128,1536]{1,0:T(8,128)(2,1)S(1)}, bf16[128,1536]{1,0:T(8,128)(2,1)S(1)}, u32[]{:S(2)}, u32[]{:S(2)}) collective-permute-start(bf16[128,1536]{1,0:T(8,128)(2,1)S(1)} %get-tuple-element.47), channel_id=1, source_target_pairs={{0,3},{1,0},{2,1},{3,2},{4,7},{5,4},{6,5},{7,6},{8,11},{9,8},{10,9... | collective-permute-start | bytes 1179656 | tf_op jit(solution)/shard_map/ppermute | solution.py:39
  85.7 14.9 %collective-permute-start.6 = (bf16[1552,128]{1,0:T(8,128)(2,1)S(1)}, bf16[1552,128]{1,0:T(8,128)(2,1)S(1)}, u32[]{:S(2)}, u32[]{:S(2)}) collective-permute-start(bf16[1552,128]{1,0:T(8,128)(2,1)S(1)} %shard_map.150.refs_0_), channel_id=1, source_target_pairs={{0,1},{1,2},{2,3},{3,0},{4,5},{5,6},{6,7},{7,4},{8,9},{9,10},{10,1... | collective-permute-start | bytes 1191944 | tf_op jit(solution)/shard_map/ppermute | solution.py:39
  88.2 15.5 %collective-permute-start.7 = (bf16[1552,128]{1,0:T(8,128)(2,1)S(1)}, bf16[1552,128]{1,0:T(8,128)(2,1)S(1)}, u32[]{:S(2)}, u32[]{:S(2)}) collective-permute-start(bf16[1552,128]{1,0:T(8,128)(2,1)S(1)} %shard_map.150.refs_0_), channel_id=1, source_target_pairs={{0,2},{1,3},{2,0},{3,1},{4,6},{5,7},{6,4},{7,5},{8,10},{9,11},{10,... | collective-permute-start | bytes 1191944 | tf_op jit(solution)/shard_map/ppermute | solution.py:39
  92.6 18.1 %collective-permute-start.8 = (bf16[1552,128]{1,0:T(8,128)(2,1)S(1)}, bf16[1552,128]{1,0:T(8,128)(2,1)S(1)}, u32[]{:S(2)}, u32[]{:S(2)}) collective-permute-start(bf16[1552,128]{1,0:T(8,128)(2,1)S(1)} %shard_map.150.refs_0_), channel_id=1, source_target_pairs={{0,3},{1,0},{2,1},{3,2},{4,7},{5,4},{6,5},{7,6},{8,11},{9,8},{10,9... | collective-permute-start | bytes 1191944 | tf_op jit(solution)/shard_map/ppermute | solution.py:39
  96.0 16.6 %all-to-all-start.3 = ((bf16[8,16,128]{2,1,0:T(8,128)(2,1)}), bf16[8,16,128]{2,1,0:T(8,128)(2,1)S(1)}, u32[]{:S(2)}, u32[]{:S(2)}) async-start(bf16[8,16,128]{2,1,0:T(8,128)(2,1)} %bitcast.16), calls=%async_computation.3 | async-start | bytes 65536 | tf_op jit(solution)/shard_map/all_to_all | solution.py:46
  112.6 10.5 %copy-start = (bf16[512,1024]{1,0:T(8,128)(2,1)S(1)}, bf16[512,1024]{1,0:T(8,128)(2,1)}, u32[]{:S(2)}) copy-start(bf16[512,1024]{1,0:T(8,128)(2,1)} %get-tuple-element.51.xg_ref) | copy-start | bytes 3145732
  112.6 0.6 copy-start.9
  113.3 34.7 %all-to-all-start.1 = ((bf16[128,8,384]{2,1,0:T(8,128)(2,1)}), bf16[128,8,384]{2,1,0:T(8,128)(2,1)S(1)}, u32[]{:S(2)}, u32[]{:S(2)}) async-start(bf16[128,8,384]{2,1,0:T(8,128)(2,1)} %bitcast.31), calls=%async_computation.1 | async-start | bytes 1572864 | tf_op jit(solution)/shard_map/all_to_all | solution.py:46
  123.6 11.8 %copy-start.10 = (bf16[8,16,128]{2,1,0:T(8,128)(2,1)S(1)}, bf16[8,16,128]{2,1,0:T(8,128)(2,1)}, u32[]{:S(2)}) copy-start(bf16[8,16,128]{2,1,0:T(8,128)(2,1)} %copy-done.9) | copy-start | bytes 98308
  123.6 15.4 %collective-permute-start.11 = (bf16[1536,128]{1,0:T(8,128)(2,1)S(1)}, bf16[1536,128]{1,0:T(8,128)(2,1)S(1)}, u32[]{:S(2)}, u32[]{:S(2)}) collective-permute-start(bf16[1536,128]{1,0:T(8,128)(2,1)S(1)} %shard_map.155), channel_id=1, source_target_pairs={{0,2},{1,3},{2,0},{3,1},{4,6},{5,7},{6,4},{7,5},{8,10},{9,11},{10,... | collective-permute-start | bytes 1179656 | tf_op jit(solution)/shard_map/ppermute | solution.py:39
  128.6 5.9 %copy-start.13 = (f32[128,2]{0,1:T(2,128)S(1)}, f32[128,2]{0,1:T(2,128)}, u32[]{:S(2)}) copy-start(f32[128,2]{0,1:T(2,128)} %param.11) | copy-start | bytes 3076
  128.6 5.9 %copy-start.12 = (s32[128,2]{0,1:T(2,128)S(1)}, s32[128,2]{0,1:T(2,128)}, u32[]{:S(2)}) copy-start(s32[128,2]{0,1:T(2,128)} %param.12) | copy-start | bytes 3076
  128.6 15.5 %collective-permute-start.9 = (bf16[1536,128]{1,0:T(8,128)(2,1)S(1)}, bf16[1536,128]{1,0:T(8,128)(2,1)S(1)}, u32[]{:S(2)}, u32[]{:S(2)}) collective-permute-start(bf16[1536,128]{1,0:T(8,128)(2,1)S(1)} %get-tuple-element.52), channel_id=1, source_target_pairs={{0,1},{1,2},{2,3},{3,0},{4,5},{5,6},{6,7},{7,4},{8,9},{9,10},{10,1... | collective-permute-start | bytes 1179656 | tf_op jit(solution)/shard_map/ppermute | solution.py:39
  131.7 14.4 %collective-permute-start.10 = (bf16[1536,128]{1,0:T(8,128)(2,1)S(1)}, bf16[1536,128]{1,0:T(8,128)(2,1)S(1)}, u32[]{:S(2)}, u32[]{:S(2)}) collective-permute-start(bf16[1536,128]{1,0:T(8,128)(2,1)S(1)} %get-tuple-element.53), channel_id=1, source_target_pairs={{0,3},{1,0},{2,1},{3,2},{4,7},{5,4},{6,5},{7,6},{8,11},{9,8},{10,9... | collective-permute-start | bytes 1179656 | tf_op jit(solution)/shard_map/ppermute | solution.py:39
  134.7 0.7 copy-start.7
  135.3 0.6 copy-start.14
  146.2 1.8 %copy-start.8 = (bf16[512,128]{1,0:T(8,128)(2,1)S(1)}, bf16[512,128]{1,0:T(8,128)(2,1)}, u32[]{:S(2)}) copy-start(bf16[512,128]{1,0:T(8,128)(2,1)} %copy-done.7) | copy-start | bytes 393220
  147.9 0.7 copy-start.15
